TPU v7x, 512 devices: a whole 4x4x16 slice. The times are simulated.
512 devices in a mesh: sp: 128 (over z, x, core), tp: 4 (over y).
Axes of the slice: x: 4, y: 4, z: 16, core: 2. Of those that a mesh axis runs over, the one named last changes fastest.
Arguments:
- tokens: bfloat16 [32768, 2048], P('sp'), may hold values from -6 to 6
- documents: int32 [32768], P('sp'), may hold values from 0 to 63, never falling along the last dimension, each value on 1 to 1024 neighbouring positions
- norm_gain: float32 [1, 2048], replicated, may hold values from 0.1 to 1.9
- w_query: bfloat16 [1, 2048, 2048], P(None, 'sp', 'tp'), may hold values from -0.125 to 0.125
- w_key: bfloat16 [1, 2048, 2048], P(None, 'sp', 'tp'), may hold values from -0.125 to 0.125
- w_value: bfloat16 [1, 2048, 2048], P(None, 'sp', 'tp'), may hold values from -0.125 to 0.125
- w_out: bfloat16 [1, 2048, 2048], P(None, None, 'sp'), may hold values from -0.59765625 to 0.59765625
- rel_bias: float32 [1, 32, 257], P(None, 'tp'), may hold values from -8 to 240
Outputs:
- mixed: bfloat16 [32768, 2048], P('sp')
Inputs may be any that keep to these rules, and one draw needn't show every extreme that they name: `documents`: document numbers never fall along the sequence; a document has 1 to 1024 positions.
All inputs are finite; a program needn't handle non-finite values.
Results may differ from a plain program's by a relative error of at most 0.007.
Values may be sent and summed in bfloat16 or wider, within the bound.
No kernel may reach another device: no remote copies, remote signals or barrier semaphores. Data moves between devices by JAX's collectives and lax.ppermute only.
A program may use at most 128 MiB of HBM per device.

v0:
```python
import jax
import jax.numpy as jnp
from jax import lax
from jax.sharding import Mesh
from jax.sharding import PartitionSpec as P

HEAD_DIM = 64
SEG = 64
LEFT = 4
REL_CLIP = 128
SP = ("sp_0", "sp_1", "sp_2")


EPS = 1e-06


def passed_along(x, axis, by):
    length = lax.axis_size(axis)
    pairs = [(i, i + by) for i in range(length) if 0 <= i + by < length]
    return lax.ppermute(x, axis, pairs)


def in_one_piece(arrays, axis, dim, along):
    ends, at = ([], 0)
    for a in arrays[:-1]:
        at += a.shape[along]
        ends.append(at)
    both = jnp.concatenate(arrays, axis=along)
    return tuple(jnp.split(lax.all_gather(both, axis, axis=dim, tiled=True), ends, axis=along))


def laid_out(pieces, dim):
    shape = list(pieces.shape[1:])
    shape[dim] *= pieces.shape[0]
    return jnp.moveaxis(pieces, 0, dim).reshape(shape)


def from_everyone(x, axis):
    length = lax.axis_size(axis)
    return lax.all_to_all(jnp.broadcast_to(x[None], (length, *x.shape)), axis, 0, 0, tiled=True)


def collect(x, axis, dim):
    return laid_out(from_everyone(x, axis), dim)


def gather_in_order(x, axes, order):
    pieces = x[None]
    for k in order:
        pieces = lax.all_gather(pieces, axes[k], axis=0, tiled=True)
    held = [lax.axis_size(axes[k]) for k in reversed(order)]
    pieces = pieces.reshape(*held, *x.shape)
    turned = sorted(range(len(order)), key=lambda place: order[len(order) - 1 - place])
    return pieces.transpose(*turned, *range(len(order), pieces.ndim)).reshape(-1, *x.shape)


def gather_axes(x, axes, order, dim):
    return laid_out(gather_in_order(x, axes, order), dim)


def banded_bias(bias_table, query_rows, key_rows, reach_rows):
    span_len = query_rows + key_rows - 1
    steps_back = jnp.arange(span_len, dtype=jnp.int32) - (key_rows - 1) + reach_rows
    lookup = jnp.clip(steps_back, -REL_CLIP, REL_CLIP) + REL_CLIP
    bias_line = jnp.take(bias_table, lookup, axis=1)
    reversed_line = bias_line[:, ::-1]
    repeated = jnp.tile(reversed_line, (1, query_rows))
    skewed = repeated[:, query_rows - 1 : query_rows - 1 + query_rows * (span_len - 1)]
    skewed = skewed.reshape(bias_table.shape[0], query_rows, span_len - 1)
    return skewed[:, :, :key_rows]


def attend(queries, keys_all, values_all, query_pos, key_pos, query_doc, key_doc, bias_table):
    query_rows = queries.shape[0]
    key_rows = keys_all.shape[0]
    reach_rows = key_rows - query_rows
    scores = jnp.einsum(
        "qhe,khe->hqk", queries, keys_all, preferred_element_type=jnp.float32
    ) * HEAD_DIM ** (-0.5)
    scores = scores + banded_bias(bias_table, query_rows, key_rows, reach_rows)
    query_seg = query_pos // SEG
    key_seg = key_pos // SEG
    allowed = (
        (key_pos[None, :] >= 0)
        & (key_seg[None, :] <= query_seg[:, None])
        & (key_seg[None, :] >= query_seg[:, None] - LEFT)
        & (key_doc[None, :] == query_doc[:, None])
    )
    scores = jnp.where(allowed[None], scores, -1e30)
    peak = jnp.max(scores, axis=-1, keepdims=True)
    raised = jnp.exp(scores - peak)
    weights_bf = (raised / jnp.sum(raised, axis=-1, keepdims=True)).astype(jnp.bfloat16)
    return jnp.einsum(
        "hqk,khe->qhe", weights_bf, values_all, preferred_element_type=jnp.float32
    ).astype(jnp.bfloat16)


def body(tokens, documents, norm_gain, w_query, w_key, w_value, w_out, rel_bias):
    local_rows = tokens.shape[0]
    reach_rows = LEFT * SEG
    width_local = w_query.shape[2]
    heads_local = width_local // HEAD_DIM
    offset = lax.axis_index(SP) * local_rows
    query_pos = offset + jnp.arange(local_rows, dtype=jnp.int32)
    key_pos = offset - reach_rows + jnp.arange(reach_rows + local_rows, dtype=jnp.int32)
    widened = tokens.astype(jnp.float32)
    normed = (
        widened
        * lax.rsqrt(jnp.mean(widened * widened, axis=-1, keepdims=True) + EPS)
        * norm_gain[0]
    ).astype(jnp.bfloat16)
    before, prior_docs = passed_along((normed, documents), SP, 1)
    extended = jnp.concatenate([before, normed], axis=0)
    pieces = in_one_piece((w_query[0], w_key[0], w_value[0]), SP, 0, 1)
    query_sum = jnp.dot(normed, pieces[0], preferred_element_type=jnp.float32)
    key_sum = jnp.dot(extended, pieces[1], preferred_element_type=jnp.float32)
    value_sum = jnp.dot(extended, pieces[2], preferred_element_type=jnp.float32)
    queries = query_sum.astype(jnp.bfloat16)
    keys_all = key_sum.astype(jnp.bfloat16)
    values_all = value_sum.astype(jnp.bfloat16)
    key_doc = jnp.concatenate([prior_docs, documents], axis=0)
    attended = attend(
        queries.reshape(local_rows, heads_local, HEAD_DIM),
        keys_all.reshape(reach_rows + local_rows, heads_local, HEAD_DIM),
        values_all.reshape(reach_rows + local_rows, heads_local, HEAD_DIM),
        query_pos,
        key_pos,
        documents,
        key_doc,
        rel_bias[0],
    ).reshape(local_rows, width_local)
    all_heads = collect(attended, "tp", 1)
    return (
        widened
        + jnp.dot(
            all_heads, gather_axes(w_out[0], SP, (1, 0, 2), 1), preferred_element_type=jnp.float32
        )
    ).astype(jnp.bfloat16)


def solution(mesh):
    split = Mesh(mesh.devices.reshape(16, 4, 2, mesh.shape["tp"]), ("sp_0", "sp_1", "sp_2", "tp"))
    placed = (
        P(SP, None),
        P(SP),
        P(),
        P(None, SP, "tp"),
        P(None, SP, "tp"),
        P(None, SP, "tp"),
        P(None, None, SP),
        P(None, "tp", None),
    )
    return jax.shard_map(body, mesh=split, in_specs=placed, out_specs=P(SP, None), check_vma=False)
```

profile of v0, /device:TPU:32, one launch (start us, length us, event | category | flops | bytes accessed | tf_op | source)
XLA Modules:
  0.0 303.6 jit_solution(17535925062422447760)
XLA Ops:
  6.6 14.3 %all_gather.13 = bf16[4,2048,16]{1,2,0:T(8,128)(2,1)} all-gather(bf16[1,2048,16]{1,2,0:T(8,128)(2,1)} %param.14), channel_id=1, replica_groups=mesh['sp_0'=16,'sp_1'=4,'sp_2'=2,'tp'=4] {'sp_1'}, dimensions={0}, use_global_device_ids=true | all-gather | bytes 327680 | tf_op jit(solution)/shard_map/all_gather | solution.py:50
  21.0 1.4 pad_maximum_fusion.7
  22.4 79.5 %all-gather.6.cloned.1.call-done = bf16[64,2048,16]{1,2,0:T(8,128)(2,1)} async-done(((bf16[4,2048,16]{1,2,0:T(8,128)(2,1)}), bf16[64,2048,16]{1,2,0:T(8,128)(2,1)}) %all-gather.6.cloned.1.call-update) | async-done | bytes 4194320 | tf_op jit(solution)/shard_map/all_gather | solution.py:50
  102.3 1.3 fusion.5
  103.5 1.9 collective-permute-start
  105.5 3.5 %collective-permute-start.1 = (s32[256]{0:T(256)S(1)}, s32[256]{0:T(256)S(1)}, u32[]{:S(2)}, u32[]{:S(2)}) collective-permute-start(s32[256]{0:T(256)S(1)} %copy-done.4), channel_id=1, source_target_pairs={{0,4},{4,8},{8,12},{12,16},{16,20},{20,24},{24,28},{28,32},{32,36}... | collective-permute-start | bytes 3080 | tf_op jit(solution)/shard_map/ppermute | solution.py:20
  109.2 1.6 gather_fusion
  111.6 3.2 %tile.4 = f32[8,256,767]{2,1,0:T(8,128)} broadcast(f32[8,767]{1,0:T(8,128)S(1)} %copy.22), dimensions={0,2} | broadcast | bytes 6307808 | tf_op jit(solution)/shard_map/tile | solution.py:67
  114.7 8.8 %tile.10 = f32[8,196352]{1,0:T(8,128)} reshape(f32[8,256,767]{2,1,0:T(8,128)} %tile.4) | data formatting | bytes 12566528 | tf_op jit(solution)/shard_map/tile | solution.py:67
  123.5 5.5 %slice.10 = f32[8,196096]{1,0:T(8,128)} slice(f32[8,196352]{1,0:T(8,128)} %tile.10), slice={[0:8], [255:196351]} | slice | bytes 12550144 | tf_op jit(solution)/shard_map/slice | solution.py:68
  128.9 12.4 %reshape.213 = f32[8,256,766]{2,1,0:T(8,128)} reshape(f32[8,196096]{1,0:T(8,128)} %slice.10) | data formatting | bytes 12550144 | tf_op jit(solution)/shard_map/reshape | solution.py:69
  141.6 104.4 %all-gather.4.cloned.1.call-done = bf16[2048,1536]{1,0:T(8,128)(2,1)} async-done(((bf16[16,1536]{1,0:T(8,128)(2,1)}), bf16[2048,1536]{1,0:T(8,128)(2,1)}) %all-gather.4.cloned.1.call-update) | async-done | bytes 6291472 | tf_op jit(solution)/shard_map/all_gather | solution.py:29
  246.0 3.5 %fusion.20 = bf16[256,512]{1,0:T(8,128)(2,1)} fusion(bf16[256,2048]{1,0:T(8,128)(2,1)} %fusion.5, bf16[2048,1536]{1,0:T(8,128)(2,1)} %all-gather.4.cloned.1.call-done), kind=kOutput, calls=%fused_computation.24 | convolution fusion | flops 537001984 | bytes 3407872 | tf_op jit(solution)/shard_map/dot_general | solution.py:115
  249.5 1.1 copy.20
  250.6 3.7 %fusion.16 = bf16[512,512]{0,1:T(8,128)(2,1)S(1)} fusion(bf16[2048,1536]{1,0:T(8,128)(2,1)} %all-gather.4.cloned.1.call-done, bf16[256,2048]{1,0:T(8,128)(2,1)} %fusion.5, bf16[256,2048]{1,0:T(8,128)(2,1)} %collective-permute-done), kind=kOutput, calls=%fused_computation.22 | convolution fusion | flops 1078198272 | bytes 4718592 | tf_op jit(solution)/shard_map/dot_general | solution.py:116
  254.3 0.9 fusion.1
  255.2 1.7 fusion.34
  257.0 3.6 %fusion.13 = bf16[512,512]{0,1:T(8,128)(2,1)S(1)} fusion(bf16[2048,1536]{1,0:T(8,128)(2,1)} %all-gather.4.cloned.1.call-done, bf16[256,2048]{1,0:T(8,128)(2,1)} %fusion.5, bf16[256,2048]{1,0:T(8,128)(2,1)} %collective-permute-done), kind=kOutput, calls=%fused_computation.21 | convolution fusion | flops 1078198272 | bytes 4718592 | tf_op jit(solution)/shard_map/dot_general | solution.py:117
  260.6 8.9 %fusion.19 = bf16[8,64,256]{2,1,0:T(8,128)(2,1)S(1)} fusion(bf16[512,8,64]{0,2,1:T(8,128)(2,1)S(1)} %bitcast.45, f32[8,256]{1,0:T(8,128)S(1)} %fusion.34, f32[8,256,512]{2,1,0:T(8,128)} %copy-done), kind=kOutput, calls=%fused_computation.23 | convolution fusion | flops 137497088 | bytes 4988928 | tf_op jit(solution)/shard_map/hqk,khe->qhe/dot_general | solution.py:93
  269.5 1.0 broadcast_in_dim.45
  270.5 4.3 %all-to-all-start = ((bf16[4,256,512]{1,2,0:T(8,128)(2,1)}), bf16[4,256,512]{1,2,0:T(8,128)(2,1)S(1)}, u32[]{:S(2)}, u32[]{:S(2)}) async-start(bf16[4,256,512]{1,2,0:T(8,128)(2,1)} %broadcast_in_dim.45), calls=%async_computation | async-start | bytes 2097152 | tf_op jit(solution)/shard_map/all_to_all | solution.py:40
  274.8 8.2 %copy.23 = bf16[16,4,2,2048,16]{3,4,2,1,0:T(8,128)(2,1)} copy(bf16[16,4,2,2048,16]{3,4,1,0,2:T(8,128)(2,1)} %bitcast.34) | data formatting | bytes 16777216 | tf_op jit(solution)/shard_map/transpose | solution.py:54
  283.1 7.3 %all-to-all-done = bf16[4,256,512]{1,2,0:T(8,128)(2,1)S(1)} async-done(((bf16[4,256,512]{1,2,0:T(8,128)(2,1)}), bf16[4,256,512]{1,2,0:T(8,128)(2,1)S(1)}, u32[]{:S(2)}, u32[]{:S(2)}) %all-to-all-start) | async-done | bytes 1048608 | tf_op jit(solution)/shard_map/all_to_all | solution.py:40
  290.4 6.7 %fusion.2 = bf16[256,2048]{1,0:T(8,128)(2,1)} fusion(bf16[256,2048]{0,1:T(8,128)(2,1)S(1)} %bitcast.37, bf16[2048,2048]{0,1:T(8,128)(2,1)} %bitcast.35, bf16[256,2048]{1,0:T(8,128)(2,1)S(1)} %copy-done.1), kind=kOutput, calls=%fused_computation.9 | convolution fusion | flops 2149056512 | bytes 11534336 | tf_op jit(solution)/shard_map/dot_general | solution.py:135
  (38 shorter events, 1.7 us)
Async XLA Ops:
  6.5 95.4 %copy-start.1 = (bf16[256,2048]{1,0:T(8,128)(2,1)S(1)}, bf16[256,2048]{1,0:T(8,128)(2,1)}, u32[]{:S(2)}) copy-start(bf16[256,2048]{1,0:T(8,128)(2,1)} %param.8) | copy-start | bytes 3145732
  6.5 95.7 %copy-start.3 = (f32[1,2048]{1,0:T(1,128)S(1)}, f32[1,2048]{1,0:T(1,128)}, u32[]{:S(2)}) copy-start(f32[1,2048]{1,0:T(1,128)} %param.10) | copy-start | bytes 24580
  6.5 98.9 %copy-start.4 = (s32[256]{0:T(256)S(1)}, s32[256]{0:T(256)}, u32[]{:S(2)}) copy-start(s32[256]{0:T(256)} %param.9) | copy-start | bytes 3076
  6.5 102.5 %copy-start.2 = (f32[1,8,257]{2,1,0:T(8,128)S(1)}, f32[1,8,257]{2,1,0:T(8,128)}, u32[]{:S(2)}) copy-start(f32[1,8,257]{2,1,0:T(8,128)} %param.15) | copy-start | bytes 24676
  6.5 95.4 %all-gather.6.cloned.1.call-start = ((), (), s32[]{:S(2)}) async-start(), calls=%async_computation.2 | async-start | bytes 4456448 | tf_op jit(solution)/shard_map/all_gather | solution.py:50
  21.0 225.1 %all-gather.4.cloned.1.call-start = ((), (), s32[]{:S(2)}) async-start(), calls=%async_computation.1 | async-start | bytes 6340608 | tf_op jit(solution)/shard_map/all_gather | solution.py:29
  22.4 252.4 %all-gather.8.cloned.1.call-start = ((), (), s32[]{:S(2)}) async-start(), calls=%async_computation.3 | async-start | bytes 12582912 | tf_op jit(solution)/shard_map/all_gather | solution.py:50
  103.5 147.0 %collective-permute-start = (bf16[256,2048]{1,0:T(8,128)(2,1)}, bf16[256,2048]{1,0:T(8,128)(2,1)}, u32[]{:S(2)}, u32[]{:S(2)}) collective-permute-start(bf16[256,2048]{1,0:T(8,128)(2,1)} %fusion.5), channel_id=1, source_target_pairs={{0,4},{4,8},{8,12},{12,16},{16,20},{20,24},{24,28},{28,32},{32,36}... | collective-permute-start | bytes 3145736 | tf_op jit(solution)/shard_map/ppermute | solution.py:20
  105.5 35.9 %collective-permute-start.1 = (s32[256]{0:T(256)S(1)}, s32[256]{0:T(256)S(1)}, u32[]{:S(2)}, u32[]{:S(2)}) collective-permute-start(s32[256]{0:T(256)S(1)} %copy-done.4), channel_id=1, source_target_pairs={{0,4},{4,8},{8,12},{12,16},{16,20},{20,24},{24,28},{28,32},{32,36}... | collective-permute-start | bytes 3080 | tf_op jit(solution)/shard_map/ppermute | solution.py:20
  246.0 8.2 %slice-start = ((s8[6291456]{0:T(1024)(128)(4,1)}), s8[2097152]{0:T(1024)(128)(4,1)S(1)}, s32[]{:S(2)}) async-start(s8[6291456]{0:T(1024)(128)(4,1)} %bitcast.32), calls=%async_computation.4 | async-start | bytes 4194304
  250.6 3.7 %slice-start.1 = ((s8[6291456]{0:T(1024)(128)(4,1)}), s8[4194304]{0:T(1024)(128)(4,1)S(1)}, s32[]{:S(2)}) async-start(s8[6291456]{0:T(1024)(128)(4,1)} %bitcast.32), calls=%async_computation.5 | async-start | bytes 8388608
  255.2 5.4 %copy-start = (f32[8,256,512]{2,1,0:T(8,128)}, f32[8,256,512]{2,1,0:T(8,128)S(1)}, u32[]{:S(2)}) copy-start(f32[8,256,512]{2,1,0:T(8,128)S(1)} %fusion.1) | copy-start | bytes 12582916
  270.5 19.9 %all-to-all-start = ((bf16[4,256,512]{1,2,0:T(8,128)(2,1)}), bf16[4,256,512]{1,2,0:T(8,128)(2,1)S(1)}, u32[]{:S(2)}, u32[]{:S(2)}) async-start(bf16[4,256,512]{1,2,0:T(8,128)(2,1)} %broadcast_in_dim.45), calls=%async_computation | async-start | bytes 2097152 | tf_op jit(solution)/shard_map/all_to_all | solution.py:40
Sparse Core Ops, SparseCore 0:
  21.1 80.7 all-gather.5
  105.0 140.9 all-gather.3
  248.1 24.9 all-gather.7
where the time goes:
time: 304 us
  waiting for transfers between devices  191 us (63%)
  local copies, waits for them, and re-layouts  42.4 us (14%)
  matrix products  27.3 us (9%)
  blocking collectives  14.3 us (5%)
  between operations  13.4 us (4%)
  starting transfers between devices  9.79 us (3%)
  other arithmetic  5.19 us (2%)
    all_gather x1, waiting for transfers between devices, in_one_piece(): lax.all_gather(both, axis, axis=dim, tiled=True)  104 us
    all_gather x2, waiting for transfers between devices, gather_in_order(): pieces = lax.all_gather(pieces, axes[k], axis=0, tiled=True)  79.5 us
    all_gather x1, blocking collectives, gather_in_order(): pieces = lax.all_gather(pieces, axes[k], axis=0, tiled=True)  14.3 us
    reshape x1, local copies, waits for them, and re-layouts, banded_bias(): skewed = skewed.reshape(bias_table.shape[0], query_rows, span_len - 1)  12.4 us
    another operation x2, local copies, waits for them, and re-layouts, banded_bias(): repeated = jnp.tile(reversed_line, (1, query_rows))  11.9 us
    dot_general x1, matrix products, attend(): jnp.einsum('hqk,khe->qhe', weights_bf, values_all, preferred_element_type...  8.9 us
    transpose x1, local copies, waits for them, and re-layouts, gather_in_order(): pieces.transpose(*turned, *range(len(order), pieces.ndim))  8.25 us
    all_to_all x1, waiting for transfers between devices, from_everyone(): lax.all_to_all(jnp.broadcast_to(x[None], (length, *x.shape)), axis, 0, 0,...  7.32 us
  transfers between devices with their start and end apart: 6, of which 3 were waited for; matrix products, arithmetic and copies ran while one was open for 22% of the time, Pallas kernels for 0%

commit v1 on v0

v1 whole, which is shorter than its diff:
```python
import jax
import jax.numpy as jnp
from jax import lax
from jax.experimental import pallas as pl
from jax.experimental.pallas import tpu as pltpu
from jax.sharding import Mesh
from jax.sharding import PartitionSpec as P

HEAD_DIM = 64
SEG = 64
LEFT = 4
REL_CLIP = 128
EPS = 1e-06
REACH = LEFT * SEG
Q_BLOCK = 2 * SEG
K_BLOCK = Q_BLOCK + REACH
SP = ("z", "x", "c")
NEG = -1e30


def to_all(x, axis):
    length = lax.axis_size(axis)
    return lax.all_to_all(jnp.broadcast_to(x[None], (length, *x.shape)), axis, 0, 0, tiled=True)


def spread(x):
    over_z = to_all(x, "z")
    return to_all(over_z, "x")


def lay(w_ref, into):
    n_x, n_z, rows = w_ref.shape[:3]
    for z in range(n_z):
        for x in range(n_x):
            at = (z * n_x + x) * rows
            into[at : at + rows, :] = w_ref[x, z]


def query_key_kernel(halo, own, w_qk, q_out, k_out, w_all):
    lay(w_qk, w_all)
    width = q_out.shape[1]
    rows = halo.shape[0]
    before = jnp.dot(halo[...], w_all[:, width:], preferred_element_type=jnp.float32)
    k_out[:rows, :] = before.astype(jnp.bfloat16)
    for i in range(own.shape[0]):
        both = jnp.dot(own[i], w_all[...], preferred_element_type=jnp.float32).astype(jnp.bfloat16)
        q_out[i * rows : (i + 1) * rows, :] = both[:, :width]
        k_out[(i + 1) * rows : (i + 2) * rows, :] = both[:, width:]


def attend_kernel(halo, own, w_v, q, k, line, q_doc, k_doc, out, w_all, v):
    lay(w_v, w_all)
    rows = halo.shape[0]
    v[:rows, :] = jnp.dot(halo[...], w_all[...], preferred_element_type=jnp.float32).astype(jnp.bfloat16)
    for i in range(own.shape[0]):
        v[(i + 1) * rows : (i + 2) * rows, :] = jnp.dot(
            own[i], w_all[...], preferred_element_type=jnp.float32
        ).astype(jnp.bfloat16)
    q_seg = lax.broadcasted_iota(jnp.int32, (Q_BLOCK, K_BLOCK), 0) // SEG
    k_seg = lax.broadcasted_iota(jnp.int32, (Q_BLOCK, K_BLOCK), 1) // SEG
    window = (k_seg >= q_seg) & (k_seg <= q_seg + LEFT)
    blocks = q.shape[0] // Q_BLOCK
    same = []
    for b in range(blocks):
        lo = b * Q_BLOCK
        same.append((q_doc[lo : lo + Q_BLOCK, :] == k_doc[:, lo : lo + K_BLOCK]) & window)
    for h in range(q.shape[1] // HEAD_DIM):
        cols = slice(h * HEAD_DIM, (h + 1) * HEAD_DIM)
        flat = jnp.broadcast_to(line[h : h + 1, :], (Q_BLOCK, line.shape[1]))
        bias = pltpu.roll(flat, 0, 1, stride=1, stride_axis=0)[:, :K_BLOCK]
        for b in range(blocks):
            lo = b * Q_BLOCK
            scores = lax.dot_general(
                q[lo : lo + Q_BLOCK, cols],
                k[lo : lo + K_BLOCK, cols],
                (((1,), (1,)), ((), ())),
                preferred_element_type=jnp.float32,
            )
            scores = jnp.where(same[b], scores * HEAD_DIM ** (-0.5) + bias, NEG)
            peak = jnp.max(scores, axis=1, keepdims=True)
            raised = jnp.exp(scores - peak)
            total = jnp.sum(raised, axis=1, keepdims=True)
            weights = (raised / total).astype(jnp.bfloat16)
            mixed = jnp.dot(weights, v[lo : lo + K_BLOCK, cols], preferred_element_type=jnp.float32)
            out[lo : lo + Q_BLOCK, cols] = mixed.astype(jnp.bfloat16)


def project_kernel(att, w_o, out):
    n_x, n_z, rows, width = w_o.shape[1:]
    lanes = n_x * rows
    for z in range(n_z):
        total = None
        for c in range(att.shape[0]):
            part = lax.dot_general(
                att[c],
                w_o[c, :, z].reshape(lanes, width),
                (((1,), (1,)), ((), ())),
                preferred_element_type=jnp.float32,
            )
            total = part if total is None else total + part
        out[:, z * lanes : (z + 1) * lanes] = total.astype(jnp.bfloat16)


def in_vmem(kernel, outs, scratch=(), flops=10**9):
    one = not isinstance(outs, (list, tuple))
    shapes = [outs] if one else list(outs)
    specs = [pl.BlockSpec(memory_space=pltpu.VMEM) for _ in shapes]

    def call(*args):
        return pl.pallas_call(
            kernel,
            out_shape=shapes[0] if one else shapes,
            in_specs=[pl.BlockSpec(memory_space=pltpu.VMEM) for _ in args],
            out_specs=specs[0] if one else specs,
            scratch_shapes=list(scratch),
            cost_estimate=pl.CostEstimate(flops=flops, bytes_accessed=4 * 2**20, transcendentals=0),
        )(*args)

    return call


def bias_line(table):
    far = table[:, 2 * REL_CLIP :]
    near = table[:, 1:][:, ::-1]
    heads = table.shape[0]
    return jnp.concatenate(
        [
            jnp.broadcast_to(far, (heads, REACH - REL_CLIP)),
            near,
            table[:, :1],
            jnp.broadcast_to(far, (heads, Q_BLOCK - 1)),
        ],
        axis=1,
    )


def body(tokens, documents, norm_gain, w_query, w_key, w_value, w_out, rel_bias):
    rows, width = tokens.shape
    local = w_query.shape[2]
    half = local // 2
    core = lax.axis_index("c")
    tp = lax.axis_index("tp")
    n_tp = lax.axis_size("tp")
    chip = lax.axis_index("z") * lax.axis_size("x") + lax.axis_index("x")
    chips = lax.axis_size("z") * lax.axis_size("x")

    piece = w_query.shape[1]
    w_mine = lax.dynamic_slice_in_dim(w_out[0].T, tp * local, local, 1)
    packed = jnp.stack(
        [
            jnp.concatenate([w[:, c * half : (c + 1) * half] for w in (w_query[0], w_key[0], w_value[0], w_mine)], axis=1)
            for c in range(2)
        ]
    )
    mine = lax.all_to_all(packed, "c", 0, 0, tiled=True).reshape(2 * piece, 4 * half)
    w_qk = spread(mine[:, : 2 * half])
    w_v = spread(mine[:, 2 * half : 3 * half])
    w_o = to_all(spread(mine[:, 3 * half :]), "c")

    widened = tokens.astype(jnp.float32)
    normed = (
        widened * lax.rsqrt(jnp.mean(widened * widened, axis=-1, keepdims=True) + EPS) * norm_gain[0]
    ).astype(jnp.bfloat16)
    own = to_all(normed, "c")
    docs = to_all(documents, "c")
    onward = [(2 * i + c, 2 * i + 2 + c) for i in range(chips - 1) for c in range(2)]
    part = rows // 2
    sent = lax.dynamic_slice_in_dim(own[1], core * part, part, 0)
    halo, prior = lax.ppermute((sent, docs[1]), SP, onward)
    halo = to_all(halo, "c").reshape(rows, width)
    prior = jnp.where(chip > 0, prior, -1)
    docs = docs.reshape(-1)
    k_doc = jnp.concatenate([prior, docs])[None, :]
    q_doc = docs[:, None]
    line = bias_line(lax.dynamic_slice_in_dim(rel_bias[0], core * (rel_bias.shape[1] // 2), rel_bias.shape[1] // 2, 0))

    bf = jnp.bfloat16
    q, k = in_vmem(
        query_key_kernel,
        [jax.ShapeDtypeStruct((2 * rows, half), bf), jax.ShapeDtypeStruct((3 * rows, half), bf)],
        [pltpu.VMEM((width, 2 * half), bf)],
    )(halo, own, w_qk)
    att = in_vmem(
        attend_kernel,
        jax.ShapeDtypeStruct((2 * rows, half), bf),
        [pltpu.VMEM((width, half), bf), pltpu.VMEM((3 * rows, half), bf)],
    )(halo, own, w_v, q, k, line, q_doc, k_doc)
    att = lax.all_to_all(att.reshape(2, rows, half), "c", 0, 0, tiled=True)
    partial = in_vmem(project_kernel, jax.ShapeDtypeStruct((rows, width), bf))(att, w_o)
    share = rows // n_tp
    partial = lax.all_to_all(partial.reshape(n_tp, share, width), "tp", 0, 0, tiled=True)
    at = lax.dynamic_slice_in_dim(tokens, tp * share, share, 0).astype(jnp.float32)
    mixed = (at + jnp.sum(partial.astype(jnp.float32), axis=0)).astype(bf)
    return to_all(mixed, "tp").reshape(rows, width)


def solution(mesh):
    split = Mesh(mesh.devices.reshape(16, 4, 2, mesh.shape["tp"]), ("z", "x", "c", "tp"))
    placed = (
        P(SP, None),
        P(SP),
        P(),
        P(None, SP, "tp"),
        P(None, SP, "tp"),
        P(None, SP, "tp"),
        P(None, None, SP),
        P(None, "tp", None),
    )
    return jax.shard_map(body, mesh=split, in_specs=placed, out_specs=P(SP, None), check_vma=False)
```

time: 304 us -> 256 us (0.84)
  the two profiles are of different devices: /device:TPU:32 before, /device:TPU:224 now
where the time goes in v1:
time: 256 us; the launch traced here: 255 us
  blocking collectives  118 us (46%)
  waiting for transfers between devices  68.4 us (27%)
  starting transfers between devices  33.2 us (13%)
  Pallas kernels  18.7 us (7%)
  local copies, waits for them, and re-layouts  11.2 us (4%)
  other arithmetic  4.95 us (2%)
    all_to_all x5, blocking collectives, to_all(): lax.all_to_all(jnp.broadcast_to(x[None], (length, *x.shape)), axis, 0, 0,...  109 us
    all_to_all x6, waiting for transfers between devices, to_all(): lax.all_to_all(jnp.broadcast_to(x[None], (length, *x.shape)), axis, 0, 0,...  47.5 us
    all_to_all x6, starting transfers between devices, to_all(): lax.all_to_all(jnp.broadcast_to(x[None], (length, *x.shape)), axis, 0, 0,...  21.4 us
    pallas_call x3, Pallas kernels, call(): pl.pallas_call(kernel, out_shape=shapes[0] if one else shapes, in_specs=[...  18.7 us
    all_to_all x1, waiting for transfers between devices, body(): lax.all_to_all(partial.reshape(n_tp, share, width), 'tp', 0, 0, tiled=True)  15.4 us
    broadcast_in_dim x11, local copies, waits for them, and re-layouts, to_all(): jnp.broadcast_to(x[None], (length, *x.shape))  7.99 us
    ppermute x2, starting transfers between devices, body(): halo, prior = lax.ppermute((sent, docs[1]), SP, onward)  7.39 us
    all_to_all x1, blocking collectives, body(): att = lax.all_to_all(att.reshape(2, rows, half), 'c', 0, 0, tiled=True)  5.79 us
  transfers between devices with their start and end apart: 9, of which 7 were waited for; matrix products, arithmetic and copies ran while one was open for 2% of the time, Pallas kernels for 6%

profile of v1, /device:TPU:224, one launch (start us, length us, event | category | flops | bytes accessed | tf_op | source)
XLA Modules:
  0.0 255.0 jit_solution(18064331461033493747)
XLA Ops:
  4.7 3.8 %all-to-all-start = ((bf16[2,256,2048]{2,1,0:T(8,128)(2,1)}), bf16[2,256,2048]{2,1,0:T(8,128)(2,1)S(1)}, u32[]{:S(2)}, u32[]{:S(2)}) async-start(bf16[2,256,2048]{2,1,0:T(8,128)(2,1)} %broadcast_in_dim.33), calls=%async_computation | async-start | bytes 4194304 | tf_op jit(solution)/shard_map/all_to_all | solution.py:23
  11.5 3.4 %collective-permute-start = (bf16[128,2048]{1,0:T(8,128)(2,1)S(1)}, bf16[128,2048]{1,0:T(8,128)(2,1)S(1)}, u32[]{:S(2)}, u32[]{:S(2)}) collective-permute-start(bf16[128,2048]{1,0:T(8,128)(2,1)S(1)} %dynamic-slice_bitcast_fusion), channel_id=1, source_target_pairs={{0,8},{4,12},{8,16},{12,20},{16,24},{20,28},{24,32},{28,36},{32,40... | collective-permute-start | bytes 1572872 | tf_op jit(solution)/shard_map/ppermute | solution.py:169
  15.0 3.8 %all_to_all.71 = bf16[2,16,1024]{2,1,0:T(8,128)(2,1)S(1)} all-to-all(bf16[2,16,1024]{2,1,0:T(8,128)(2,1)S(1)} %pad_maximum_fusion), channel_id=1, replica_groups=mesh['z'=16,'x'=4,'c'=2,'tp'=4] {'c'}, dimensions={0} | all-to-all | bytes 131072 | tf_op jit(solution)/shard_map/all_to_all | solution.py:155
  19.4 3.2 %all-to-all-start.7 = ((s32[2,1,256]{2,1,0:T(1,128)}), s32[2,1,256]{2,1,0:T(1,128)S(1)}, u32[]{:S(2)}, u32[]{:S(2)}) async-start(s32[2,1,256]{2,1,0:T(1,128)} %broadcast_in_dim.43), calls=%async_computation.7 | async-start | bytes 4096 | tf_op jit(solution)/shard_map/all_to_all | solution.py:23
  24.0 5.5 %collective-permute-done = bf16[128,2048]{1,0:T(8,128)(2,1)S(1)} collective-permute-done((bf16[128,2048]{1,0:T(8,128)(2,1)S(1)}, bf16[128,2048]{1,0:T(8,128)(2,1)S(1)}, u32[]{:S(2)}, u32[]{:S(2)}) %collective-permute-start) | collective-permute-done | bytes 524320 | tf_op jit(solution)/shard_map/ppermute | solution.py:169
  29.6 5.4 %all_to_all.72 = bf16[2,128,2048]{2,1,0:T(8,128)(2,1)} all-to-all(bf16[2,128,2048]{2,1,0:T(8,128)(2,1)S(1)} %broadcast_in_dim.34), channel_id=1, replica_groups=mesh['z'=16,'x'=4,'c'=2,'tp'=4] {'c'}, dimensions={0} | all-to-all | bytes 2097152 | tf_op jit(solution)/shard_map/all_to_all | solution.py:23
  35.0 28.0 %all_to_all.73 = bf16[16,32,256]{2,1,0:T(8,128)(2,1)S(1)} all-to-all(bf16[16,32,256]{2,1,0:T(8,128)(2,1)S(1)} %broadcast_in_dim.35), channel_id=1, replica_groups=mesh['z'=16,'x'=4,'c'=2,'tp'=4] {'z'}, dimensions={0} | all-to-all | bytes 524288 | tf_op jit(solution)/shard_map/all_to_all | solution.py:23
  63.0 24.0 %all_to_all.74 = bf16[16,32,256]{2,1,0:T(8,128)(2,1)S(1)} all-to-all(bf16[16,32,256]{2,1,0:T(8,128)(2,1)S(1)} %broadcast_in_dim.46), channel_id=1, replica_groups=mesh['z'=16,'x'=4,'c'=2,'tp'=4] {'z'}, dimensions={0} | all-to-all | bytes 524288 | tf_op jit(solution)/shard_map/all_to_all | solution.py:23
  88.1 3.5 %all-to-all-start.4 = ((bf16[4,16,32,256]{3,2,1,0:T(8,128)(2,1)}), bf16[4,16,32,256]{3,2,1,0:T(8,128)(2,1)S(1)}, u32[]{:S(2)}, u32[]{:S(2)}) async-start(bf16[4,16,32,256]{3,2,1,0:T(8,128)(2,1)} %broadcast_in_dim.36), calls=%async_computation.4 | async-start | bytes 2097152 | tf_op jit(solution)/shard_map/all_to_all | solution.py:23
  91.7 15.3 %all-to-all-done.4.w_v = bf16[4,16,32,256]{3,2,1,0:T(8,128)(2,1)S(1)} async-done(((bf16[4,16,32,256]{3,2,1,0:T(8,128)(2,1)}), bf16[4,16,32,256]{3,2,1,0:T(8,128)(2,1)S(1)}, u32[]{:S(2)}, u32[]{:S(2)}) %all-to-all-start.4) | async-done | bytes 1048608 | tf_op jit(solution)/shard_map/all_to_all | solution.py:23
  107.0 34.3 %all_to_all.75 = bf16[16,32,512]{2,1,0:T(8,128)(2,1)S(1)} all-to-all(bf16[16,32,512]{2,1,0:T(8,128)(2,1)S(1)} %broadcast_in_dim.37), channel_id=1, replica_groups=mesh['z'=16,'x'=4,'c'=2,'tp'=4] {'z'}, dimensions={0} | all-to-all | bytes 1048576 | tf_op jit(solution)/shard_map/all_to_all | solution.py:23
  142.8 3.6 %all-to-all-start.6 = ((bf16[4,16,32,512]{3,2,1,0:T(8,128)(2,1)}), bf16[4,16,32,512]{3,2,1,0:T(8,128)(2,1)S(1)}, u32[]{:S(2)}, u32[]{:S(2)}) async-start(bf16[4,16,32,512]{3,2,1,0:T(8,128)(2,1)} %broadcast_in_dim.38), calls=%async_computation.6 | async-start | bytes 4194304 | tf_op jit(solution)/shard_map/all_to_all | solution.py:23
  146.5 4.0 %collective-permute-start.1 = (s32[256]{0:T(256)S(1)}, s32[256]{0:T(256)S(1)}, u32[]{:S(2)}, u32[]{:S(2)}) collective-permute-start(s32[256]{0:T(256)S(1)} %bitcast.37), channel_id=1, source_target_pairs={{0,8},{4,12},{8,16},{12,20},{16,24},{20,28},{24,32},{28,36},{32,40... | collective-permute-start | bytes 3080 | tf_op jit(solution)/shard_map/ppermute | solution.py:169
  150.5 21.9 %all-to-all-done.6.w_qk = bf16[4,16,32,512]{3,2,1,0:T(8,128)(2,1)S(1)} async-done(((bf16[4,16,32,512]{3,2,1,0:T(8,128)(2,1)}), bf16[4,16,32,512]{3,2,1,0:T(8,128)(2,1)S(1)}, u32[]{:S(2)}, u32[]{:S(2)}) %all-to-all-start.6) | async-done | bytes 2097184 | tf_op jit(solution)/shard_map/all_to_all | solution.py:23
  173.6 3.5 %all-to-all-start.10 = ((bf16[4,16,32,256]{3,2,1,0:T(8,128)(2,1)}), bf16[4,16,32,256]{3,2,1,0:T(8,128)(2,1)S(1)}, u32[]{:S(2)}, u32[]{:S(2)}) async-start(bf16[4,16,32,256]{3,2,1,0:T(8,128)(2,1)} %broadcast_in_dim.47), calls=%async_computation.10 | async-start | bytes 2097152 | tf_op jit(solution)/shard_map/all_to_all | solution.py:23
  179.8 4.9 %shard_map.82 = (bf16[512,256]{1,0:T(8,128)(2,1)}, bf16[768,256]{1,0:T(8,128)(2,1)}) custom-call(bf16[256,2048]{1,0:T(8,128)(2,1)} %bitcast.24, bf16[2,256,2048]{2,1,0:T(8,128)(2,1)} %copy-done.1, bf16[4,16,32,512]{3,2,1,0:T(8,128)(2,1)} %copy-done.2), custom_call_target="tpu_custom_call" | custom-call | flops 1000000000 | bytes 4194304 | tf_op jit(solution)/shard_map/pallas_call | solution.py:110
  184.7 6.2 %all-to-all-done.10 = bf16[4,16,32,256]{3,2,1,0:T(8,128)(2,1)S(1)} async-done(((bf16[4,16,32,256]{3,2,1,0:T(8,128)(2,1)}), bf16[4,16,32,256]{3,2,1,0:T(8,128)(2,1)S(1)}, u32[]{:S(2)}, u32[]{:S(2)}) %all-to-all-start.10) | async-done | bytes 1048608 | tf_op jit(solution)/shard_map/all_to_all | solution.py:23
  192.5 3.8 %all-to-all-start.11 = ((bf16[2,4,16,32,256]{4,3,2,1,0:T(8,128)(2,1)}), bf16[2,4,16,32,256]{4,3,2,1,0:T(8,128)(2,1)S(1)}, u32[]{:S(2)}, u32[]{:S(2)}) async-start(bf16[2,4,16,32,256]{4,3,2,1,0:T(8,128)(2,1)} %broadcast_in_dim.48), calls=%async_computation.11 | async-start | bytes 4194304 | tf_op jit(solution)/shard_map/all_to_all | solution.py:23
  196.3 9.9 %shard_map.83 = bf16[512,256]{1,0:T(8,128)(2,1)} custom-call(bf16[256,2048]{1,0:T(8,128)(2,1)} %bitcast.25, bf16[2,256,2048]{2,1,0:T(8,128)(2,1)} %copy-done.1, bf16[4,16,32,256]{3,2,1,0:T(8,128)(2,1)} %copy-done.3, bf16[512,256]{1,0:T(8,128)(2,1)} %get-tuple-element.7.q, bf16[768,256]{1,0:T(8,128)(2,1)} %get-tuple-element.8.k, ...), custom_call_target="tpu_custom_call" | custom-call | flops 1000000000 | bytes 4194304 | tf_op jit(solution)/shard_map/pallas_call | solution.py:110
  206.2 5.8 %all_to_all.76.att = bf16[2,256,256]{2,1,0:T(8,128)(2,1)} all-to-all(bf16[2,256,256]{2,1,0:T(8,128)(2,1)} %bitcast.27), channel_id=1, replica_groups=mesh['z'=16,'x'=4,'c'=2,'tp'=4] {'c'}, dimensions={0} | all-to-all | bytes 524288 | tf_op jit(solution)/shard_map/all_to_all | solution.py:188
  212.0 3.9 %shard_map.84 = bf16[256,2048]{1,0:T(8,128)(2,1)} custom-call(bf16[2,256,256]{2,1,0:T(8,128)(2,1)} %all_to_all.76.att, bf16[2,4,16,32,256]{4,3,2,1,0:T(8,128)(2,1)} %copy-done.4), custom_call_target="tpu_custom_call" | custom-call | flops 1000000000 | bytes 4194304 | tf_op jit(solution)/shard_map/pallas_call | solution.py:110
  215.9 4.5 %all-to-all-start.12 = ((bf16[4,64,2048]{2,1,0:T(8,128)(2,1)}), bf16[4,64,2048]{2,1,0:T(8,128)(2,1)S(1)}, u32[]{:S(2)}, u32[]{:S(2)}) async-start(bf16[4,64,2048]{2,1,0:T(8,128)(2,1)} %bitcast.28), calls=%async_computation.12 | async-start | bytes 2097152 | tf_op jit(solution)/shard_map/all_to_all | solution.py:191
  220.3 15.4 %all-to-all-done.12 = bf16[4,64,2048]{2,1,0:T(8,128)(2,1)S(1)} async-done(((bf16[4,64,2048]{2,1,0:T(8,128)(2,1)}), bf16[4,64,2048]{2,1,0:T(8,128)(2,1)S(1)}, u32[]{:S(2)}, u32[]{:S(2)}) %all-to-all-start.12) | async-done | bytes 1048608 | tf_op jit(solution)/shard_map/all_to_all | solution.py:191
  237.0 17.0 %all_to_all.77 = bf16[4,64,2048]{2,1,0:T(8,128)(2,1)S(1)} all-to-all(bf16[4,64,2048]{2,1,0:T(8,128)(2,1)S(1)} %broadcast_in_dim.49), channel_id=1, replica_groups=mesh['z'=16,'x'=4,'c'=2,'tp'=4] {'tp'}, dimensions={0} | all-to-all | bytes 2097152 | tf_op jit(solution)/shard_map/all_to_all | solution.py:23
  (64 shorter events, 20.2 us)
Async XLA Ops:
  0.0 14.9 %copy-start = (bf16[1,2048,16]{1,2,0:T(8,128)(2,1)S(1)}, bf16[1,2048,16]{1,2,0:T(8,128)(2,1)}, u32[]{:S(2)}) copy-start(bf16[1,2048,16]{1,2,0:T(8,128)(2,1)} %param.14) | copy-start | bytes 196612
  4.7 6.6 %all-to-all-start = ((bf16[2,256,2048]{2,1,0:T(8,128)(2,1)}), bf16[2,256,2048]{2,1,0:T(8,128)(2,1)S(1)}, u32[]{:S(2)}, u32[]{:S(2)}) async-start(bf16[2,256,2048]{2,1,0:T(8,128)(2,1)} %broadcast_in_dim.33), calls=%async_computation | async-start | bytes 4194304 | tf_op jit(solution)/shard_map/all_to_all | solution.py:23
  8.5 6.5 %copy-start.5 = (bf16[1,16,512]{2,1,0:T(8,128)(2,1)S(1)}, bf16[1,16,512]{2,1,0:T(8,128)(2,1)}, u32[]{:S(2)}) copy-start(bf16[1,16,512]{2,1,0:T(8,128)(2,1)} %param.11) | copy-start | bytes 49156
  8.5 6.5 %copy-start.6 = (bf16[1,16,512]{2,1,0:T(8,128)(2,1)S(1)}, bf16[1,16,512]{2,1,0:T(8,128)(2,1)}, u32[]{:S(2)}) copy-start(bf16[1,16,512]{2,1,0:T(8,128)(2,1)} %param.12) | copy-start | bytes 49156
  8.5 6.5 %copy-start.7 = (bf16[1,16,512]{2,1,0:T(8,128)(2,1)S(1)}, bf16[1,16,512]{2,1,0:T(8,128)(2,1)}, u32[]{:S(2)}) copy-start(bf16[1,16,512]{2,1,0:T(8,128)(2,1)} %param.13) | copy-start | bytes 49156
  8.5 10.3 %copy-start.9 = (s32[256]{0:T(256)S(1)}, s32[256]{0:T(256)}, u32[]{:S(2)}) copy-start(s32[256]{0:T(256)} %param.9) | copy-start | bytes 3076
  11.3 18.3 %copy-start.1 = (bf16[2,256,2048]{2,1,0:T(8,128)(2,1)}, bf16[2,256,2048]{2,1,0:T(8,128)(2,1)S(1)}, u32[]{:S(2)}) copy-start(bf16[2,256,2048]{2,1,0:T(8,128)(2,1)S(1)} %all-to-all-done.own) | copy-start | bytes 6291460
  11.5 18.0 %collective-permute-start = (bf16[128,2048]{1,0:T(8,128)(2,1)S(1)}, bf16[128,2048]{1,0:T(8,128)(2,1)S(1)}, u32[]{:S(2)}, u32[]{:S(2)}) collective-permute-start(bf16[128,2048]{1,0:T(8,128)(2,1)S(1)} %dynamic-slice_bitcast_fusion), channel_id=1, source_target_pairs={{0,8},{4,12},{8,16},{12,20},{16,24},{20,28},{24,32},{28,36},{32,40... | collective-permute-start | bytes 1572872 | tf_op jit(solution)/shard_map/ppermute | solution.py:169
  19.4 4.6 %all-to-all-start.7 = ((s32[2,1,256]{2,1,0:T(1,128)}), s32[2,1,256]{2,1,0:T(1,128)S(1)}, u32[]{:S(2)}, u32[]{:S(2)}) async-start(s32[2,1,256]{2,1,0:T(1,128)} %broadcast_in_dim.43), calls=%async_computation.7 | async-start | bytes 4096 | tf_op jit(solution)/shard_map/all_to_all | solution.py:23
  88.1 18.8 %all-to-all-start.4 = ((bf16[4,16,32,256]{3,2,1,0:T(8,128)(2,1)}), bf16[4,16,32,256]{3,2,1,0:T(8,128)(2,1)S(1)}, u32[]{:S(2)}, u32[]{:S(2)}) async-start(bf16[4,16,32,256]{3,2,1,0:T(8,128)(2,1)} %broadcast_in_dim.36), calls=%async_computation.4 | async-start | bytes 2097152 | tf_op jit(solution)/shard_map/all_to_all | solution.py:23
  106.9 35.9 %copy-start.3 = (bf16[4,16,32,256]{3,2,1,0:T(8,128)(2,1)}, bf16[4,16,32,256]{3,2,1,0:T(8,128)(2,1)S(1)}, u32[]{:S(2)}) copy-start(bf16[4,16,32,256]{3,2,1,0:T(8,128)(2,1)S(1)} %all-to-all-done.4.w_v) | copy-start | bytes 3145732
  142.8 29.5 %all-to-all-start.6 = ((bf16[4,16,32,512]{3,2,1,0:T(8,128)(2,1)}), bf16[4,16,32,512]{3,2,1,0:T(8,128)(2,1)S(1)}, u32[]{:S(2)}, u32[]{:S(2)}) async-start(bf16[4,16,32,512]{3,2,1,0:T(8,128)(2,1)} %broadcast_in_dim.38), calls=%async_computation.6 | async-start | bytes 4194304 | tf_op jit(solution)/shard_map/all_to_all | solution.py:23
  146.4 30.7 %copy-start.8 = (f32[1,8,257]{2,1,0:T(8,128)S(1)}, f32[1,8,257]{2,1,0:T(8,128)}, u32[]{:S(2)}) copy-start(f32[1,8,257]{2,1,0:T(8,128)} %param.15) | copy-start | bytes 24676
  146.5 32.8 %collective-permute-start.1 = (s32[256]{0:T(256)S(1)}, s32[256]{0:T(256)S(1)}, u32[]{:S(2)}, u32[]{:S(2)}) collective-permute-start(s32[256]{0:T(256)S(1)} %bitcast.37), channel_id=1, source_target_pairs={{0,8},{4,12},{8,16},{12,20},{16,24},{20,28},{24,32},{28,36},{32,40... | collective-permute-start | bytes 3080 | tf_op jit(solution)/shard_map/ppermute | solution.py:169
  172.4 7.5 %copy-start.2 = (bf16[4,16,32,512]{3,2,1,0:T(8,128)(2,1)}, bf16[4,16,32,512]{3,2,1,0:T(8,128)(2,1)S(1)}, u32[]{:S(2)}) copy-start(bf16[4,16,32,512]{3,2,1,0:T(8,128)(2,1)S(1)} %all-to-all-done.6.w_qk) | copy-start | bytes 6291460
  173.6 17.3 %all-to-all-start.10 = ((bf16[4,16,32,256]{3,2,1,0:T(8,128)(2,1)}), bf16[4,16,32,256]{3,2,1,0:T(8,128)(2,1)S(1)}, u32[]{:S(2)}, u32[]{:S(2)}) async-start(bf16[4,16,32,256]{3,2,1,0:T(8,128)(2,1)} %broadcast_in_dim.47), calls=%async_computation.10 | async-start | bytes 2097152 | tf_op jit(solution)/shard_map/all_to_all | solution.py:23
  192.5 13.6 %all-to-all-start.11 = ((bf16[2,4,16,32,256]{4,3,2,1,0:T(8,128)(2,1)}), bf16[2,4,16,32,256]{4,3,2,1,0:T(8,128)(2,1)S(1)}, u32[]{:S(2)}, u32[]{:S(2)}) async-start(bf16[2,4,16,32,256]{4,3,2,1,0:T(8,128)(2,1)} %broadcast_in_dim.48), calls=%async_computation.11 | async-start | bytes 4194304 | tf_op jit(solution)/shard_map/all_to_all | solution.py:23
  206.2 5.8 %copy-start.4 = (bf16[2,4,16,32,256]{4,3,2,1,0:T(8,128)(2,1)}, bf16[2,4,16,32,256]{4,3,2,1,0:T(8,128)(2,1)S(1)}, u32[]{:S(2)}) copy-start(bf16[2,4,16,32,256]{4,3,2,1,0:T(8,128)(2,1)S(1)} %all-to-all-done.11.w_o) | copy-start | bytes 6291460
  215.9 19.9 %all-to-all-start.12 = ((bf16[4,64,2048]{2,1,0:T(8,128)(2,1)}), bf16[4,64,2048]{2,1,0:T(8,128)(2,1)S(1)}, u32[]{:S(2)}, u32[]{:S(2)}) async-start(bf16[4,64,2048]{2,1,0:T(8,128)(2,1)} %bitcast.28), calls=%async_computation.12 | async-start | bytes 2097152 | tf_op jit(solution)/shard_map/all_to_all | solution.py:191

commit v2 on v1

v2 whole, which is shorter than its diff:
```python
import jax
import jax.numpy as jnp
from jax import lax
from jax.experimental import pallas as pl
from jax.experimental.pallas import tpu as pltpu
from jax.sharding import Mesh
from jax.sharding import PartitionSpec as P

HEAD_DIM = 64
SEG = 64
LEFT = 4
REL_CLIP = 128
EPS = 1e-06
REACH = LEFT * SEG
Q_BLOCK = 2 * SEG
K_BLOCK = Q_BLOCK + REACH
SP = ("zh", "zl", "x", "c")
NEG = -1e30


def to_all(x, axis):
    length = lax.axis_size(axis)
    return lax.all_to_all(jnp.broadcast_to(x[None], (length, *x.shape)), axis, 0, 0, tiled=True)


def lay(w_ref, cols, into):
    n_x, n_l, n_h, rows = w_ref.shape[:4]
    for h in range(n_h):
        for l in range(n_l):
            for x in range(n_x):
                at = ((h * n_l + l) * n_x + x) * rows
                into[at : at + rows, :] = w_ref[x, l, h, :, cols]


def query_key_kernel(halo, first, second, w_in, q_out, k_out, w_all):
    width = q_out.shape[1]
    rows = halo.shape[0]
    lay(w_in, slice(0, 2 * width), w_all)
    before = jnp.dot(halo[...], w_all[:, width:], preferred_element_type=jnp.float32)
    k_out[:rows, :] = before.astype(jnp.bfloat16)
    for i, own in enumerate((first, second)):
        both = jnp.dot(own[...], w_all[...], preferred_element_type=jnp.float32).astype(jnp.bfloat16)
        q_out[i * rows : (i + 1) * rows, :] = both[:, :width]
        k_out[(i + 1) * rows : (i + 2) * rows, :] = both[:, width:]


def attend_kernel(halo, first, second, w_in, q, k, line, q_doc, k_doc, out, w_all, v):
    width = q.shape[1]
    rows = halo.shape[0]
    lay(w_in, slice(2 * width, 3 * width), w_all)
    for i, part in enumerate((halo, first, second)):
        v[i * rows : (i + 1) * rows, :] = jnp.dot(
            part[...], w_all[...], preferred_element_type=jnp.float32
        ).astype(jnp.bfloat16)
    q_seg = lax.broadcasted_iota(jnp.int32, (Q_BLOCK, K_BLOCK), 0) // SEG
    k_seg = lax.broadcasted_iota(jnp.int32, (Q_BLOCK, K_BLOCK), 1) // SEG
    window = (k_seg >= q_seg) & (k_seg <= q_seg + LEFT)
    blocks = q.shape[0] // Q_BLOCK
    same = []
    for b in range(blocks):
        lo = b * Q_BLOCK
        same.append((q_doc[lo : lo + Q_BLOCK, :] == k_doc[:, lo : lo + K_BLOCK]) & window)
    for h in range(q.shape[1] // HEAD_DIM):
        cols = slice(h * HEAD_DIM, (h + 1) * HEAD_DIM)
        flat = jnp.broadcast_to(line[h : h + 1, :], (Q_BLOCK, line.shape[1]))
        bias = pltpu.roll(flat, 0, 1, stride=1, stride_axis=0)[:, :K_BLOCK]
        for b in range(blocks):
            lo = b * Q_BLOCK
            scores = lax.dot_general(
                q[lo : lo + Q_BLOCK, cols],
                k[lo : lo + K_BLOCK, cols],
                (((1,), (1,)), ((), ())),
                preferred_element_type=jnp.float32,
            )
            scores = jnp.where(same[b], scores * HEAD_DIM ** (-0.5) + bias, NEG)
            peak = jnp.max(scores, axis=1, keepdims=True)
            raised = jnp.exp(scores - peak)
            total = jnp.sum(raised, axis=1, keepdims=True)
            mixed = jnp.dot(
                raised.astype(jnp.bfloat16), v[lo : lo + K_BLOCK, cols], preferred_element_type=jnp.float32
            )
            out[lo : lo + Q_BLOCK, cols] = (mixed / total).astype(jnp.bfloat16)


def project_kernel(att, w_o, out):
    n_x, n_l, n_h, rows, width = w_o.shape[1:]
    lanes = n_x * rows
    for h in range(n_h):
        for l in range(n_l):
            total = None
            for c in range(att.shape[0]):
                part = lax.dot_general(
                    att[c],
                    w_o[c, :, l, h].reshape(lanes, width),
                    (((1,), (1,)), ((), ())),
                    preferred_element_type=jnp.float32,
                )
                total = part if total is None else total + part
            at = (h * n_l + l) * lanes
            out[:, at : at + lanes] = total.astype(jnp.bfloat16)


def in_vmem(kernel, outs, scratch=(), grant=16, flops=2 * 10**10):
    one = not isinstance(outs, (list, tuple))
    shapes = [outs] if one else list(outs)
    specs = [pl.BlockSpec(memory_space=pltpu.VMEM) for _ in shapes]

    def call(*args):
        return pl.pallas_call(
            kernel,
            out_shape=shapes[0] if one else shapes,
            in_specs=[pl.BlockSpec(memory_space=pltpu.VMEM) for _ in args],
            out_specs=specs[0] if one else specs,
            scratch_shapes=list(scratch),
            compiler_params=pltpu.CompilerParams(vmem_limit_bytes=grant * 2**20),
            cost_estimate=pl.CostEstimate(flops=flops, bytes_accessed=4 * 2**20, transcendentals=0),
        )(*args)

    return call


def bias_line(table):
    far = table[:, 2 * REL_CLIP :]
    near = table[:, 1:][:, ::-1]
    heads = table.shape[0]
    return jnp.concatenate(
        [
            jnp.broadcast_to(far, (heads, REACH - REL_CLIP)),
            near,
            table[:, :1],
            jnp.broadcast_to(far, (heads, Q_BLOCK - 1)),
        ],
        axis=1,
    )


def body(tokens, documents, norm_gain, w_query, w_key, w_value, w_out, rel_bias):
    rows, width = tokens.shape
    local = w_query.shape[2]
    half = local // 2
    core = lax.axis_index("c")
    tp = lax.axis_index("tp")
    n_tp = lax.axis_size("tp")
    chips = lax.axis_size(SP[:-1])
    chip = lax.axis_index(SP[:-1])

    piece = w_query.shape[1]
    w_mine = lax.dynamic_slice_in_dim(w_out[0].T, tp * local, local, 1)
    packed = jnp.stack(
        [
            jnp.concatenate([w[:, c * half : (c + 1) * half] for w in (w_query[0], w_key[0], w_value[0], w_mine)], axis=1)
            for c in range(2)
        ]
    )
    mine = lax.all_to_all(packed, "c", 0, 0, tiled=True).reshape(2 * piece, 4 * half)
    over_z = to_all(to_all(mine, "zh"), "zl")
    w_in = to_all(over_z[..., : 3 * half], "x")
    last, w_in = lax.optimization_barrier((over_z[..., 3 * half :], w_in))
    last = to_all(last, "x")

    widened = tokens.astype(jnp.float32)
    normed = (
        widened * lax.rsqrt(jnp.mean(widened * widened, axis=-1, keepdims=True) + EPS) * norm_gain[0]
    ).astype(jnp.bfloat16)
    swap = [(0, 1), (1, 0)]
    other, other_doc = lax.ppermute((normed, documents), "c", swap)
    first, second = jnp.where(core == 0, normed, other), jnp.where(core == 0, other, normed)
    doc_1, doc_2 = jnp.where(core == 0, documents, other_doc), jnp.where(core == 0, other_doc, documents)
    onward = [(2 * i + c, 2 * i + 2 + c) for i in range(chips - 1) for c in range(2)]
    halo, prior = lax.ppermute((second, doc_2), SP, onward)
    prior = jnp.where(chip > 0, prior, -1)
    k_doc = jnp.concatenate([prior, doc_1, doc_2])[None, :]
    q_doc = jnp.concatenate([doc_1, doc_2])[:, None]
    line = bias_line(lax.dynamic_slice_in_dim(rel_bias[0], core * (rel_bias.shape[1] // 2), rel_bias.shape[1] // 2, 0))

    bf = jnp.bfloat16
    q, k = in_vmem(
        query_key_kernel,
        [jax.ShapeDtypeStruct((2 * rows, half), bf), jax.ShapeDtypeStruct((3 * rows, half), bf)],
        [pltpu.VMEM((width, 2 * half), bf)],
    )(halo, first, second, w_in)
    q, k, last = lax.optimization_barrier((q, k, last))
    w_o = to_all(last, "c")
    att = in_vmem(
        attend_kernel,
        jax.ShapeDtypeStruct((2 * rows, half), bf),
        [pltpu.VMEM((width, half), bf), pltpu.VMEM((3 * rows, half), bf)],
    )(halo, first, second, w_in, q, k, line, q_doc, k_doc)
    att, w_o = lax.optimization_barrier((att, w_o))
    att = lax.all_to_all(att.reshape(2, rows, half), "c", 0, 0, tiled=True)
    partial = in_vmem(project_kernel, jax.ShapeDtypeStruct((rows, width), bf))(att, w_o)
    share = rows // n_tp
    partial = lax.all_to_all(partial.reshape(n_tp, share, width), "tp", 0, 0, tiled=True)
    at = lax.dynamic_slice_in_dim(tokens, tp * share, share, 0).astype(jnp.float32)
    mixed = (at + jnp.sum(partial.astype(jnp.float32), axis=0)).astype(bf)
    return to_all(mixed, "tp").reshape(rows, width)


def solution(mesh):
    split = Mesh(mesh.devices.reshape(4, 4, 4, 2, mesh.shape["tp"]), (*SP, "tp"))
    placed = (
        P(SP, None),
        P(SP),
        P(),
        P(None, SP, "tp"),
        P(None, SP, "tp"),
        P(None, SP, "tp"),
        P(None, None, SP),
        P(None, "tp", None),
    )
    return jax.shard_map(body, mesh=split, in_specs=placed, out_specs=P(SP, None), check_vma=False)
```

time: 256 us -> 236 us (0.922)
  the two profiles are of different devices: /device:TPU:224 before, /device:TPU:128 now
where the time goes in v2:
time: 236 us; the launch traced here: 235 us
  waiting for transfers between devices  87.1 us (37%)
  blocking collectives  56.8 us (24%)
  starting transfers between devices  49.5 us (21%)
  local copies, waits for them, and re-layouts  21.1 us (9%)
  Pallas kernels  13.8 us (6%)
  other arithmetic  6.5 us (3%)
    all_to_all x2, blocking collectives, to_all(): lax.all_to_all(jnp.broadcast_to(x[None], (length, *x.shape)), axis, 0, 0,...  48 us
    ppermute x2, waiting for transfers between devices, body(): halo, prior = lax.ppermute((second, doc_2), SP, onward)  42.1 us
    all_to_all x4, starting transfers between devices, to_all(): lax.all_to_all(jnp.broadcast_to(x[None], (length, *x.shape)), axis, 0, 0,...  34 us
    all_to_all x4, waiting for transfers between devices, to_all(): lax.all_to_all(jnp.broadcast_to(x[None], (length, *x.shape)), axis, 0, 0,...  29.6 us
    all_to_all x1, waiting for transfers between devices, body(): lax.all_to_all(partial.reshape(n_tp, share, width), 'tp', 0, 0, tiled=True)  15.4 us
    pallas_call x3, Pallas kernels, call(): pl.pallas_call(kernel, out_shape=shapes[0] if one else shapes, in_specs=[...  13.8 us
    unnamed x27, local copies, waits for them, and re-layouts  8.38 us
    broadcast_in_dim x6, local copies, waits for them, and re-layouts, to_all(): jnp.broadcast_to(x[None], (length, *x.shape))  8.16 us
  transfers between devices with their start and end apart: 9, of which 5 were waited for; matrix products, arithmetic and copies ran while one was open for 5% of the time, Pallas kernels for 4%

profile of v2, /device:TPU:128, one launch (start us, length us, event | category | flops | bytes accessed | tf_op | source)
XLA Modules:
  0.0 235.1 jit_solution(16286241646353604485)
XLA Ops:
  3.0 3.8 %all_to_all.45 = bf16[2,16,1024]{2,1,0:T(8,128)(2,1)S(1)} all-to-all(bf16[2,16,1024]{2,1,0:T(8,128)(2,1)S(1)} %pad_maximum_fusion), channel_id=1, replica_groups=mesh['zh'=4,'zl'=4,'x'=4,'c'=2,'tp'=4] {'c'}, dimensions={0} | all-to-all | bytes 131072 | tf_op jit(solution)/shard_map/all_to_all | solution.py:155
  6.8 31.0 %all_to_all.46 = bf16[4,32,1024]{2,1,0:T(8,128)(2,1)S(1)} all-to-all(bf16[4,32,1024]{2,1,0:T(8,128)(2,1)S(1)} %broadcast_in_dim.29), channel_id=1, replica_groups=mesh['zh'=4,'zl'=4,'x'=4,'c'=2,'tp'=4] {'zh'}, dimensions={0} | all-to-all | bytes 524288 | tf_op jit(solution)/shard_map/all_to_all | solution.py:23
  39.0 3.5 %all-to-all-start.2 = ((bf16[4,4,32,1024]{3,2,1,0:T(8,128)(2,1)}), bf16[4,4,32,1024]{3,2,1,0:T(8,128)(2,1)S(1)}, u32[]{:S(2)}, u32[]{:S(2)}) async-start(bf16[4,4,32,1024]{3,2,1,0:T(8,128)(2,1)} %broadcast_in_dim.30), calls=%async_computation.2 | async-start | bytes 2097152 | tf_op jit(solution)/shard_map/all_to_all | solution.py:23
  44.1 1.9 collective-permute-start
  46.0 20.5 %all-to-all-done.2 = bf16[4,4,32,1024]{3,2,1,0:T(8,128)(2,1)S(1)} async-done(((bf16[4,4,32,1024]{3,2,1,0:T(8,128)(2,1)}), bf16[4,4,32,1024]{3,2,1,0:T(8,128)(2,1)S(1)}, u32[]{:S(2)}, u32[]{:S(2)}) %all-to-all-start.2) | async-done | bytes 1048608 | tf_op jit(solution)/shard_map/all_to_all | solution.py:23
  66.6 2.0 broadcast_in_dim.31
  68.6 4.4 %all-to-all-start.3 = ((bf16[4,4,4,32,768]{4,3,2,1,0:T(8,128)(2,1)}), bf16[4,4,4,32,768]{4,3,2,1,0:T(8,128)(2,1)S(1)}, u32[]{:S(2)}, u32[]{:S(2)}) async-start(bf16[4,4,4,32,768]{4,3,2,1,0:T(8,128)(2,1)} %broadcast_in_dim.31), calls=%async_computation.3 | async-start | bytes 6291456 | tf_op jit(solution)/shard_map/all_to_all | solution.py:23
  73.0 1.9 collective-permute-start.2
  75.0 3.7 %broadcast_select_fusion = (bf16[256,2048]{1,0:T(8,128)(2,1)}, bf16[256,2048]{1,0:T(8,128)(2,1)}) fusion(bf16[256,2048]{1,0:T(8,128)(2,1)} %collective-permute-done, pred[]{:T(512)S(6)} %eq.2, f32[2048]{0:T(1024)S(1)} %bitcast.23, f32[256]{0:T(256)S(1)} %add_rsqrt_fusion, bf16[256,2048]{1,0:T(8,128)(2,1)} %param.8), kind=kLoop, calls=%fused_computation.6 | loop fusion | flops 3145728 | bytes 4203521 | tf_op jit(solution)/shard_map/jit(_where)/select_n | solution.py:167
  78.6 3.9 %collective-permute-start.1 = (bf16[256,2048]{1,0:T(8,128)(2,1)}, bf16[256,2048]{1,0:T(8,128)(2,1)}, u32[]{:S(2)}, u32[]{:S(2)}) collective-permute-start(bf16[256,2048]{1,0:T(8,128)(2,1)} %get-tuple-element.24.second), channel_id=1, source_target_pairs={{0,8},{4,12},{8,16},{12,20},{16,24},{20,28},{24,32},{28,36},{32,40... | collective-permute-start | bytes 3145736 | tf_op jit(solution)/shard_map/ppermute | solution.py:170
  83.2 3.4 %collective-permute-start.3 = (s32[256]{0:T(256)S(1)}, s32[256]{0:T(256)S(1)}, u32[]{:S(2)}, u32[]{:S(2)}) collective-permute-start(s32[256]{0:T(256)S(1)} %get-tuple-element.36), channel_id=1, source_target_pairs={{0,8},{4,12},{8,16},{12,20},{16,24},{20,28},{24,32},{28,36},{32,40... | collective-permute-start | bytes 3080 | tf_op jit(solution)/shard_map/ppermute | solution.py:170
  86.7 42.1 %collective-permute-done.3 = s32[256]{0:T(256)S(1)} collective-permute-done((s32[256]{0:T(256)S(1)}, s32[256]{0:T(256)S(1)}, u32[]{:S(2)}, u32[]{:S(2)}) %collective-permute-start.3) | collective-permute-done | bytes 1056 | tf_op jit(solution)/shard_map/ppermute | solution.py:170
  132.1 2.0 broadcast_in_dim.32
  134.1 21.2 %all-to-all-start.4 = ((bf16[4,4,4,32,256]{4,3,2,1,0:T(8,128)(2,1)}), bf16[4,4,4,32,256]{4,3,2,1,0:T(8,128)(2,1)}, u32[]{:S(2)}, u32[]{:S(2)}) async-start(bf16[4,4,4,32,256]{4,3,2,1,0:T(8,128)(2,1)} %broadcast_in_dim.32), calls=%async_computation.4 | async-start | bytes 2097152 | tf_op jit(solution)/shard_map/all_to_all | solution.py:23
  156.6 3.1 %shard_map.82 = (bf16[512,256]{1,0:T(8,128)(2,1)S(1)}, bf16[768,256]{1,0:T(8,128)(2,1)S(1)}) custom-call(bf16[256,2048]{1,0:T(8,128)(2,1)} %collective-permute-done.1.halo, bf16[256,2048]{1,0:T(8,128)(2,1)S(1)} %copy-done.1, bf16[256,2048]{1,0:T(8,128)(2,1)} %get-tuple-element.24.second, bf16[4,4,4,32,768]{4,3,2,1,0:T(8,128)(2,1)S(1)} %all-to-all-done.3.w_in), custom_call_target="tpu_custom_call" | custom-call | flops 20000000000 | bytes 4194304 | tf_op jit(solution)/shard_map/pallas_call | solution.py:109
  161.1 7.6 %all-to-all-done.4 = bf16[4,4,4,32,256]{4,3,2,1,0:T(8,128)(2,1)} async-done(((bf16[4,4,4,32,256]{4,3,2,1,0:T(8,128)(2,1)}), bf16[4,4,4,32,256]{4,3,2,1,0:T(8,128)(2,1)}, u32[]{:S(2)}, u32[]{:S(2)}) %all-to-all-start.4) | async-done | bytes 1048608 | tf_op jit(solution)/shard_map/all_to_all | solution.py:23
  168.7 2.8 %broadcast_in_dim.71 = bf16[2,4,4,4,32,256]{5,4,3,2,1,0:T(8,128)(2,1)} broadcast(bf16[4,4,4,32,256]{4,3,2,1,0:T(8,128)(2,1)} %all-to-all-done.4), dimensions={1,2,3,4,5} | broadcast | bytes 3145728 | tf_op jit(solution)/shard_map/broadcast_in_dim | solution.py:23
  171.5 4.8 %all-to-all-start.5 = ((bf16[2,4,4,4,32,256]{5,4,3,2,1,0:T(8,128)(2,1)}), bf16[2,4,4,4,32,256]{5,4,3,2,1,0:T(8,128)(2,1)}, u32[]{:S(2)}, u32[]{:S(2)}) async-start(bf16[2,4,4,4,32,256]{5,4,3,2,1,0:T(8,128)(2,1)} %broadcast_in_dim.71), calls=%async_computation.5 | async-start | bytes 4194304 | tf_op jit(solution)/shard_map/all_to_all | solution.py:23
  179.5 7.0 %shard_map.83 = bf16[512,256]{1,0:T(8,128)(2,1)S(1)} custom-call(bf16[256,2048]{1,0:T(8,128)(2,1)} %collective-permute-done.1.halo, bf16[256,2048]{1,0:T(8,128)(2,1)S(1)} %copy-done.2, bf16[256,2048]{1,0:T(8,128)(2,1)} %get-tuple-element.24.second, bf16[4,4,4,32,768]{4,3,2,1,0:T(8,128)(2,1)S(1)} %all-to-all-done.3.w_in, bf16[512,256]{1,0:T(8,128)(2,1)S(1)} %copy-done.7, ...), custom_call_target="tpu_custom_call" | custom-call | flops 20000000000 | bytes 4194304 | tf_op jit(solution)/shard_map/pallas_call | solution.py:109
  187.2 5.0 %all_to_all.47.att = bf16[2,256,256]{2,1,0:T(8,128)(2,1)S(1)} all-to-all(bf16[2,256,256]{2,1,0:T(8,128)(2,1)} %bitcast.19), channel_id=1, replica_groups=mesh['zh'=4,'zl'=4,'x'=4,'c'=2,'tp'=4] {'c'}, dimensions={0} | all-to-all | bytes 524288 | tf_op jit(solution)/shard_map/all_to_all | solution.py:190
  192.2 3.8 %shard_map.84 = bf16[256,2048]{1,0:T(8,128)(2,1)} custom-call(bf16[2,256,256]{2,1,0:T(8,128)(2,1)S(1)} %all_to_all.47.att, bf16[2,4,4,4,32,256]{5,4,3,2,1,0:T(8,128)(2,1)} %all-to-all-done.5.w_o), custom_call_target="tpu_custom_call" | custom-call | flops 20000000000 | bytes 4194304 | tf_op jit(solution)/shard_map/pallas_call | solution.py:109
  196.0 4.5 %all-to-all-start.7 = ((bf16[4,64,2048]{2,1,0:T(8,128)(2,1)}), bf16[4,64,2048]{2,1,0:T(8,128)(2,1)S(1)}, u32[]{:S(2)}, u32[]{:S(2)}) async-start(bf16[4,64,2048]{2,1,0:T(8,128)(2,1)} %bitcast.13), calls=%async_computation.7 | async-start | bytes 2097152 | tf_op jit(solution)/shard_map/all_to_all | solution.py:193
  200.5 15.4 %all-to-all-done.7 = bf16[4,64,2048]{2,1,0:T(8,128)(2,1)S(1)} async-done(((bf16[4,64,2048]{2,1,0:T(8,128)(2,1)}), bf16[4,64,2048]{2,1,0:T(8,128)(2,1)S(1)}, u32[]{:S(2)}, u32[]{:S(2)}) %all-to-all-start.7) | async-done | bytes 1048608 | tf_op jit(solution)/shard_map/all_to_all | solution.py:193
  217.2 17.0 %all_to_all.48 = bf16[4,64,2048]{2,1,0:T(8,128)(2,1)S(1)} all-to-all(bf16[4,64,2048]{2,1,0:T(8,128)(2,1)S(1)} %broadcast_in_dim.72), channel_id=1, replica_groups=mesh['zh'=4,'zl'=4,'x'=4,'c'=2,'tp'=4] {'tp'}, dimensions={0} | all-to-all | bytes 2097152 | tf_op jit(solution)/shard_map/all_to_all | solution.py:23
  (62 shorter events, 18.7 us)
Async XLA Ops:
  0.0 0.8 copy-start
  6.8 35.7 %copy-start.8 = (bf16[256,2048]{1,0:T(8,128)(2,1)S(1)}, bf16[256,2048]{1,0:T(8,128)(2,1)}, u32[]{:S(2)}) copy-start(bf16[256,2048]{1,0:T(8,128)(2,1)} %param.8) | copy-start | bytes 3145732
  37.9 5.0 %copy-start.10 = (f32[1,2048]{1,0:T(1,128)S(1)}, f32[1,2048]{1,0:T(1,128)}, u32[]{:S(2)}) copy-start(f32[1,2048]{1,0:T(1,128)} %param.10) | copy-start | bytes 24580
  39.0 27.5 %all-to-all-start.2 = ((bf16[4,4,32,1024]{3,2,1,0:T(8,128)(2,1)}), bf16[4,4,32,1024]{3,2,1,0:T(8,128)(2,1)S(1)}, u32[]{:S(2)}, u32[]{:S(2)}) async-start(bf16[4,4,32,1024]{3,2,1,0:T(8,128)(2,1)} %broadcast_in_dim.30), calls=%async_computation.2 | async-start | bytes 2097152 | tf_op jit(solution)/shard_map/all_to_all | solution.py:23
  44.1 30.9 %collective-permute-start = (bf16[256,2048]{1,0:T(8,128)(2,1)}, bf16[256,2048]{1,0:T(8,128)(2,1)}, u32[]{:S(2)}, u32[]{:S(2)}) collective-permute-start(bf16[256,2048]{1,0:T(8,128)(2,1)} %fusion.2), channel_id=1, source_target_pairs={{0,4},{4,0},{1,5},{5,1},{2,6},{6,2},{3,7},{7,3},{8,12},{12,8},{9,1... | collective-permute-start | bytes 3145736 | tf_op jit(solution)/shard_map/ppermute | solution.py:166
  66.5 2.1 copy-start.9
  68.6 4.4 %copy-start.12 = (s32[256]{0:T(256)S(1)}, s32[256]{0:T(256)}, u32[]{:S(2)}) copy-start(s32[256]{0:T(256)} %param.9) | copy-start | bytes 3076
  68.6 63.5 %all-to-all-start.3 = ((bf16[4,4,4,32,768]{4,3,2,1,0:T(8,128)(2,1)}), bf16[4,4,4,32,768]{4,3,2,1,0:T(8,128)(2,1)S(1)}, u32[]{:S(2)}, u32[]{:S(2)}) async-start(bf16[4,4,4,32,768]{4,3,2,1,0:T(8,128)(2,1)} %broadcast_in_dim.31), calls=%async_computation.3 | async-start | bytes 6291456 | tf_op jit(solution)/shard_map/all_to_all | solution.py:23
  73.0 10.2 %collective-permute-start.2 = (s32[256]{0:T(256)S(1)}, s32[256]{0:T(256)S(1)}, u32[]{:S(2)}, u32[]{:S(2)}) collective-permute-start(s32[256]{0:T(256)S(1)} %copy-done.12), channel_id=1, source_target_pairs={{0,4},{4,0},{1,5},{5,1},{2,6},{6,2},{3,7},{7,3},{8,12},{12,8},{9,1... | collective-permute-start | bytes 3080 | tf_op jit(solution)/shard_map/ppermute | solution.py:166
  75.0 7.6 %copy-start.11 = (f32[1,8,257]{2,1,0:T(8,128)S(1)}, f32[1,8,257]{2,1,0:T(8,128)}, u32[]{:S(2)}) copy-start(f32[1,8,257]{2,1,0:T(8,128)} %param.15) | copy-start | bytes 24676
  78.6 76.7 %collective-permute-start.1 = (bf16[256,2048]{1,0:T(8,128)(2,1)}, bf16[256,2048]{1,0:T(8,128)(2,1)}, u32[]{:S(2)}, u32[]{:S(2)}) collective-permute-start(bf16[256,2048]{1,0:T(8,128)(2,1)} %get-tuple-element.24.second), channel_id=1, source_target_pairs={{0,8},{4,12},{8,16},{12,20},{16,24},{20,28},{24,32},{28,36},{32,40... | collective-permute-start | bytes 3145736 | tf_op jit(solution)/shard_map/ppermute | solution.py:170
  83.2 45.6 %collective-permute-start.3 = (s32[256]{0:T(256)S(1)}, s32[256]{0:T(256)S(1)}, u32[]{:S(2)}, u32[]{:S(2)}) collective-permute-start(s32[256]{0:T(256)S(1)} %get-tuple-element.36), channel_id=1, source_target_pairs={{0,8},{4,12},{8,16},{12,20},{16,24},{20,28},{24,32},{28,36},{32,40... | collective-permute-start | bytes 3080 | tf_op jit(solution)/shard_map/ppermute | solution.py:170
  134.1 34.6 %all-to-all-start.4 = ((bf16[4,4,4,32,256]{4,3,2,1,0:T(8,128)(2,1)}), bf16[4,4,4,32,256]{4,3,2,1,0:T(8,128)(2,1)}, u32[]{:S(2)}, u32[]{:S(2)}) async-start(bf16[4,4,4,32,256]{4,3,2,1,0:T(8,128)(2,1)} %broadcast_in_dim.32), calls=%async_computation.4 | async-start | bytes 2097152 | tf_op jit(solution)/shard_map/all_to_all | solution.py:23
  155.3 1.2 copy-start.1
  159.6 0.8 copy-start.4
  160.4 0.7 copy-start.6
  171.5 15.7 %all-to-all-start.5 = ((bf16[2,4,4,4,32,256]{5,4,3,2,1,0:T(8,128)(2,1)}), bf16[2,4,4,4,32,256]{5,4,3,2,1,0:T(8,128)(2,1)}, u32[]{:S(2)}, u32[]{:S(2)}) async-start(bf16[2,4,4,4,32,256]{5,4,3,2,1,0:T(8,128)(2,1)} %broadcast_in_dim.71), calls=%async_computation.5 | async-start | bytes 4194304 | tf_op jit(solution)/shard_map/all_to_all | solution.py:23
  176.4 1.2 copy-start.2
  177.6 1.0 copy-start.5
  178.6 0.9 copy-start.7
  186.5 0.7 copy-start.3
  196.0 19.9 %all-to-all-start.7 = ((bf16[4,64,2048]{2,1,0:T(8,128)(2,1)}), bf16[4,64,2048]{2,1,0:T(8,128)(2,1)S(1)}, u32[]{:S(2)}, u32[]{:S(2)}) async-start(bf16[4,64,2048]{2,1,0:T(8,128)(2,1)} %bitcast.13), calls=%async_computation.7 | async-start | bytes 2097152 | tf_op jit(solution)/shard_map/all_to_all | solution.py:193

commit v3 on v2

v3 whole, which is shorter than its diff:
```python
import jax
import jax.numpy as jnp
from jax import lax
from jax.experimental import pallas as pl
from jax.experimental.pallas import tpu as pltpu
from jax.sharding import Mesh
from jax.sharding import PartitionSpec as P

HEAD_DIM = 64
SEG = 64
LEFT = 4
REL_CLIP = 128
EPS = 1e-06
REACH = LEFT * SEG
Q_BLOCK = 2 * SEG
K_BLOCK = Q_BLOCK + REACH
SP = ("zh", "zl", "x", "c")
NEG = -1e30


def to_all(x, axis):
    length = lax.axis_size(axis)
    return lax.all_to_all(jnp.broadcast_to(x[None], (length, *x.shape)), axis, 0, 0, tiled=True)


def lay(w_ref, cols, into):
    n_x, n_l, n_h, rows = w_ref.shape[:4]
    for h in range(n_h):
        for l in range(n_l):
            for x in range(n_x):
                at = ((h * n_l + l) * n_x + x) * rows
                into[at : at + rows, :] = w_ref[x, l, h, :, cols]


def norm_kernel(tokens, gain, docs, out):
    rows = tokens.shape[0]
    wide = tokens[...].astype(jnp.float32)
    scale = lax.rsqrt(jnp.mean(wide * wide, axis=1, keepdims=True) + EPS)
    out[:rows, :] = (wide * scale * gain[...]).astype(jnp.bfloat16)
    extra = out.shape[0] - rows
    out[rows:, :rows] = jnp.broadcast_to(docs[...].astype(jnp.float32), (extra, rows)).astype(jnp.bfloat16)
    out[rows:, rows:] = jnp.zeros((extra, out.shape[1] - rows), jnp.bfloat16)


def attend_kernel(ids, halo, mine, other, w_in, line, out, w_all, q, k, v, docs):
    width = q.shape[1]
    rows = q.shape[0] // 2
    core = ids[0]
    lay(w_in, slice(0, 3 * width), w_all)

    def doc_row(part):
        return part[rows : rows + 16, :rows].astype(jnp.float32)[0:1]

    docs[0:1, :rows] = jnp.where(ids[1] > 0, doc_row(halo), -1.0)
    before = jnp.dot(halo[:rows, :], w_all[:, width:], preferred_element_type=jnp.float32).astype(jnp.bfloat16)
    k[:rows, :] = before[:, :width]
    v[:rows, :] = before[:, width:]
    for part, at in ((mine, core), (other, 1 - core)):
        total = jnp.dot(part[:rows, :], w_all[...], preferred_element_type=jnp.float32).astype(jnp.bfloat16)
        to = pl.multiple_of(at * rows, rows)
        q[pl.ds(to, rows), :] = total[:, :width]
        k[pl.ds(to + rows, rows), :] = total[:, width : 2 * width]
        v[pl.ds(to + rows, rows), :] = total[:, 2 * width :]
    docs[0:1, rows : 2 * rows] = jnp.where(core == 0, doc_row(mine), doc_row(other))
    docs[0:1, 2 * rows :] = jnp.where(core == 0, doc_row(other), doc_row(mine))
    q_seg = lax.broadcasted_iota(jnp.int32, (Q_BLOCK, K_BLOCK), 0) // SEG
    k_seg = lax.broadcasted_iota(jnp.int32, (Q_BLOCK, K_BLOCK), 1) // SEG
    window = (k_seg >= q_seg) & (k_seg <= q_seg + LEFT)
    blocks = q.shape[0] // Q_BLOCK
    same = []
    for b in range(blocks):
        lo = b * Q_BLOCK
        across = jnp.broadcast_to(docs[0:1, rows + lo : rows + lo + Q_BLOCK], (Q_BLOCK, Q_BLOCK))
        down = jnp.concatenate([across.T] * (K_BLOCK // Q_BLOCK), axis=1)
        same.append((down == docs[0:1, lo : lo + K_BLOCK]) & window)
    for h in range(q.shape[1] // HEAD_DIM):
        cols = slice(h * HEAD_DIM, (h + 1) * HEAD_DIM)
        flat = jnp.broadcast_to(line[h : h + 1, :], (Q_BLOCK, line.shape[1]))
        bias = pltpu.roll(flat, 0, 1, stride=1, stride_axis=0)[:, :K_BLOCK]
        for b in range(blocks):
            lo = b * Q_BLOCK
            scores = lax.dot_general(
                q[lo : lo + Q_BLOCK, cols],
                k[lo : lo + K_BLOCK, cols],
                (((1,), (1,)), ((), ())),
                preferred_element_type=jnp.float32,
            )
            scores = jnp.where(same[b], scores * HEAD_DIM ** (-0.5) + bias, NEG)
            peak = jnp.max(scores, axis=1, keepdims=True)
            raised = jnp.exp(scores - peak)
            total = jnp.sum(raised, axis=1, keepdims=True)
            mixed = jnp.dot(
                raised.astype(jnp.bfloat16), v[lo : lo + K_BLOCK, cols], preferred_element_type=jnp.float32
            )
            out[lo : lo + Q_BLOCK, cols] = (mixed / total).astype(jnp.bfloat16)


def project_kernel(ids, att, w_in, w_other, out):
    n_x, n_l, n_h, rows, width = w_other.shape
    lanes = n_x * rows
    core = ids[0]
    start = w_in.shape[-1] - width
    for h in range(n_h):
        for l in range(n_l):
            mine = w_in[:, l, h, :, start:].reshape(lanes, width)
            other = w_other[:, l, h].reshape(lanes, width)
            total = sum(
                lax.dot_general(att[i], w, (((1,), (1,)), ((), ())), preferred_element_type=jnp.float32)
                for i, w in ((core, mine), (1 - core, other))
            )
            at = (h * n_l + l) * lanes
            out[:, at : at + lanes] = total.astype(jnp.bfloat16)


def in_vmem(kernel, outs, scratch=(), grant=16, flops=2 * 10**10):
    one = not isinstance(outs, (list, tuple))
    shapes = [outs] if one else list(outs)
    specs = [pl.BlockSpec(memory_space=pltpu.VMEM) for _ in shapes]

    def call(*args):
        return pl.pallas_call(
            kernel,
            out_shape=shapes[0] if one else shapes,
            in_specs=[pl.BlockSpec(memory_space=pltpu.SMEM if a.shape == (2,) else pltpu.VMEM) for a in args],
            out_specs=specs[0] if one else specs,
            scratch_shapes=list(scratch),
            compiler_params=pltpu.CompilerParams(vmem_limit_bytes=grant * 2**20),
            cost_estimate=pl.CostEstimate(flops=flops, bytes_accessed=4 * 2**20, transcendentals=0),
        )(*args)

    return call


def bias_line(table):
    far = table[:, 2 * REL_CLIP :]
    near = table[:, 1:][:, ::-1]
    heads = table.shape[0]
    return jnp.concatenate(
        [
            jnp.broadcast_to(far, (heads, REACH - REL_CLIP)),
            near,
            table[:, :1],
            jnp.broadcast_to(far, (heads, Q_BLOCK - 1)),
        ],
        axis=1,
    )


def body(tokens, documents, norm_gain, w_query, w_key, w_value, w_out, rel_bias):
    rows, width = tokens.shape
    local = w_query.shape[2]
    half = local // 2
    core = lax.axis_index("c")
    tp = lax.axis_index("tp")
    n_tp = lax.axis_size("tp")
    chips = lax.axis_size(SP[:-1])
    chip = lax.axis_index(SP[:-1])

    piece = w_query.shape[1]
    w_mine = lax.dynamic_slice_in_dim(w_out[0].T, tp * local, local, 1)
    packed = jnp.stack(
        [
            jnp.concatenate([w[:, c * half : (c + 1) * half] for w in (w_query[0], w_key[0], w_value[0], w_mine)], axis=1)
            for c in range(2)
        ]
    )
    bf = jnp.bfloat16
    share = rows // n_tp
    at = lax.dynamic_slice_in_dim(tokens, tp * share, share, 0).astype(jnp.float32)
    line = bias_line(lax.dynamic_slice_in_dim(rel_bias[0], core * (rel_bias.shape[1] // 2), rel_bias.shape[1] // 2, 0))
    ids = jnp.stack([core, chip])
    block = in_vmem(norm_kernel, jax.ShapeDtypeStruct((rows + 16, width), bf), flops=10**9)(
        tokens, norm_gain, documents[None, :]
    )
    other = lax.ppermute(block, "c", [(0, 1), (1, 0)])
    mine = lax.all_to_all(packed, "c", 0, 0, tiled=True).reshape(2 * piece, 4 * half)
    last = jnp.where(core == 0, other, block)
    last, mine, line, at, ids = lax.optimization_barrier((last, mine, line, at, ids))
    onward = [(2 * i + c, 2 * i + 2 + c) for i in range(chips - 1) for c in range(2)]
    halo = lax.ppermute(last, SP, onward)
    over_far = to_all(mine, "zh")
    w_in = to_all(to_all(over_far, "zl"), "x")
    w_other = lax.ppermute(w_in[..., 3 * half :], "c", [(0, 1), (1, 0)])
    att = in_vmem(
        attend_kernel,
        jax.ShapeDtypeStruct((2 * rows, half), bf),
        [
            pltpu.VMEM((width, 3 * half), bf),
            pltpu.VMEM((2 * rows, half), bf),
            pltpu.VMEM((3 * rows, half), bf),
            pltpu.VMEM((3 * rows, half), bf),
            pltpu.VMEM((8, 3 * rows), jnp.float32),
        ],
    )(ids, halo, block, other, w_in, line)
    att = lax.all_to_all(att.reshape(2, rows, half), "c", 0, 0, tiled=True)
    partial = in_vmem(project_kernel, jax.ShapeDtypeStruct((rows, width), bf))(ids, att, w_in, w_other)
    partial = lax.all_to_all(partial.reshape(n_tp, share, width), "tp", 0, 0, tiled=True)
    mixed = (at + jnp.sum(partial.astype(jnp.float32), axis=0)).astype(bf)
    return to_all(mixed, "tp").reshape(rows, width)


def solution(mesh):
    split = Mesh(mesh.devices.reshape(4, 4, 4, 2, mesh.shape["tp"]), (*SP, "tp"))
    placed = (
        P(SP, None),
        P(SP),
        P(),
        P(None, SP, "tp"),
        P(None, SP, "tp"),
        P(None, SP, "tp"),
        P(None, None, SP),
        P(None, "tp", None),
    )

    def step(*args):
        return body(*args)

    step = jax.shard_map(step, mesh=split, in_specs=placed, out_specs=P(SP, None), check_vma=False)
    return step
```

time: 236 us -> 214 us (0.907)
  the two profiles are of different devices: /device:TPU:128 before, /device:TPU:32 now
where the time goes in v3:
time: 214 us; the launch traced here: 213 us
  blocking collectives  103 us (48%)
  waiting for transfers between devices  67.2 us (31%)
  starting transfers between devices  15.8 us (7%)
  Pallas kernels  13.2 us (6%)
  local copies, waits for them, and re-layouts  9.2 us (4%)
  other arithmetic  3.99 us (2%)
    all_to_all x3, blocking collectives, to_all(): lax.all_to_all(jnp.broadcast_to(x[None], (length, *x.shape)), axis, 0, 0,...  79.4 us
    all_to_all x1, waiting for transfers between devices, to_all(): lax.all_to_all(jnp.broadcast_to(x[None], (length, *x.shape)), axis, 0, 0,...  67.2 us
    all_to_all x1, blocking collectives, body(): lax.all_to_all(partial.reshape(n_tp, share, width), 'tp', 0, 0, tiled=True)  19.7 us
    pallas_call x3, Pallas kernels, call(): pl.pallas_call(kernel, out_shape=shapes[0] if one else shapes, in_specs=[...  13.2 us
    all_to_all x1, starting transfers between devices, to_all(): lax.all_to_all(jnp.broadcast_to(x[None], (length, *x.shape)), axis, 0, 0,...  4.84 us
    unnamed x19, local copies, waits for them, and re-layouts  4.5 us
  transfers between devices with their start and end apart: 5, of which 1 were waited for; matrix products, arithmetic and copies ran while one was open for 3% of the time, Pallas kernels for 4%

profile of v3, /device:TPU:32, one launch (start us, length us, event | category | flops | bytes accessed | tf_op | source)
XLA Modules:
  0.0 212.8 jit_solution(17527228399529544255)
XLA Ops:
  0.0 1.3 copy-done.1
  1.3 0.7 copy-done.2
  2.0 0.7 copy-done.3
  2.6 0.4 shard_map.82.mine
  3.1 1.9 collective-permute-start
  5.1 0.6 pad_maximum_fusion
  5.7 3.3 %all-to-all-start = ((bf16[2,16,1024]{2,1,0:T(8,128)(2,1)}), bf16[2,16,1024]{2,1,0:T(8,128)(2,1)S(1)}, u32[]{:S(2)}, u32[]{:S(2)}) async-start(bf16[2,16,1024]{2,1,0:T(8,128)(2,1)} %pad_maximum_fusion), calls=%async_computation | async-start | bytes 131072 | tf_op jit(solution)/shard_map/all_to_all | solution.py:176
  9.8 1.8 dynamic-slice_convert_fusion
  11.5 1.2 broadcast_select_fusion
  12.8 36.0 %all_to_all.35 = bf16[4,32,1024]{2,1,0:T(8,128)(2,1)S(1)} all-to-all(bf16[4,32,1024]{2,1,0:T(8,128)(2,1)S(1)} %broadcast_in_dim.20), channel_id=1, replica_groups=mesh['zh'=4,'zl'=4,'x'=4,'c'=2,'tp'=4] {'zh'}, dimensions={0} | all-to-all | bytes 524288 | tf_op jit(solution)/shard_map/all_to_all | solution.py:23
  48.9 26.8 %all_to_all.36 = bf16[4,4,32,1024]{3,2,1,0:T(8,128)(2,1)S(1)} all-to-all(bf16[4,4,32,1024]{3,2,1,0:T(8,128)(2,1)S(1)} %broadcast_in_dim.21), channel_id=1, replica_groups=mesh['zh'=4,'zl'=4,'x'=4,'c'=2,'tp'=4] {'zl'}, dimensions={0} | all-to-all | bytes 2097152 | tf_op jit(solution)/shard_map/all_to_all | solution.py:23
  75.6 2.6 %broadcast_in_dim.22 = bf16[4,4,4,32,1024]{4,3,2,1,0:T(8,128)(2,1)} broadcast(bf16[4,4,32,1024]{3,2,1,0:T(8,128)(2,1)S(1)} %all_to_all.36), dimensions={1,2,3,4} | broadcast | bytes 5242880 | tf_op jit(solution)/shard_map/broadcast_in_dim | solution.py:23
  78.2 4.8 %all-to-all-start.3 = ((bf16[4,4,4,32,1024]{4,3,2,1,0:T(8,128)(2,1)}), bf16[4,4,4,32,1024]{4,3,2,1,0:T(8,128)(2,1)}, u32[]{:S(2)}, u32[]{:S(2)}) async-start(bf16[4,4,4,32,1024]{4,3,2,1,0:T(8,128)(2,1)} %broadcast_in_dim.22), calls=%async_computation.3 | async-start | bytes 8388608 | tf_op jit(solution)/shard_map/all_to_all | solution.py:23
  83.1 3.9 %collective-permute-start.1 = (bf16[272,2048]{1,0:T(8,128)(2,1)}, bf16[272,2048]{1,0:T(8,128)(2,1)S(1)}, u32[]{:S(2)}, u32[]{:S(2)}) collective-permute-start(bf16[272,2048]{1,0:T(8,128)(2,1)} %broadcast_select_fusion), channel_id=1, source_target_pairs={{0,8},{4,12},{8,16},{12,20},{16,24},{20,28},{24,32},{28,36},{32,40... | collective-permute-start | bytes 3342344 | tf_op jit(solution)/shard_map/ppermute | solution.py:180
  87.0 67.2 %all-to-all-done.3.w_in = bf16[4,4,4,32,1024]{4,3,2,1,0:T(8,128)(2,1)} async-done(((bf16[4,4,4,32,1024]{4,3,2,1,0:T(8,128)(2,1)}), bf16[4,4,4,32,1024]{4,3,2,1,0:T(8,128)(2,1)}, u32[]{:S(2)}, u32[]{:S(2)}) %all-to-all-start.3) | async-done | bytes 4194336 | tf_op jit(solution)/shard_map/all_to_all | solution.py:23
  154.2 1.3 slice.59
  155.5 1.9 collective-permute-start.2
  157.4 9.4 %shard_map.83 = bf16[512,256]{1,0:T(8,128)(2,1)S(1)} custom-call(s32[2]{0:T(128)S(1)} %pad_add_fusion.ids, bf16[272,2048]{1,0:T(8,128)(2,1)S(1)} %collective-permute-done.1.halo, bf16[272,2048]{1,0:T(8,128)(2,1)S(1)} %shard_map.82.mine, bf16[272,2048]{1,0:T(8,128)(2,1)S(1)} %collective-permute-done.other, bf16[4,4,4,32,1024]{4,3,2,1,0:T(8,128)(2,1)} %all-to-all-done.3.w_in, ...), custom_call_target="tpu_custom_call" | custom-call | flops 20000000000 | bytes 4194304 | tf_op jit(solution)/shard_map/pallas_call | solution.py:121
  166.8 4.0 %all_to_all.37.att = bf16[2,256,256]{2,1,0:T(8,128)(2,1)S(1)} all-to-all(bf16[2,256,256]{2,1,0:T(8,128)(2,1)S(1)} %bitcast.21), channel_id=1, replica_groups=mesh['zh'=4,'zl'=4,'x'=4,'c'=2,'tp'=4] {'c'}, dimensions={0} | all-to-all | bytes 524288 | tf_op jit(solution)/shard_map/all_to_all | solution.py:195
  170.8 3.4 %shard_map.84 = bf16[256,2048]{1,0:T(8,128)(2,1)S(1)} custom-call(s32[2]{0:T(128)S(1)} %pad_add_fusion.ids, bf16[2,256,256]{2,1,0:T(8,128)(2,1)S(1)} %all_to_all.37.att, bf16[4,4,4,32,1024]{4,3,2,1,0:T(8,128)(2,1)} %all-to-all-done.3.w_in, bf16[4,4,4,32,256]{4,3,2,1,0:T(8,128)(2,1)S(1)} %collective-permute-done.2.w_other), custom_call_target="tpu_custom_call" | custom-call | flops 20000000000 | bytes 4194304 | tf_op jit(solution)/shard_map/pallas_call | solution.py:121
  174.2 19.7 %all_to_all.38 = bf16[4,64,2048]{2,1,0:T(8,128)(2,1)S(1)} all-to-all(bf16[4,64,2048]{2,1,0:T(8,128)(2,1)S(1)} %bitcast.20), channel_id=1, replica_groups=mesh['zh'=4,'zl'=4,'x'=4,'c'=2,'tp'=4] {'tp'}, dimensions={0} | all-to-all | bytes 2097152 | tf_op jit(solution)/shard_map/all_to_all | solution.py:197
  194.1 0.9 copy-done.4
  195.1 16.7 %all_to_all.39 = bf16[4,64,2048]{2,1,0:T(8,128)(2,1)S(1)} all-to-all(bf16[4,64,2048]{2,1,0:T(8,128)(2,1)S(1)} %broadcast_in_dim.46), channel_id=1, replica_groups=mesh['zh'=4,'zl'=4,'x'=4,'c'=2,'tp'=4] {'tp'}, dimensions={0} | all-to-all | bytes 2097152 | tf_op jit(solution)/shard_map/all_to_all | solution.py:23
  211.8 1.0 copy.10
  (37 shorter events, 1.2 us)
Async XLA Ops:
  0.0 5.0 %copy-start = (bf16[1,2048,16]{1,2,0:T(8,128)(2,1)S(1)}, bf16[1,2048,16]{1,2,0:T(8,128)(2,1)}, u32[]{:S(2)}) copy-start(bf16[1,2048,16]{1,2,0:T(8,128)(2,1)} %param.14) | copy-start | bytes 196612
  0.0 1.3 copy-start.1
  1.3 0.7 copy-start.2
  2.0 0.7 copy-start.3
  2.6 2.4 %copy-start.5 = (bf16[1,16,512]{2,1,0:T(8,128)(2,1)S(1)}, bf16[1,16,512]{2,1,0:T(8,128)(2,1)}, u32[]{:S(2)}) copy-start(bf16[1,16,512]{2,1,0:T(8,128)(2,1)} %param.11) | copy-start | bytes 49156
  2.6 2.4 %copy-start.6 = (bf16[1,16,512]{2,1,0:T(8,128)(2,1)S(1)}, bf16[1,16,512]{2,1,0:T(8,128)(2,1)}, u32[]{:S(2)}) copy-start(bf16[1,16,512]{2,1,0:T(8,128)(2,1)} %param.12) | copy-start | bytes 49156
  2.6 2.4 %copy-start.7 = (bf16[1,16,512]{2,1,0:T(8,128)(2,1)S(1)}, bf16[1,16,512]{2,1,0:T(8,128)(2,1)}, u32[]{:S(2)}) copy-start(bf16[1,16,512]{2,1,0:T(8,128)(2,1)} %param.13) | copy-start | bytes 49156
  2.6 6.4 %copy-start.8 = (f32[1,8,257]{2,1,0:T(8,128)S(1)}, f32[1,8,257]{2,1,0:T(8,128)}, u32[]{:S(2)}) copy-start(f32[1,8,257]{2,1,0:T(8,128)} %param.15) | copy-start | bytes 24676
  3.1 8.5 %collective-permute-start = (bf16[272,2048]{1,0:T(8,128)(2,1)S(1)}, bf16[272,2048]{1,0:T(8,128)(2,1)S(1)}, u32[]{:S(2)}, u32[]{:S(2)}) collective-permute-start(bf16[272,2048]{1,0:T(8,128)(2,1)S(1)} %shard_map.82.mine), channel_id=1, source_target_pairs={{0,4},{4,0},{1,5},{5,1},{2,6},{6,2},{3,7},{7,3},{8,12},{12,8},{9,1... | collective-permute-start | bytes 3342344 | tf_op jit(solution)/shard_map/ppermute | solution.py:175
  5.7 7.0 %all-to-all-start = ((bf16[2,16,1024]{2,1,0:T(8,128)(2,1)}), bf16[2,16,1024]{2,1,0:T(8,128)(2,1)S(1)}, u32[]{:S(2)}, u32[]{:S(2)}) async-start(bf16[2,16,1024]{2,1,0:T(8,128)(2,1)} %pad_maximum_fusion), calls=%async_computation | async-start | bytes 131072 | tf_op jit(solution)/shard_map/all_to_all | solution.py:176
  78.2 76.0 %all-to-all-start.3 = ((bf16[4,4,4,32,1024]{4,3,2,1,0:T(8,128)(2,1)}), bf16[4,4,4,32,1024]{4,3,2,1,0:T(8,128)(2,1)}, u32[]{:S(2)}, u32[]{:S(2)}) async-start(bf16[4,4,4,32,1024]{4,3,2,1,0:T(8,128)(2,1)} %broadcast_in_dim.22), calls=%async_computation.3 | async-start | bytes 8388608 | tf_op jit(solution)/shard_map/all_to_all | solution.py:23
  83.1 74.4 %collective-permute-start.1 = (bf16[272,2048]{1,0:T(8,128)(2,1)}, bf16[272,2048]{1,0:T(8,128)(2,1)S(1)}, u32[]{:S(2)}, u32[]{:S(2)}) collective-permute-start(bf16[272,2048]{1,0:T(8,128)(2,1)} %broadcast_select_fusion), channel_id=1, source_target_pairs={{0,8},{4,12},{8,16},{12,20},{16,24},{20,28},{24,32},{28,36},{32,40... | collective-permute-start | bytes 3342344 | tf_op jit(solution)/shard_map/ppermute | solution.py:180
  155.5 15.3 %collective-permute-start.2 = (bf16[4,4,4,32,256]{4,3,2,1,0:T(8,128)(2,1)S(1)}, bf16[4,4,4,32,256]{4,3,2,1,0:T(8,128)(2,1)S(1)}, u32[]{:S(2)}, u32[]{:S(2)}) collective-permute-start(bf16[4,4,4,32,256]{4,3,2,1,0:T(8,128)(2,1)S(1)} %slice.59), channel_id=1, source_target_pairs={{0,4},{4,0},{1,5},{5,1},{2,6},{6,2},{3,7},{7,3},{8,12},{12,8},{9,1... | collective-permute-start | bytes 3145736 | tf_op jit(solution)/shard_map/ppermute | solution.py:183
  193.9 1.0 copy-start.4

commit v4 on v3

v4 whole, which is shorter than its diff:
```python
import jax
import jax.numpy as jnp
from jax import lax
from jax.experimental import pallas as pl
from jax.experimental.pallas import tpu as pltpu
from jax.sharding import Mesh
from jax.sharding import PartitionSpec as P

HEAD_DIM = 64
SEG = 64
LEFT = 4
REL_CLIP = 128
EPS = 1e-06
REACH = LEFT * SEG
Q_BLOCK = 2 * SEG
K_BLOCK = Q_BLOCK + REACH
SP = ("zh", "zl", "x", "c")
NEG = -1e30


def to_all(x, axis):
    length = lax.axis_size(axis)
    return lax.all_to_all(jnp.broadcast_to(x[None], (length, *x.shape)), axis, 0, 0, tiled=True)


def norm_kernel(tokens, gain, docs, out):
    rows = tokens.shape[0]
    wide = tokens[...].astype(jnp.float32)
    scale = lax.rsqrt(jnp.mean(wide * wide, axis=1, keepdims=True) + EPS)
    out[:rows, :] = (wide * scale * gain[...]).astype(jnp.bfloat16)
    extra = out.shape[0] - rows
    out[rows:, :rows] = jnp.broadcast_to(docs[...].astype(jnp.float32), (extra, rows)).astype(jnp.bfloat16)
    out[rows:, rows:] = jnp.zeros((extra, out.shape[1] - rows), jnp.bfloat16)


def qkv_kernel(ids, b0, s0, b1, s1, b2, s2, b3, s3, w_in, qkv, docs, tail, w_all):
    rows = qkv.shape[0] // 8
    n_l, n_h, lanes = w_in.shape[:3]
    for h in range(n_h):
        for l in range(n_l):
            at = (h * n_l + l) * lanes
            w_all[at : at + lanes, :] = w_in[l, h]
    core, x = ids[0], ids[1]
    for back, pair in enumerate(((b0, s0), (b1, s1), (b2, s2), (b3, s3))):
        for c, part in zip((core, 1 - core), pair):
            at = ((x + 4 - back) & 3) * 2 + c
            total = jnp.dot(part[:rows, :], w_all[...], preferred_element_type=jnp.float32)
            qkv[pl.ds(pl.multiple_of(at * rows, rows), rows), :] = total.astype(jnp.bfloat16)
            docs[pl.ds(at, 1), :] = part[rows : rows + 16, :rows].astype(jnp.float32)[0:1]
    tail[:rows, :] = qkv[7 * rows :, :]
    tail[rows:, :] = jnp.broadcast_to(docs[7:8, :], (16, rows)).astype(jnp.bfloat16)


def attend_kernel(ids, qkv, halo, docs, line, out):
    rows = docs.shape[1]
    flat = jnp.broadcast_to(line[...], (Q_BLOCK, line.shape[1]))
    bias = pltpu.roll(flat, 0, 1, stride=1, stride_axis=0)[:, :K_BLOCK]
    q_seg = lax.broadcasted_iota(jnp.int32, (Q_BLOCK, K_BLOCK), 0) // SEG
    k_seg = lax.broadcasted_iota(jnp.int32, (Q_BLOCK, K_BLOCK), 1) // SEG
    bias = jnp.where((k_seg >= q_seg) & (k_seg <= q_seg + LEFT), bias, NEG)
    prior = jnp.where(ids[2] > 0, halo[rows : rows + 16, :].astype(jnp.float32)[0:1], -1.0)

    def doc_part(b):
        if b < 0:
            return prior[:, rows + b * Q_BLOCK : rows + (b + 1) * Q_BLOCK]
        at = b * Q_BLOCK % rows
        return docs[b * Q_BLOCK // rows : b * Q_BLOCK // rows + 1, at : at + Q_BLOCK]

    def row_part(b, cols):
        if b < 0:
            return halo[rows + b * Q_BLOCK : rows + (b + 1) * Q_BLOCK, cols]
        return qkv[b * Q_BLOCK : (b + 1) * Q_BLOCK, cols]

    def key_rows(b, cols):
        if b >= 2:
            return qkv[(b - 2) * Q_BLOCK : (b + 1) * Q_BLOCK, cols]
        return jnp.concatenate([row_part(i, cols) for i in range(b - 2, b + 1)], axis=0)

    for b in range(qkv.shape[0] // Q_BLOCK):
        across = jnp.broadcast_to(doc_part(b), (Q_BLOCK, Q_BLOCK)).T
        same = jnp.concatenate([across == doc_part(i) for i in range(b - 2, b + 1)], axis=1)
        scores = lax.dot_general(
            qkv[b * Q_BLOCK : (b + 1) * Q_BLOCK, :HEAD_DIM],
            key_rows(b, slice(HEAD_DIM, 2 * HEAD_DIM)),
            (((1,), (1,)), ((), ())),
            preferred_element_type=jnp.float32,
        )
        scores = jnp.where(same, scores * HEAD_DIM ** (-0.5) + bias, NEG)
        peak = jnp.max(scores, axis=1, keepdims=True)
        raised = jnp.exp(scores - peak)
        total = jnp.sum(raised, axis=1, keepdims=True)
        mixed = jnp.dot(
            raised.astype(jnp.bfloat16),
            key_rows(b, slice(2 * HEAD_DIM, 3 * HEAD_DIM)),
            preferred_element_type=jnp.float32,
        )
        lane = b % 2 * HEAD_DIM
        out[b // 2, :, lane : lane + HEAD_DIM] = (mixed / total).astype(jnp.bfloat16)


def out_rows_kernel(w_in, out):
    n_l, n_h = w_in.shape[:2]
    for h in range(n_h):
        for l in range(n_l):
            at = (h * n_l + l) * 16
            out[at : at + 16, :] = jnp.concatenate(
                [w_in[l, h, 16 * j : 16 * j + 16, 3 * HEAD_DIM :] for j in range(8)], axis=1
            )


def project_kernel(ids, att, w_mine, w_other, out, lhs, rhs):
    half = att.shape[1]
    for i in range(att.shape[0]):
        lhs[:half, i * HEAD_DIM : (i + 1) * HEAD_DIM] = att[i, :, :HEAD_DIM]
        lhs[half:, i * HEAD_DIM : (i + 1) * HEAD_DIM] = att[i, :, HEAD_DIM:]
    core = ids[0]
    for c, w in ((core, w_mine), (1 - core, w_other)):
        for z in range(16):
            for x in range(4):
                to = pl.multiple_of(z * 128 + x * 32 + c * 16, 16)
                rhs[pl.ds(to, 16), :] = w[x, z * 16 : z * 16 + 16, :]
    out[...] = lax.dot_general(
        lhs[...], rhs[...], (((1,), (1,)), ((), ())), preferred_element_type=jnp.float32
    ).astype(jnp.bfloat16)


def in_vmem(kernel, outs, scratch=(), grant=16, flops=2 * 10**10):
    one = not isinstance(outs, (list, tuple))
    shapes = [outs] if one else list(outs)
    specs = [pl.BlockSpec(memory_space=pltpu.VMEM) for _ in shapes]

    def call(*args):
        return pl.pallas_call(
            kernel,
            out_shape=shapes[0] if one else shapes,
            in_specs=[pl.BlockSpec(memory_space=pltpu.SMEM if a.ndim == 1 else pltpu.VMEM) for a in args],
            out_specs=specs[0] if one else specs,
            scratch_shapes=list(scratch),
            compiler_params=pltpu.CompilerParams(vmem_limit_bytes=grant * 2**20),
            cost_estimate=pl.CostEstimate(flops=flops, bytes_accessed=4 * 2**20, transcendentals=0),
        )(*args)

    return call


def bias_line(table):
    far = table[:, 2 * REL_CLIP :]
    near = table[:, 1:][:, ::-1]
    heads = table.shape[0]
    return jnp.concatenate(
        [
            jnp.broadcast_to(far, (heads, REACH - REL_CLIP)),
            near,
            table[:, :1],
            jnp.broadcast_to(far, (heads, Q_BLOCK - 1)),
        ],
        axis=1,
    )


def body(tokens, documents, norm_gain, w_query, w_key, w_value, w_out, rel_bias):
    rows, width = tokens.shape
    local = w_query.shape[2]
    core = lax.axis_index("c")
    x = lax.axis_index("x")
    z = lax.axis_index(("zh", "zl"))
    tp = lax.axis_index("tp")
    n_tp = lax.axis_size("tp")
    plane = ("x", "c")
    group = lax.axis_size(plane)
    bf = jnp.bfloat16

    piece = w_query.shape[1]
    w_mine = lax.dynamic_slice_in_dim(w_out[0].T, tp * local, local, 1)
    by_head = [w.reshape(piece, group, HEAD_DIM).swapaxes(0, 1) for w in (w_query[0], w_key[0], w_value[0], w_mine)]
    packed = jnp.concatenate(by_head[:3], axis=2)

    share = rows // n_tp
    at = lax.dynamic_slice_in_dim(tokens, tp * share, share, 0).astype(jnp.float32)
    line = bias_line(lax.dynamic_slice_in_dim(rel_bias[0], x * 2 + core, 1, 0))
    ids = jnp.stack([core, x, z])
    block = in_vmem(norm_kernel, jax.ShapeDtypeStruct((rows + 16, width), bf), flops=10**9)(
        tokens, norm_gain, documents[None, :]
    )
    swap = [(0, 1), (1, 0)]
    parts = [block, lax.ppermute(block, "c", swap)]
    mine = lax.all_to_all(packed, plane, 0, 0, tiled=True)
    mine = jnp.concatenate([mine, by_head[3]], axis=2).reshape(group * piece, 4 * HEAD_DIM)
    mine, line, at, ids = lax.optimization_barrier((mine, line, at, ids))
    for back in (1, 2, 3):
        got = lax.ppermute(block, "x", [(i, (i + back) % 4) for i in range(4)])
        parts += [got, lax.ppermute(got, "c", swap)]
    over_far = to_all(mine, "zh")
    w_in = to_all(over_far, "zl")
    rows_out = in_vmem(out_rows_kernel, jax.ShapeDtypeStruct((16 * piece, local), bf), flops=10**9)(w_in)
    w_mine = to_all(rows_out, "x")
    w_other = lax.ppermute(w_mine, "c", swap)
    qkv, docs, tail = in_vmem(
        qkv_kernel,
        [
            jax.ShapeDtypeStruct((group * rows, 4 * HEAD_DIM), bf),
            jax.ShapeDtypeStruct((group, rows), jnp.float32),
            jax.ShapeDtypeStruct((rows + 16, 4 * HEAD_DIM), bf),
        ],
        [pltpu.VMEM((width, 4 * HEAD_DIM), bf)],
        grant=24,
    )(ids, *parts, w_in)
    halo = lax.ppermute(tail, ("zh", "zl"), [(i, i + 1) for i in range(15)])
    att = in_vmem(attend_kernel, jax.ShapeDtypeStruct((group, rows // 2, 2 * HEAD_DIM), bf))(
        ids, qkv, halo, docs, line
    )
    att = lax.all_to_all(att, plane, 0, 0, tiled=True)
    partial = in_vmem(
        project_kernel,
        jax.ShapeDtypeStruct((rows, width), bf),
        [pltpu.VMEM((rows, local), bf), pltpu.VMEM((width, local), bf)],
    )(ids, att, w_mine, w_other)
    partial = lax.all_to_all(partial.reshape(n_tp, share, width), "tp", 0, 0, tiled=True)
    mixed = (at + jnp.sum(partial.astype(jnp.float32), axis=0)).astype(bf)
    return to_all(mixed, "tp").reshape(rows, width)


def solution(mesh):
    split = Mesh(mesh.devices.reshape(4, 4, 4, 2, mesh.shape["tp"]), (*SP, "tp"))
    placed = (
        P(SP, None),
        P(SP),
        P(),
        P(None, SP, "tp"),
        P(None, SP, "tp"),
        P(None, SP, "tp"),
        P(None, None, SP),
        P(None, "tp", None),
    )

    def step(*args):
        return body(*args)

    step = jax.shard_map(step, mesh=split, in_specs=placed, out_specs=P(SP, None), check_vma=False)
    return step
```

time: 214 us -> 191 us (0.89)
  waiting for transfers between devices: 67.2 us -> 44 us
  blocking collectives: 103 us -> 80.8 us
  starting transfers between devices: 15.8 us -> 36.5 us
  local copies, waits for them, and re-layouts: 9.2 us -> 12.5 us
    all_to_all x1 -> x2, waiting for transfers between devices: 67.2 us -> 5.84 us  [to_all(): lax.all_to_all(jnp.broadcast_to(x[None], (length, *x.shape)), axis, 0, 0,...]
    ppermute x3 -> x9, waiting for transfers between devices: 0.01 us -> 38 us  [the longest x3 38 us: body(): got = lax.ppermute(block, 'x', [(i, (i + back) % 4) for i in range(4)])]
    all_to_all x3 -> x2, blocking collectives: 79.4 us -> 51.8 us  [to_all(): lax.all_to_all(jnp.broadcast_to(x[None], (length, *x.shape)), axis, 0, 0,...]
    ppermute x3 -> x9, starting transfers between devices: 7.71 us -> 24.7 us  [the longest x3 11.5 us: body(): got = lax.ppermute(block, 'x', [(i, (i + back) % 4) for i in range(4)])]
    all_to_all x1, blocking collectives: 3.95 us -> 9.94 us  [body(): att = lax.all_to_all(att, plane, 0, 0, tiled=True)]
    all_to_all x1 -> x2, starting transfers between devices: 4.84 us -> 7.48 us  [to_all(): lax.all_to_all(jnp.broadcast_to(x[None], (length, *x.shape)), axis, 0, 0,...]
    another operation x0 -> x3, local copies, waits for them, and re-layouts: none -> 2.47 us  [body(): w.reshape(piece, group, HEAD_DIM).swapaxes(0, 1)]
    unnamed x19 -> x15, local copies, waits for them, and re-layouts: 4.5 us -> 4.05 us
  transfers between devices with their start and end apart: 5 -> 12, of which waited for: 1 -> 4; matrix products, arithmetic and copies ran while one was open for 3% -> 3% of each run, Pallas kernels for 4% -> 6%
where the time goes in v4:
time: 191 us; the launch traced here: 190 us
  blocking collectives  80.8 us (42%)
  waiting for transfers between devices  44 us (23%)
  starting transfers between devices  36.5 us (19%)
  Pallas kernels  13 us (7%)
  local copies, waits for them, and re-layouts  12.5 us (7%)
  other arithmetic  2.89 us (2%)
    all_to_all x2, blocking collectives, to_all(): lax.all_to_all(jnp.broadcast_to(x[None], (length, *x.shape)), axis, 0, 0,...  51.8 us
    ppermute x3, waiting for transfers between devices, body(): got = lax.ppermute(block, 'x', [(i, (i + back) % 4) for i in range(4)])  38 us
    all_to_all x1, blocking collectives, body(): lax.all_to_all(partial.reshape(n_tp, share, width), 'tp', 0, 0, tiled=True)  19 us
    pallas_call x5, Pallas kernels, call(): pl.pallas_call(kernel, out_shape=shapes[0] if one else shapes, in_specs=[...  13 us
    ppermute x3, starting transfers between devices, body(): got = lax.ppermute(block, 'x', [(i, (i + back) % 4) for i in range(4)])  11.5 us
    all_to_all x1, blocking collectives, body(): att = lax.all_to_all(att, plane, 0, 0, tiled=True)  9.94 us
    all_to_all x2, starting transfers between devices, to_all(): lax.all_to_all(jnp.broadcast_to(x[None], (length, *x.shape)), axis, 0, 0,...  7.48 us
    ppermute x3, starting transfers between devices, body(): parts += [got, lax.ppermute(got, 'c', swap)]  6.23 us
  transfers between devices with their start and end apart: 12, of which 4 were waited for; matrix products, arithmetic and copies ran while one was open for 3% of the time, Pallas kernels for 6%

profile of v4, /device:TPU:32, one launch (start us, length us, event | category | flops | bytes accessed | tf_op | source)
XLA Modules:
  0.0 189.9 jit_solution(15007761698036205020)
XLA Ops:
  3.2 4.3 %all-to-all-start = ((bf16[8,16,192]{2,1,0:T(8,128)(2,1)}), bf16[8,16,192]{2,1,0:T(8,128)(2,1)S(1)}, u32[]{:S(2)}, u32[]{:S(2)}) async-start(bf16[8,16,192]{2,1,0:T(8,128)(2,1)} %copy.10), calls=%async_computation | async-start | bytes 131072 | tf_op jit(solution)/shard_map/all_to_all | solution.py:187
  10.4 1.8 dynamic-slice_convert_fusion
  13.3 35.8 %all_to_all.35 = bf16[4,128,256]{2,1,0:T(8,128)(2,1)S(1)} all-to-all(bf16[4,128,256]{2,1,0:T(8,128)(2,1)S(1)} %broadcast_in_dim.20), channel_id=1, replica_groups=mesh['zh'=4,'zl'=4,'x'=4,'c'=2,'tp'=4] {'zh'}, dimensions={0} | all-to-all | bytes 524288 | tf_op jit(solution)/shard_map/all_to_all | solution.py:23
  50.2 4.0 %all-to-all-start.2 = ((bf16[4,4,128,256]{3,2,1,0:T(8,128)(2,1)}), bf16[4,4,128,256]{3,2,1,0:T(8,128)(2,1)S(1)}, u32[]{:S(2)}, u32[]{:S(2)}) async-start(bf16[4,4,128,256]{3,2,1,0:T(8,128)(2,1)} %broadcast_in_dim.21), calls=%async_computation.2 | async-start | bytes 2097152 | tf_op jit(solution)/shard_map/all_to_all | solution.py:23
  54.6 3.5 %collective-permute-start.1 = (bf16[272,2048]{1,0:T(8,128)(2,1)S(1)}, bf16[272,2048]{1,0:T(8,128)(2,1)}, u32[]{:S(2)}, u32[]{:S(2)}) collective-permute-start(bf16[272,2048]{1,0:T(8,128)(2,1)S(1)} %shard_map.82.b0), channel_id=1, source_target_pairs={{0,8},{8,16},{16,24},{24,0},{1,9},{9,17},{17,25},{25,1},{2,10},{10... | collective-permute-start | bytes 3342344 | tf_op jit(solution)/shard_map/ppermute | solution.py:191
  58.1 4.6 %collective-permute-start.3 = (bf16[272,2048]{1,0:T(8,128)(2,1)S(1)}, bf16[272,2048]{1,0:T(8,128)(2,1)}, u32[]{:S(2)}, u32[]{:S(2)}) collective-permute-start(bf16[272,2048]{1,0:T(8,128)(2,1)S(1)} %shard_map.82.b0), channel_id=1, source_target_pairs={{0,16},{8,24},{16,0},{24,8},{1,17},{9,25},{17,1},{25,9},{2,18},{10... | collective-permute-start | bytes 3342344 | tf_op jit(solution)/shard_map/ppermute | solution.py:191
  62.7 3.4 %collective-permute-start.5 = (bf16[272,2048]{1,0:T(8,128)(2,1)S(1)}, bf16[272,2048]{1,0:T(8,128)(2,1)}, u32[]{:S(2)}, u32[]{:S(2)}) collective-permute-start(bf16[272,2048]{1,0:T(8,128)(2,1)S(1)} %shard_map.82.b0), channel_id=1, source_target_pairs={{0,24},{8,0},{16,8},{24,16},{1,25},{9,1},{17,9},{25,17},{2,26},{10... | collective-permute-start | bytes 3342344 | tf_op jit(solution)/shard_map/ppermute | solution.py:191
  66.1 1.9 %collective-permute-start = (bf16[272,2048]{1,0:T(8,128)(2,1)S(1)}, bf16[272,2048]{1,0:T(8,128)(2,1)}, u32[]{:S(2)}, u32[]{:S(2)}) collective-permute-start(bf16[272,2048]{1,0:T(8,128)(2,1)S(1)} %shard_map.82.b0), channel_id=1, source_target_pairs={{0,4},{4,0},{1,5},{5,1},{2,6},{6,2},{3,7},{7,3},{8,12},{12,8},{9,1... | collective-permute-start | bytes 3342344 | tf_op jit(solution)/shard_map/ppermute | solution.py:186
  68.0 16.1 %collective-permute-done.1.b1 = bf16[272,2048]{1,0:T(8,128)(2,1)} collective-permute-done((bf16[272,2048]{1,0:T(8,128)(2,1)S(1)}, bf16[272,2048]{1,0:T(8,128)(2,1)}, u32[]{:S(2)}, u32[]{:S(2)}) %collective-permute-start.1) | collective-permute-done | bytes 1114144 | tf_op jit(solution)/shard_map/ppermute | solution.py:191
  84.2 1.9 %collective-permute-start.2 = (bf16[272,2048]{1,0:T(8,128)(2,1)}, bf16[272,2048]{1,0:T(8,128)(2,1)}, u32[]{:S(2)}, u32[]{:S(2)}) collective-permute-start(bf16[272,2048]{1,0:T(8,128)(2,1)} %collective-permute-done.1.b1), channel_id=1, source_target_pairs={{0,4},{4,0},{1,5},{5,1},{2,6},{6,2},{3,7},{7,3},{8,12},{12,8},{9,1... | collective-permute-start | bytes 3342344 | tf_op jit(solution)/shard_map/ppermute | solution.py:192
  86.1 21.9 %collective-permute-done.3.b2 = bf16[272,2048]{1,0:T(8,128)(2,1)} collective-permute-done((bf16[272,2048]{1,0:T(8,128)(2,1)S(1)}, bf16[272,2048]{1,0:T(8,128)(2,1)}, u32[]{:S(2)}, u32[]{:S(2)}) %collective-permute-start.3) | collective-permute-done | bytes 1114144 | tf_op jit(solution)/shard_map/ppermute | solution.py:191
  108.0 1.9 %collective-permute-start.4 = (bf16[272,2048]{1,0:T(8,128)(2,1)}, bf16[272,2048]{1,0:T(8,128)(2,1)}, u32[]{:S(2)}, u32[]{:S(2)}) collective-permute-start(bf16[272,2048]{1,0:T(8,128)(2,1)} %collective-permute-done.3.b2), channel_id=1, source_target_pairs={{0,4},{4,0},{1,5},{5,1},{2,6},{6,2},{3,7},{7,3},{8,12},{12,8},{9,1... | collective-permute-start | bytes 3342344 | tf_op jit(solution)/shard_map/ppermute | solution.py:192
  109.9 2.4 %collective-permute-start.6 = (bf16[272,2048]{1,0:T(8,128)(2,1)}, bf16[272,2048]{1,0:T(8,128)(2,1)}, u32[]{:S(2)}, u32[]{:S(2)}) collective-permute-start(bf16[272,2048]{1,0:T(8,128)(2,1)} %collective-permute-done.5.b3), channel_id=1, source_target_pairs={{0,4},{4,0},{1,5},{5,1},{2,6},{6,2},{3,7},{7,3},{8,12},{12,8},{9,1... | collective-permute-start | bytes 3342344 | tf_op jit(solution)/shard_map/ppermute | solution.py:192
  113.6 3.5 %all-to-all-start.4 = ((bf16[4,256,512]{2,1,0:T(8,128)(2,1)}), bf16[4,256,512]{2,1,0:T(8,128)(2,1)S(1)}, u32[]{:S(2)}, u32[]{:S(2)}) async-start(bf16[4,256,512]{2,1,0:T(8,128)(2,1)} %broadcast_in_dim.22), calls=%async_computation.4 | async-start | bytes 2097152 | tf_op jit(solution)/shard_map/all_to_all | solution.py:23
  117.1 5.7 %shard_map.83 = (bf16[2048,256]{1,0:T(8,128)(2,1)S(1)}, f32[8,256]{1,0:T(8,128)S(1)}, bf16[272,256]{1,0:T(8,128)(2,1)S(1)}) custom-call(s32[3]{0:T(128)S(1)} %pad_add_fusion.ids, bf16[272,2048]{1,0:T(8,128)(2,1)S(1)} %shard_map.82.b0, bf16[272,2048]{1,0:T(8,128)(2,1)} %collective-permute-done.s0, bf16[272,2048]{1,0:T(8,128)(2,1)} %collective-permute-done.1.b1, ...), custom_call_target="tpu_custom_call" | custom-call | flops 20000000000 | bytes 4194304 | tf_op jit(solution)/shard_map/pallas_call | solution.py:133
  123.8 3.1 %collective-permute-start.7 = (bf16[272,256]{1,0:T(8,128)(2,1)S(1)}, bf16[272,256]{1,0:T(8,128)(2,1)S(1)}, u32[]{:S(2)}, u32[]{:S(2)}) collective-permute-start(bf16[272,256]{1,0:T(8,128)(2,1)S(1)} %get-tuple-element.16), channel_id=1, source_target_pairs={{0,32},{32,64},{64,96},{96,128},{128,160},{160,192},{192,224},{224... | collective-permute-start | bytes 417800 | tf_op jit(solution)/shard_map/ppermute | solution.py:208
  126.9 5.8 %all-to-all-done.4.w_mine = bf16[4,256,512]{2,1,0:T(8,128)(2,1)S(1)} async-done(((bf16[4,256,512]{2,1,0:T(8,128)(2,1)}), bf16[4,256,512]{2,1,0:T(8,128)(2,1)S(1)}, u32[]{:S(2)}, u32[]{:S(2)}) %all-to-all-start.4) | async-done | bytes 1048608 | tf_op jit(solution)/shard_map/all_to_all | solution.py:23
  132.8 1.9 %collective-permute-start.8 = (bf16[4,256,512]{2,1,0:T(8,128)(2,1)S(1)}, bf16[4,256,512]{2,1,0:T(8,128)(2,1)S(1)}, u32[]{:S(2)}, u32[]{:S(2)}) collective-permute-start(bf16[4,256,512]{2,1,0:T(8,128)(2,1)S(1)} %all-to-all-done.4.w_mine), channel_id=1, source_target_pairs={{0,4},{4,0},{1,5},{5,1},{2,6},{6,2},{3,7},{7,3},{8,12},{12,8},{9,1... | collective-permute-start | bytes 3145736 | tf_op jit(solution)/shard_map/ppermute | solution.py:197
  134.7 1.2 copy-done.5
  135.9 5.3 %shard_map.84 = bf16[8,128,128]{2,1,0:T(8,128)(2,1)S(1)} custom-call(s32[3]{0:T(128)S(1)} %pad_add_fusion.ids, bf16[2048,256]{1,0:T(8,128)(2,1)S(1)} %copy-done.5, bf16[272,256]{1,0:T(8,128)(2,1)S(1)} %collective-permute-done.7.halo, f32[8,256]{1,0:T(8,128)S(1)} %get-tuple-element.17.docs, f32[1,512]{1,0:T(1,128)S(1)} %maximum_maximum_fusion.line), custom_call_target="tpu_custom_call" | custom-call | flops 20000000000 | bytes 4194304 | tf_op jit(solution)/shard_map/pallas_call | solution.py:133
  141.3 9.9 %all_to_all.36.att = bf16[8,128,128]{2,1,0:T(8,128)(2,1)S(1)} all-to-all(bf16[8,128,128]{2,1,0:T(8,128)(2,1)S(1)} %shard_map.84), channel_id=1, replica_groups=mesh['zh'=4,'zl'=4,'x'=4,'c'=2,'tp'=4] {'x','c'}, dimensions={0} | all-to-all | bytes 524288 | tf_op jit(solution)/shard_map/all_to_all | solution.py:212
  151.2 1.5 shard_map.86
  152.7 19.0 %all_to_all.37 = bf16[4,64,2048]{2,1,0:T(8,128)(2,1)S(1)} all-to-all(bf16[4,64,2048]{2,1,0:T(8,128)(2,1)S(1)} %bitcast.20), channel_id=1, replica_groups=mesh['zh'=4,'zl'=4,'x'=4,'c'=2,'tp'=4] {'tp'}, dimensions={0} | all-to-all | bytes 2097152 | tf_op jit(solution)/shard_map/all_to_all | solution.py:218
  172.9 16.0 %all_to_all.38 = bf16[4,64,2048]{2,1,0:T(8,128)(2,1)S(1)} all-to-all(bf16[4,64,2048]{2,1,0:T(8,128)(2,1)S(1)} %broadcast_in_dim.46), channel_id=1, replica_groups=mesh['zh'=4,'zl'=4,'x'=4,'c'=2,'tp'=4] {'tp'}, dimensions={0} | all-to-all | bytes 2097152 | tf_op jit(solution)/shard_map/all_to_all | solution.py:23
  (50 shorter events, 13.0 us)
Async XLA Ops:
  0.0 12.2 %copy-start = (bf16[1,2048,16]{1,2,0:T(8,128)(2,1)S(1)}, bf16[1,2048,16]{1,2,0:T(8,128)(2,1)}, u32[]{:S(2)}) copy-start(bf16[1,2048,16]{1,2,0:T(8,128)(2,1)} %param.14) | copy-start | bytes 196612
  3.2 9.9 %all-to-all-start = ((bf16[8,16,192]{2,1,0:T(8,128)(2,1)}), bf16[8,16,192]{2,1,0:T(8,128)(2,1)S(1)}, u32[]{:S(2)}, u32[]{:S(2)}) async-start(bf16[8,16,192]{2,1,0:T(8,128)(2,1)} %copy.10), calls=%async_computation | async-start | bytes 131072 | tf_op jit(solution)/shard_map/all_to_all | solution.py:187
  50.2 4.0 %copy-start.1 = (bf16[256,2048]{1,0:T(8,128)(2,1)S(1)}, bf16[256,2048]{1,0:T(8,128)(2,1)}, u32[]{:S(2)}) copy-start(bf16[256,2048]{1,0:T(8,128)(2,1)} %tokens.1) | copy-start | bytes 3145732
  50.2 4.0 %copy-start.2 = (f32[1,2048]{1,0:T(1,128)S(1)}, f32[1,2048]{1,0:T(1,128)}, u32[]{:S(2)}) copy-start(f32[1,2048]{1,0:T(1,128)} %gain.1) | copy-start | bytes 24580
  50.2 4.0 %copy-start.3 = (s32[256]{0:T(256)S(1)}, s32[256]{0:T(256)}, u32[]{:S(2)}) copy-start(s32[256]{0:T(256)} %param.9) | copy-start | bytes 3076
  50.2 62.1 %all-to-all-start.2 = ((bf16[4,4,128,256]{3,2,1,0:T(8,128)(2,1)}), bf16[4,4,128,256]{3,2,1,0:T(8,128)(2,1)S(1)}, u32[]{:S(2)}, u32[]{:S(2)}) async-start(bf16[4,4,128,256]{3,2,1,0:T(8,128)(2,1)} %broadcast_in_dim.21), calls=%async_computation.2 | async-start | bytes 2097152 | tf_op jit(solution)/shard_map/all_to_all | solution.py:23
  54.6 29.6 %collective-permute-start.1 = (bf16[272,2048]{1,0:T(8,128)(2,1)S(1)}, bf16[272,2048]{1,0:T(8,128)(2,1)}, u32[]{:S(2)}, u32[]{:S(2)}) collective-permute-start(bf16[272,2048]{1,0:T(8,128)(2,1)S(1)} %shard_map.82.b0), channel_id=1, source_target_pairs={{0,8},{8,16},{16,24},{24,0},{1,9},{9,17},{17,25},{25,1},{2,10},{10... | collective-permute-start | bytes 3342344 | tf_op jit(solution)/shard_map/ppermute | solution.py:191
  58.1 49.8 %collective-permute-start.3 = (bf16[272,2048]{1,0:T(8,128)(2,1)S(1)}, bf16[272,2048]{1,0:T(8,128)(2,1)}, u32[]{:S(2)}, u32[]{:S(2)}) collective-permute-start(bf16[272,2048]{1,0:T(8,128)(2,1)S(1)} %shard_map.82.b0), channel_id=1, source_target_pairs={{0,16},{8,24},{16,0},{24,8},{1,17},{9,25},{17,1},{25,9},{2,18},{10... | collective-permute-start | bytes 3342344 | tf_op jit(solution)/shard_map/ppermute | solution.py:191
  62.7 47.2 %collective-permute-start.5 = (bf16[272,2048]{1,0:T(8,128)(2,1)S(1)}, bf16[272,2048]{1,0:T(8,128)(2,1)}, u32[]{:S(2)}, u32[]{:S(2)}) collective-permute-start(bf16[272,2048]{1,0:T(8,128)(2,1)S(1)} %shard_map.82.b0), channel_id=1, source_target_pairs={{0,24},{8,0},{16,8},{24,16},{1,25},{9,1},{17,9},{25,17},{2,26},{10... | collective-permute-start | bytes 3342344 | tf_op jit(solution)/shard_map/ppermute | solution.py:191
  66.1 51.0 %collective-permute-start = (bf16[272,2048]{1,0:T(8,128)(2,1)S(1)}, bf16[272,2048]{1,0:T(8,128)(2,1)}, u32[]{:S(2)}, u32[]{:S(2)}) collective-permute-start(bf16[272,2048]{1,0:T(8,128)(2,1)S(1)} %shard_map.82.b0), channel_id=1, source_target_pairs={{0,4},{4,0},{1,5},{5,1},{2,6},{6,2},{3,7},{7,3},{8,12},{12,8},{9,1... | collective-permute-start | bytes 3342344 | tf_op jit(solution)/shard_map/ppermute | solution.py:186
  84.2 32.9 %collective-permute-start.2 = (bf16[272,2048]{1,0:T(8,128)(2,1)}, bf16[272,2048]{1,0:T(8,128)(2,1)}, u32[]{:S(2)}, u32[]{:S(2)}) collective-permute-start(bf16[272,2048]{1,0:T(8,128)(2,1)} %collective-permute-done.1.b1), channel_id=1, source_target_pairs={{0,4},{4,0},{1,5},{5,1},{2,6},{6,2},{3,7},{7,3},{8,12},{12,8},{9,1... | collective-permute-start | bytes 3342344 | tf_op jit(solution)/shard_map/ppermute | solution.py:192
  108.0 9.2 %collective-permute-start.4 = (bf16[272,2048]{1,0:T(8,128)(2,1)}, bf16[272,2048]{1,0:T(8,128)(2,1)}, u32[]{:S(2)}, u32[]{:S(2)}) collective-permute-start(bf16[272,2048]{1,0:T(8,128)(2,1)} %collective-permute-done.3.b2), channel_id=1, source_target_pairs={{0,4},{4,0},{1,5},{5,1},{2,6},{6,2},{3,7},{7,3},{8,12},{12,8},{9,1... | collective-permute-start | bytes 3342344 | tf_op jit(solution)/shard_map/ppermute | solution.py:192
  109.9 7.2 %collective-permute-start.6 = (bf16[272,2048]{1,0:T(8,128)(2,1)}, bf16[272,2048]{1,0:T(8,128)(2,1)}, u32[]{:S(2)}, u32[]{:S(2)}) collective-permute-start(bf16[272,2048]{1,0:T(8,128)(2,1)} %collective-permute-done.5.b3), channel_id=1, source_target_pairs={{0,4},{4,0},{1,5},{5,1},{2,6},{6,2},{3,7},{7,3},{8,12},{12,8},{9,1... | collective-permute-start | bytes 3342344 | tf_op jit(solution)/shard_map/ppermute | solution.py:192
  113.6 19.2 %all-to-all-start.4 = ((bf16[4,256,512]{2,1,0:T(8,128)(2,1)}), bf16[4,256,512]{2,1,0:T(8,128)(2,1)S(1)}, u32[]{:S(2)}, u32[]{:S(2)}) async-start(bf16[4,256,512]{2,1,0:T(8,128)(2,1)} %broadcast_in_dim.22), calls=%async_computation.4 | async-start | bytes 2097152 | tf_op jit(solution)/shard_map/all_to_all | solution.py:23
  122.8 1.0 copy-start.4
  123.8 10.9 %collective-permute-start.7 = (bf16[272,256]{1,0:T(8,128)(2,1)S(1)}, bf16[272,256]{1,0:T(8,128)(2,1)S(1)}, u32[]{:S(2)}, u32[]{:S(2)}) collective-permute-start(bf16[272,256]{1,0:T(8,128)(2,1)S(1)} %get-tuple-element.16), channel_id=1, source_target_pairs={{0,32},{32,64},{64,96},{96,128},{128,160},{160,192},{192,224},{224... | collective-permute-start | bytes 417800 | tf_op jit(solution)/shard_map/ppermute | solution.py:208
  132.8 18.4 %collective-permute-start.8 = (bf16[4,256,512]{2,1,0:T(8,128)(2,1)S(1)}, bf16[4,256,512]{2,1,0:T(8,128)(2,1)S(1)}, u32[]{:S(2)}, u32[]{:S(2)}) collective-permute-start(bf16[4,256,512]{2,1,0:T(8,128)(2,1)S(1)} %all-to-all-done.4.w_mine), channel_id=1, source_target_pairs={{0,4},{4,0},{1,5},{5,1},{2,6},{6,2},{3,7},{7,3},{8,12},{12,8},{9,1... | collective-permute-start | bytes 3145736 | tf_op jit(solution)/shard_map/ppermute | solution.py:197
  134.7 1.2 copy-start.5
  171.7 1.0 copy-start.6

commit v5 on v4

--- a/solution.py
+++ b/solution.py
@@ -21,6 +21,24 @@
 def to_all(x, axis):
     length = lax.axis_size(axis)
     return lax.all_to_all(jnp.broadcast_to(x[None], (length, *x.shape)), axis, 0, 0, tiled=True)
+
+
+def pack_kernel(ids, w_q, w_k, w_v, w_o, heads, rest):
+    n = heads.shape[0]
+    own = w_o[:, pl.ds(pl.multiple_of(ids[3] * n * HEAD_DIM, n * HEAD_DIM), n * HEAD_DIM)]
+    for i in range(n):
+        cols = slice(i * HEAD_DIM, (i + 1) * HEAD_DIM)
+        heads[i] = jnp.concatenate([w_q[:, cols], w_k[:, cols], w_v[:, cols]], axis=1)
+        rest[i] = own[:, cols]
+
+
+def sum_kernel(partial, tokens, out):
+    total = tokens[...].astype(jnp.float32)
+    for i in range(partial.shape[0]):
+        total = total + partial[i].astype(jnp.float32)
+    total = total.astype(jnp.bfloat16)
+    for i in range(out.shape[0]):
+        out[i] = total
 
 
 def norm_kernel(tokens, gain, docs, out):
@@ -171,22 +189,27 @@
     bf = jnp.bfloat16
 
     piece = w_query.shape[1]
-    w_mine = lax.dynamic_slice_in_dim(w_out[0].T, tp * local, local, 1)
-    by_head = [w.reshape(piece, group, HEAD_DIM).swapaxes(0, 1) for w in (w_query[0], w_key[0], w_value[0], w_mine)]
-    packed = jnp.concatenate(by_head[:3], axis=2)
+    ids = jnp.stack([core, x, z, tp])
+    packed, rest = in_vmem(
+        pack_kernel,
+        [
+            jax.ShapeDtypeStruct((group, piece, 3 * HEAD_DIM), bf),
+            jax.ShapeDtypeStruct((group, piece, HEAD_DIM), bf),
+        ],
+        flops=10**8,
+    )(ids, w_query[0], w_key[0], w_value[0], w_out[0].T)
 
     share = rows // n_tp
-    at = lax.dynamic_slice_in_dim(tokens, tp * share, share, 0).astype(jnp.float32)
+    at = lax.dynamic_slice_in_dim(tokens, tp * share, share, 0)
     line = bias_line(lax.dynamic_slice_in_dim(rel_bias[0], x * 2 + core, 1, 0))
-    ids = jnp.stack([core, x, z])
     block = in_vmem(norm_kernel, jax.ShapeDtypeStruct((rows + 16, width), bf), flops=10**9)(
         tokens, norm_gain, documents[None, :]
     )
     swap = [(0, 1), (1, 0)]
     parts = [block, lax.ppermute(block, "c", swap)]
     mine = lax.all_to_all(packed, plane, 0, 0, tiled=True)
-    mine = jnp.concatenate([mine, by_head[3]], axis=2).reshape(group * piece, 4 * HEAD_DIM)
-    mine, line, at, ids = lax.optimization_barrier((mine, line, at, ids))
+    mine = jnp.concatenate([mine, rest], axis=2).reshape(group * piece, 4 * HEAD_DIM)
+    mine, line, at = lax.optimization_barrier((mine, line, at))
     for back in (1, 2, 3):
         got = lax.ppermute(block, "x", [(i, (i + back) % 4) for i in range(4)])
         parts += [got, lax.ppermute(got, "c", swap)]
@@ -216,8 +239,8 @@
         [pltpu.VMEM((rows, local), bf), pltpu.VMEM((width, local), bf)],
     )(ids, att, w_mine, w_other)
     partial = lax.all_to_all(partial.reshape(n_tp, share, width), "tp", 0, 0, tiled=True)
-    mixed = (at + jnp.sum(partial.astype(jnp.float32), axis=0)).astype(bf)
-    return to_all(mixed, "tp").reshape(rows, width)
+    mixed = in_vmem(sum_kernel, jax.ShapeDtypeStruct((n_tp, share, width), bf), flops=10**8)(partial, at)
+    return lax.all_to_all(mixed, "tp", 0, 0, tiled=True).reshape(rows, width)
 
 
 def solution(mesh):

time: 191 us -> 190 us (level)
  other arithmetic: 2.89 us -> 0.85 us
  Pallas kernels: 13 us -> 15 us
    all_to_all x2 -> x1, blocking collectives: 51.8 us -> 35.2 us  [to_all(): lax.all_to_all(jnp.broadcast_to(x[None], (length, *x.shape)), axis, 0, 0,...]
    all_to_all x0 -> x1, blocking collectives: none -> 16 us  [body(): return lax.all_to_all(mixed, 'tp', 0, 0, tiled=True).reshape(rows, width)]
    another operation x3 -> x0, local copies, waits for them, and re-layouts: 2.47 us -> none  [body(): w.reshape(piece, group, HEAD_DIM).swapaxes(0, 1)]
    unnamed x15 -> x21, local copies, waits for them, and re-layouts: 4.05 us -> 6.17 us
    pallas_call x5 -> x7, Pallas kernels: 13 us -> 15 us  [call(): pl.pallas_call(kernel, out_shape=shapes[0] if one else shapes, in_specs=[...]
  transfers between devices with their start and end apart: 12 -> 12, of which waited for: 4 -> 5; matrix products, arithmetic and copies ran while one was open for 3% -> 3% of each run, Pallas kernels for 6% -> 6%
where the time goes in v5:
time: 190 us; the launch traced here: 189 us
  blocking collectives  80.1 us (42%)
  waiting for transfers between devices  45.5 us (24%)
  starting transfers between devices  35.4 us (19%)
  Pallas kernels  15 us (8%)
  local copies, waits for them, and re-layouts  11.6 us (6%)
    ppermute x3, waiting for transfers between devices, body(): got = lax.ppermute(block, 'x', [(i, (i + back) % 4) for i in range(4)])  38.5 us
    all_to_all x1, blocking collectives, to_all(): lax.all_to_all(jnp.broadcast_to(x[None], (length, *x.shape)), axis, 0, 0,...  35.2 us
    all_to_all x1, blocking collectives, body(): lax.all_to_all(partial.reshape(n_tp, share, width), 'tp', 0, 0, tiled=True)  19 us
    all_to_all x1, blocking collectives, body(): return lax.all_to_all(mixed, 'tp', 0, 0, tiled=True).reshape(rows, width)  16 us
    pallas_call x7, Pallas kernels, call(): pl.pallas_call(kernel, out_shape=shapes[0] if one else shapes, in_specs=[...  15 us
    ppermute x3, starting transfers between devices, body(): got = lax.ppermute(block, 'x', [(i, (i + back) % 4) for i in range(4)])  10.6 us
    all_to_all x1, blocking collectives, body(): att = lax.all_to_all(att, plane, 0, 0, tiled=True)  9.91 us
    all_to_all x2, starting transfers between devices, to_all(): lax.all_to_all(jnp.broadcast_to(x[None], (length, *x.shape)), axis, 0, 0,...  7.85 us
  transfers between devices with their start and end apart: 12, of which 5 were waited for; matrix products, arithmetic and copies ran while one was open for 3% of the time, Pallas kernels for 6%

profile of v5, /device:TPU:32, one launch (start us, length us, event | category | flops | bytes accessed | tf_op | source)
XLA Modules:
  0.0 188.7 jit_solution(18129191211178368367)
XLA Ops:
  3.1 1.2 shard_map.83
  4.3 4.3 %all-to-all-start = ((bf16[8,16,192]{2,1,0:T(8,128)(2,1)}), bf16[8,16,192]{2,1,0:T(8,128)(2,1)S(1)}, u32[]{:S(2)}, u32[]{:S(2)}) async-start(bf16[8,16,192]{2,1,0:T(8,128)(2,1)} %get-tuple-element.13), calls=%async_computation | async-start | bytes 131072 | tf_op jit(solution)/shard_map/all_to_all | solution.py:210
  12.5 1.7 all-to-all-done
  14.4 35.2 %all_to_all.35 = bf16[4,128,256]{2,1,0:T(8,128)(2,1)S(1)} all-to-all(bf16[4,128,256]{2,1,0:T(8,128)(2,1)S(1)} %broadcast_in_dim.18), channel_id=1, replica_groups=mesh['zh'=4,'zl'=4,'x'=4,'c'=2,'tp'=4] {'zh'}, dimensions={0} | all-to-all | bytes 524288 | tf_op jit(solution)/shard_map/all_to_all | solution.py:23
  50.6 4.0 %all-to-all-start.2 = ((bf16[4,4,128,256]{3,2,1,0:T(8,128)(2,1)}), bf16[4,4,128,256]{3,2,1,0:T(8,128)(2,1)S(1)}, u32[]{:S(2)}, u32[]{:S(2)}) async-start(bf16[4,4,128,256]{3,2,1,0:T(8,128)(2,1)} %broadcast_in_dim.38), calls=%async_computation.2 | async-start | bytes 2097152 | tf_op jit(solution)/shard_map/all_to_all | solution.py:23
  55.0 2.6 %collective-permute-start.1 = (bf16[272,2048]{1,0:T(8,128)(2,1)S(1)}, bf16[272,2048]{1,0:T(8,128)(2,1)}, u32[]{:S(2)}, u32[]{:S(2)}) collective-permute-start(bf16[272,2048]{1,0:T(8,128)(2,1)S(1)} %shard_map.82.b0), channel_id=1, source_target_pairs={{0,8},{8,16},{16,24},{24,0},{1,9},{9,17},{17,25},{25,1},{2,10},{10... | collective-permute-start | bytes 3342344 | tf_op jit(solution)/shard_map/ppermute | solution.py:214
  57.6 4.6 %collective-permute-start.3 = (bf16[272,2048]{1,0:T(8,128)(2,1)S(1)}, bf16[272,2048]{1,0:T(8,128)(2,1)}, u32[]{:S(2)}, u32[]{:S(2)}) collective-permute-start(bf16[272,2048]{1,0:T(8,128)(2,1)S(1)} %shard_map.82.b0), channel_id=1, source_target_pairs={{0,16},{8,24},{16,0},{24,8},{1,17},{9,25},{17,1},{25,9},{2,18},{10... | collective-permute-start | bytes 3342344 | tf_op jit(solution)/shard_map/ppermute | solution.py:214
  62.2 3.4 %collective-permute-start.5 = (bf16[272,2048]{1,0:T(8,128)(2,1)S(1)}, bf16[272,2048]{1,0:T(8,128)(2,1)}, u32[]{:S(2)}, u32[]{:S(2)}) collective-permute-start(bf16[272,2048]{1,0:T(8,128)(2,1)S(1)} %shard_map.82.b0), channel_id=1, source_target_pairs={{0,24},{8,0},{16,8},{24,16},{1,25},{9,1},{17,9},{25,17},{2,26},{10... | collective-permute-start | bytes 3342344 | tf_op jit(solution)/shard_map/ppermute | solution.py:214
  65.6 1.9 %collective-permute-start = (bf16[272,2048]{1,0:T(8,128)(2,1)S(1)}, bf16[272,2048]{1,0:T(8,128)(2,1)}, u32[]{:S(2)}, u32[]{:S(2)}) collective-permute-start(bf16[272,2048]{1,0:T(8,128)(2,1)S(1)} %shard_map.82.b0), channel_id=1, source_target_pairs={{0,4},{4,0},{1,5},{5,1},{2,6},{6,2},{3,7},{7,3},{8,12},{12,8},{9,1... | collective-permute-start | bytes 3342344 | tf_op jit(solution)/shard_map/ppermute | solution.py:209
  67.5 18.0 %collective-permute-done.1.b1 = bf16[272,2048]{1,0:T(8,128)(2,1)} collective-permute-done((bf16[272,2048]{1,0:T(8,128)(2,1)S(1)}, bf16[272,2048]{1,0:T(8,128)(2,1)}, u32[]{:S(2)}, u32[]{:S(2)}) %collective-permute-start.1) | collective-permute-done | bytes 1114144 | tf_op jit(solution)/shard_map/ppermute | solution.py:214
  85.5 1.9 %collective-permute-start.2 = (bf16[272,2048]{1,0:T(8,128)(2,1)}, bf16[272,2048]{1,0:T(8,128)(2,1)}, u32[]{:S(2)}, u32[]{:S(2)}) collective-permute-start(bf16[272,2048]{1,0:T(8,128)(2,1)} %collective-permute-done.1.b1), channel_id=1, source_target_pairs={{0,4},{4,0},{1,5},{5,1},{2,6},{6,2},{3,7},{7,3},{8,12},{12,8},{9,1... | collective-permute-start | bytes 3342344 | tf_op jit(solution)/shard_map/ppermute | solution.py:215
  87.4 20.0 %collective-permute-done.3.b2 = bf16[272,2048]{1,0:T(8,128)(2,1)} collective-permute-done((bf16[272,2048]{1,0:T(8,128)(2,1)S(1)}, bf16[272,2048]{1,0:T(8,128)(2,1)}, u32[]{:S(2)}, u32[]{:S(2)}) %collective-permute-start.3) | collective-permute-done | bytes 1114144 | tf_op jit(solution)/shard_map/ppermute | solution.py:214
  107.4 1.9 %collective-permute-start.4 = (bf16[272,2048]{1,0:T(8,128)(2,1)}, bf16[272,2048]{1,0:T(8,128)(2,1)}, u32[]{:S(2)}, u32[]{:S(2)}) collective-permute-start(bf16[272,2048]{1,0:T(8,128)(2,1)} %collective-permute-done.3.b2), channel_id=1, source_target_pairs={{0,4},{4,0},{1,5},{5,1},{2,6},{6,2},{3,7},{7,3},{8,12},{12,8},{9,1... | collective-permute-start | bytes 3342344 | tf_op jit(solution)/shard_map/ppermute | solution.py:215
  109.8 1.9 %collective-permute-start.6 = (bf16[272,2048]{1,0:T(8,128)(2,1)}, bf16[272,2048]{1,0:T(8,128)(2,1)}, u32[]{:S(2)}, u32[]{:S(2)}) collective-permute-start(bf16[272,2048]{1,0:T(8,128)(2,1)} %collective-permute-done.5.b3), channel_id=1, source_target_pairs={{0,4},{4,0},{1,5},{5,1},{2,6},{6,2},{3,7},{7,3},{8,12},{12,8},{9,1... | collective-permute-start | bytes 3342344 | tf_op jit(solution)/shard_map/ppermute | solution.py:215
  113.1 3.9 %all-to-all-start.4 = ((bf16[4,256,512]{2,1,0:T(8,128)(2,1)}), bf16[4,256,512]{2,1,0:T(8,128)(2,1)S(1)}, u32[]{:S(2)}, u32[]{:S(2)}) async-start(bf16[4,256,512]{2,1,0:T(8,128)(2,1)} %broadcast_in_dim.39), calls=%async_computation.4 | async-start | bytes 2097152 | tf_op jit(solution)/shard_map/all_to_all | solution.py:23
  117.0 6.3 %shard_map.84 = (bf16[2048,256]{1,0:T(8,128)(2,1)S(1)}, f32[8,256]{1,0:T(8,128)S(1)}, bf16[272,256]{1,0:T(8,128)(2,1)}) custom-call(s32[4]{0:T(128)S(1)} %pad_add_fusion.ids, bf16[272,2048]{1,0:T(8,128)(2,1)S(1)} %shard_map.82.b0, bf16[272,2048]{1,0:T(8,128)(2,1)} %collective-permute-done.s0, bf16[272,2048]{1,0:T(8,128)(2,1)} %collective-permute-done.1.b1, ...), custom_call_target="tpu_custom_call" | custom-call | flops 20000000000 | bytes 4194304 | tf_op jit(solution)/shard_map/pallas_call | solution.py:151
  124.2 3.1 %collective-permute-start.7 = (bf16[272,256]{1,0:T(8,128)(2,1)}, bf16[272,256]{1,0:T(8,128)(2,1)S(1)}, u32[]{:S(2)}, u32[]{:S(2)}) collective-permute-start(bf16[272,256]{1,0:T(8,128)(2,1)} %get-tuple-element.17), channel_id=1, source_target_pairs={{0,32},{32,64},{64,96},{96,128},{128,160},{160,192},{192,224},{224... | collective-permute-start | bytes 417800 | tf_op jit(solution)/shard_map/ppermute | solution.py:231
  127.4 5.3 %all-to-all-done.4.w_mine = bf16[4,256,512]{2,1,0:T(8,128)(2,1)S(1)} async-done(((bf16[4,256,512]{2,1,0:T(8,128)(2,1)}), bf16[4,256,512]{2,1,0:T(8,128)(2,1)S(1)}, u32[]{:S(2)}, u32[]{:S(2)}) %all-to-all-start.4) | async-done | bytes 1048608 | tf_op jit(solution)/shard_map/all_to_all | solution.py:23
  132.7 1.9 %collective-permute-start.8 = (bf16[4,256,512]{2,1,0:T(8,128)(2,1)S(1)}, bf16[4,256,512]{2,1,0:T(8,128)(2,1)S(1)}, u32[]{:S(2)}, u32[]{:S(2)}) collective-permute-start(bf16[4,256,512]{2,1,0:T(8,128)(2,1)S(1)} %all-to-all-done.4.w_mine), channel_id=1, source_target_pairs={{0,4},{4,0},{1,5},{5,1},{2,6},{6,2},{3,7},{7,3},{8,12},{12,8},{9,1... | collective-permute-start | bytes 3145736 | tf_op jit(solution)/shard_map/ppermute | solution.py:220
  135.8 5.3 %shard_map.85 = bf16[8,128,128]{2,1,0:T(8,128)(2,1)S(1)} custom-call(s32[4]{0:T(128)S(1)} %pad_add_fusion.ids, bf16[2048,256]{1,0:T(8,128)(2,1)S(1)} %copy-done.9, bf16[272,256]{1,0:T(8,128)(2,1)S(1)} %collective-permute-done.7.halo, f32[8,256]{1,0:T(8,128)S(1)} %get-tuple-element.18.docs, f32[1,512]{1,0:T(1,128)S(1)} %maximum_maximum_fusion.line), custom_call_target="tpu_custom_call" | custom-call | flops 20000000000 | bytes 4194304 | tf_op jit(solution)/shard_map/pallas_call | solution.py:151
  141.2 9.9 %all_to_all.36.att = bf16[8,128,128]{2,1,0:T(8,128)(2,1)S(1)} all-to-all(bf16[8,128,128]{2,1,0:T(8,128)(2,1)S(1)} %shard_map.85), channel_id=1, replica_groups=mesh['zh'=4,'zl'=4,'x'=4,'c'=2,'tp'=4] {'x','c'}, dimensions={0} | all-to-all | bytes 524288 | tf_op jit(solution)/shard_map/all_to_all | solution.py:235
  151.1 1.5 shard_map.87
  152.6 19.0 %all_to_all.37.partial = bf16[4,64,2048]{2,1,0:T(8,128)(2,1)S(1)} all-to-all(bf16[4,64,2048]{2,1,0:T(8,128)(2,1)S(1)} %bitcast.19), channel_id=1, replica_groups=mesh['zh'=4,'zl'=4,'x'=4,'c'=2,'tp'=4] {'tp'}, dimensions={0} | all-to-all | bytes 2097152 | tf_op jit(solution)/shard_map/all_to_all | solution.py:241
  171.7 16.0 %all_to_all.38 = bf16[4,64,2048]{2,1,0:T(8,128)(2,1)S(1)} all-to-all(bf16[4,64,2048]{2,1,0:T(8,128)(2,1)S(1)} %shard_map.88), channel_id=1, replica_groups=mesh['zh'=4,'zl'=4,'x'=4,'c'=2,'tp'=4] {'tp'}, dimensions={0} | all-to-all | bytes 2097152 | tf_op jit(solution)/shard_map/all_to_all | solution.py:243
  (47 shorter events, 13.6 us)
Async XLA Ops:
  0.0 8.6 %copy-start = (f32[1,8,257]{2,1,0:T(8,128)S(1)}, f32[1,8,257]{2,1,0:T(8,128)}, u32[]{:S(2)}) copy-start(f32[1,8,257]{2,1,0:T(8,128)} %param.15) | copy-start | bytes 24676
  0.1 0.8 copy-start.2
  0.9 0.7 copy-start.3
  1.6 0.7 copy-start.4
  2.4 0.7 copy-start.5
  4.3 9.9 %all-to-all-start = ((bf16[8,16,192]{2,1,0:T(8,128)(2,1)}), bf16[8,16,192]{2,1,0:T(8,128)(2,1)S(1)}, u32[]{:S(2)}, u32[]{:S(2)}) async-start(bf16[8,16,192]{2,1,0:T(8,128)(2,1)} %get-tuple-element.13), calls=%async_computation | async-start | bytes 131072 | tf_op jit(solution)/shard_map/all_to_all | solution.py:210
  50.6 4.0 %copy-start.1 = (bf16[256,2048]{1,0:T(8,128)(2,1)S(1)}, bf16[256,2048]{1,0:T(8,128)(2,1)}, u32[]{:S(2)}) copy-start(bf16[256,2048]{1,0:T(8,128)(2,1)} %tokens.1) | copy-start | bytes 3145732
  50.6 4.0 %copy-start.6 = (f32[1,2048]{1,0:T(1,128)S(1)}, f32[1,2048]{1,0:T(1,128)}, u32[]{:S(2)}) copy-start(f32[1,2048]{1,0:T(1,128)} %gain.1) | copy-start | bytes 24580
  50.6 4.0 %copy-start.7 = (s32[256]{0:T(256)S(1)}, s32[256]{0:T(256)}, u32[]{:S(2)}) copy-start(s32[256]{0:T(256)} %param.9) | copy-start | bytes 3076
  50.6 61.2 %all-to-all-start.2 = ((bf16[4,4,128,256]{3,2,1,0:T(8,128)(2,1)}), bf16[4,4,128,256]{3,2,1,0:T(8,128)(2,1)S(1)}, u32[]{:S(2)}, u32[]{:S(2)}) async-start(bf16[4,4,128,256]{3,2,1,0:T(8,128)(2,1)} %broadcast_in_dim.38), calls=%async_computation.2 | async-start | bytes 2097152 | tf_op jit(solution)/shard_map/all_to_all | solution.py:23
  55.0 30.5 %collective-permute-start.1 = (bf16[272,2048]{1,0:T(8,128)(2,1)S(1)}, bf16[272,2048]{1,0:T(8,128)(2,1)}, u32[]{:S(2)}, u32[]{:S(2)}) collective-permute-start(bf16[272,2048]{1,0:T(8,128)(2,1)S(1)} %shard_map.82.b0), channel_id=1, source_target_pairs={{0,8},{8,16},{16,24},{24,0},{1,9},{9,17},{17,25},{25,1},{2,10},{10... | collective-permute-start | bytes 3342344 | tf_op jit(solution)/shard_map/ppermute | solution.py:214
  57.6 49.8 %collective-permute-start.3 = (bf16[272,2048]{1,0:T(8,128)(2,1)S(1)}, bf16[272,2048]{1,0:T(8,128)(2,1)}, u32[]{:S(2)}, u32[]{:S(2)}) collective-permute-start(bf16[272,2048]{1,0:T(8,128)(2,1)S(1)} %shard_map.82.b0), channel_id=1, source_target_pairs={{0,16},{8,24},{16,0},{24,8},{1,17},{9,25},{17,1},{25,9},{2,18},{10... | collective-permute-start | bytes 3342344 | tf_op jit(solution)/shard_map/ppermute | solution.py:214
  62.2 47.6 %collective-permute-start.5 = (bf16[272,2048]{1,0:T(8,128)(2,1)S(1)}, bf16[272,2048]{1,0:T(8,128)(2,1)}, u32[]{:S(2)}, u32[]{:S(2)}) collective-permute-start(bf16[272,2048]{1,0:T(8,128)(2,1)S(1)} %shard_map.82.b0), channel_id=1, source_target_pairs={{0,24},{8,0},{16,8},{24,16},{1,25},{9,1},{17,9},{25,17},{2,26},{10... | collective-permute-start | bytes 3342344 | tf_op jit(solution)/shard_map/ppermute | solution.py:214
  65.6 51.4 %collective-permute-start = (bf16[272,2048]{1,0:T(8,128)(2,1)S(1)}, bf16[272,2048]{1,0:T(8,128)(2,1)}, u32[]{:S(2)}, u32[]{:S(2)}) collective-permute-start(bf16[272,2048]{1,0:T(8,128)(2,1)S(1)} %shard_map.82.b0), channel_id=1, source_target_pairs={{0,4},{4,0},{1,5},{5,1},{2,6},{6,2},{3,7},{7,3},{8,12},{12,8},{9,1... | collective-permute-start | bytes 3342344 | tf_op jit(solution)/shard_map/ppermute | solution.py:209
  85.5 31.4 %collective-permute-start.2 = (bf16[272,2048]{1,0:T(8,128)(2,1)}, bf16[272,2048]{1,0:T(8,128)(2,1)}, u32[]{:S(2)}, u32[]{:S(2)}) collective-permute-start(bf16[272,2048]{1,0:T(8,128)(2,1)} %collective-permute-done.1.b1), channel_id=1, source_target_pairs={{0,4},{4,0},{1,5},{5,1},{2,6},{6,2},{3,7},{7,3},{8,12},{12,8},{9,1... | collective-permute-start | bytes 3342344 | tf_op jit(solution)/shard_map/ppermute | solution.py:215
  107.4 9.5 %collective-permute-start.4 = (bf16[272,2048]{1,0:T(8,128)(2,1)}, bf16[272,2048]{1,0:T(8,128)(2,1)}, u32[]{:S(2)}, u32[]{:S(2)}) collective-permute-start(bf16[272,2048]{1,0:T(8,128)(2,1)} %collective-permute-done.3.b2), channel_id=1, source_target_pairs={{0,4},{4,0},{1,5},{5,1},{2,6},{6,2},{3,7},{7,3},{8,12},{12,8},{9,1... | collective-permute-start | bytes 3342344 | tf_op jit(solution)/shard_map/ppermute | solution.py:215
  109.8 7.1 %collective-permute-start.6 = (bf16[272,2048]{1,0:T(8,128)(2,1)}, bf16[272,2048]{1,0:T(8,128)(2,1)}, u32[]{:S(2)}, u32[]{:S(2)}) collective-permute-start(bf16[272,2048]{1,0:T(8,128)(2,1)} %collective-permute-done.5.b3), channel_id=1, source_target_pairs={{0,4},{4,0},{1,5},{5,1},{2,6},{6,2},{3,7},{7,3},{8,12},{12,8},{9,1... | collective-permute-start | bytes 3342344 | tf_op jit(solution)/shard_map/ppermute | solution.py:215
  113.1 19.6 %all-to-all-start.4 = ((bf16[4,256,512]{2,1,0:T(8,128)(2,1)}), bf16[4,256,512]{2,1,0:T(8,128)(2,1)S(1)}, u32[]{:S(2)}, u32[]{:S(2)}) async-start(bf16[4,256,512]{2,1,0:T(8,128)(2,1)} %broadcast_in_dim.39), calls=%async_computation.4 | async-start | bytes 2097152 | tf_op jit(solution)/shard_map/all_to_all | solution.py:23
  123.3 1.0 copy-start.8
  124.2 10.4 %collective-permute-start.7 = (bf16[272,256]{1,0:T(8,128)(2,1)}, bf16[272,256]{1,0:T(8,128)(2,1)S(1)}, u32[]{:S(2)}, u32[]{:S(2)}) collective-permute-start(bf16[272,256]{1,0:T(8,128)(2,1)} %get-tuple-element.17), channel_id=1, source_target_pairs={{0,32},{32,64},{64,96},{96,128},{128,160},{160,192},{192,224},{224... | collective-permute-start | bytes 417800 | tf_op jit(solution)/shard_map/ppermute | solution.py:231
  132.7 18.4 %collective-permute-start.8 = (bf16[4,256,512]{2,1,0:T(8,128)(2,1)S(1)}, bf16[4,256,512]{2,1,0:T(8,128)(2,1)S(1)}, u32[]{:S(2)}, u32[]{:S(2)}) collective-permute-start(bf16[4,256,512]{2,1,0:T(8,128)(2,1)S(1)} %all-to-all-done.4.w_mine), channel_id=1, source_target_pairs={{0,4},{4,0},{1,5},{5,1},{2,6},{6,2},{3,7},{7,3},{8,12},{12,8},{9,1... | collective-permute-start | bytes 3145736 | tf_op jit(solution)/shard_map/ppermute | solution.py:220
  134.6 1.2 copy-start.9

commit v6 on v5

--- a/solution.py
+++ b/solution.py
@@ -14,7 +14,7 @@
 REACH = LEFT * SEG
 Q_BLOCK = 2 * SEG
 K_BLOCK = Q_BLOCK + REACH
-SP = ("zh", "zl", "x", "c")
+SP = ("z", "x", "c")
 NEG = -1e30
 
 
@@ -51,32 +51,29 @@
     out[rows:, rows:] = jnp.zeros((extra, out.shape[1] - rows), jnp.bfloat16)
 
 
-def qkv_kernel(ids, b0, s0, b1, s1, b2, s2, b3, s3, w_in, qkv, docs, tail, w_all):
+def qkv_kernel(ids, b0, s0, b1, s1, b2, s2, b3, s3, w_in, qkv, docs, tail):
     rows = qkv.shape[0] // 8
-    n_l, n_h, lanes = w_in.shape[:3]
-    for h in range(n_h):
-        for l in range(n_l):
-            at = (h * n_l + l) * lanes
-            w_all[at : at + lanes, :] = w_in[l, h]
+    weights = w_in[...].reshape(-1, w_in.shape[2])
     core, x = ids[0], ids[1]
     for back, pair in enumerate(((b0, s0), (b1, s1), (b2, s2), (b3, s3))):
         for c, part in zip((core, 1 - core), pair):
             at = ((x + 4 - back) & 3) * 2 + c
-            total = jnp.dot(part[:rows, :], w_all[...], preferred_element_type=jnp.float32)
+            total = jnp.dot(part[:rows, :], weights, preferred_element_type=jnp.float32)
             qkv[pl.ds(pl.multiple_of(at * rows, rows), rows), :] = total.astype(jnp.bfloat16)
             docs[pl.ds(at, 1), :] = part[rows : rows + 16, :rows].astype(jnp.float32)[0:1]
     tail[:rows, :] = qkv[7 * rows :, :]
     tail[rows:, :] = jnp.broadcast_to(docs[7:8, :], (16, rows)).astype(jnp.bfloat16)
 
 
-def attend_kernel(ids, qkv, halo, docs, line, out):
+def attend(blocks, ids, qkv, halo, docs, line, out):
     rows = docs.shape[1]
     flat = jnp.broadcast_to(line[...], (Q_BLOCK, line.shape[1]))
     bias = pltpu.roll(flat, 0, 1, stride=1, stride_axis=0)[:, :K_BLOCK]
     q_seg = lax.broadcasted_iota(jnp.int32, (Q_BLOCK, K_BLOCK), 0) // SEG
     k_seg = lax.broadcasted_iota(jnp.int32, (Q_BLOCK, K_BLOCK), 1) // SEG
     bias = jnp.where((k_seg >= q_seg) & (k_seg <= q_seg + LEFT), bias, NEG)
-    prior = jnp.where(ids[2] > 0, halo[rows : rows + 16, :].astype(jnp.float32)[0:1], -1.0)
+    if halo is not None:
+        prior = jnp.where(ids[2] > 0, halo[rows : rows + 16, :].astype(jnp.float32)[0:1], -1.0)
 
     def doc_part(b):
         if b < 0:
@@ -94,7 +91,7 @@
             return qkv[(b - 2) * Q_BLOCK : (b + 1) * Q_BLOCK, cols]
         return jnp.concatenate([row_part(i, cols) for i in range(b - 2, b + 1)], axis=0)
 
-    for b in range(qkv.shape[0] // Q_BLOCK):
+    for b in blocks:
         across = jnp.broadcast_to(doc_part(b), (Q_BLOCK, Q_BLOCK)).T
         same = jnp.concatenate([across == doc_part(i) for i in range(b - 2, b + 1)], axis=1)
         scores = lax.dot_general(
@@ -116,14 +113,21 @@
         out[b // 2, :, lane : lane + HEAD_DIM] = (mixed / total).astype(jnp.bfloat16)
 
 
+def later_kernel(qkv, docs, line, out):
+    out[0] = jnp.zeros(out.shape[1:], out.dtype)
+    attend(range(2, qkv.shape[0] // Q_BLOCK), None, qkv, None, docs, line, out)
+
+
+def early_kernel(ids, qkv, halo, docs, line, later, out):
+    out[1:] = later[1:]
+    attend(range(2), ids, qkv, halo, docs, line, out)
+
+
 def out_rows_kernel(w_in, out):
-    n_l, n_h = w_in.shape[:2]
-    for h in range(n_h):
-        for l in range(n_l):
-            at = (h * n_l + l) * 16
-            out[at : at + 16, :] = jnp.concatenate(
-                [w_in[l, h, 16 * j : 16 * j + 16, 3 * HEAD_DIM :] for j in range(8)], axis=1
-            )
+    for z in range(w_in.shape[0]):
+        out[16 * z : 16 * z + 16, :] = jnp.concatenate(
+            [w_in[z, 16 * j : 16 * j + 16, 3 * HEAD_DIM :] for j in range(8)], axis=1
+        )
 
 
 def project_kernel(ids, att, w_mine, w_other, out, lhs, rhs):
@@ -181,7 +185,7 @@
     local = w_query.shape[2]
     core = lax.axis_index("c")
     x = lax.axis_index("x")
-    z = lax.axis_index(("zh", "zl"))
+    z = lax.axis_index("z")
     tp = lax.axis_index("tp")
     n_tp = lax.axis_size("tp")
     plane = ("x", "c")
@@ -209,12 +213,11 @@
     parts = [block, lax.ppermute(block, "c", swap)]
     mine = lax.all_to_all(packed, plane, 0, 0, tiled=True)
     mine = jnp.concatenate([mine, rest], axis=2).reshape(group * piece, 4 * HEAD_DIM)
-    mine, line, at = lax.optimization_barrier((mine, line, at))
     for back in (1, 2, 3):
         got = lax.ppermute(block, "x", [(i, (i + back) % 4) for i in range(4)])
         parts += [got, lax.ppermute(got, "c", swap)]
-    over_far = to_all(mine, "zh")
-    w_in = to_all(over_far, "zl")
+    w_in = to_all(mine, "z")
+    w_in, line, at = lax.optimization_barrier((w_in, line, at))
     rows_out = in_vmem(out_rows_kernel, jax.ShapeDtypeStruct((16 * piece, local), bf), flops=10**9)(w_in)
     w_mine = to_all(rows_out, "x")
     w_other = lax.ppermute(w_mine, "c", swap)
@@ -225,13 +228,12 @@
             jax.ShapeDtypeStruct((group, rows), jnp.float32),
             jax.ShapeDtypeStruct((rows + 16, 4 * HEAD_DIM), bf),
         ],
-        [pltpu.VMEM((width, 4 * HEAD_DIM), bf)],
         grant=24,
     )(ids, *parts, w_in)
-    halo = lax.ppermute(tail, ("zh", "zl"), [(i, i + 1) for i in range(15)])
-    att = in_vmem(attend_kernel, jax.ShapeDtypeStruct((group, rows // 2, 2 * HEAD_DIM), bf))(
-        ids, qkv, halo, docs, line
-    )
+    halo = lax.ppermute(tail, "z", [(i, i + 1) for i in range(15)])
+    att_shape = jax.ShapeDtypeStruct((group, rows // 2, 2 * HEAD_DIM), bf)
+    att = in_vmem(later_kernel, att_shape)(qkv, docs, line)
+    att = in_vmem(early_kernel, att_shape, flops=10**9)(ids, qkv, halo, docs, line, att)
     att = lax.all_to_all(att, plane, 0, 0, tiled=True)
     partial = in_vmem(
         project_kernel,
@@ -244,7 +246,7 @@
 
 
 def solution(mesh):
-    split = Mesh(mesh.devices.reshape(4, 4, 4, 2, mesh.shape["tp"]), (*SP, "tp"))
+    split = Mesh(mesh.devices.reshape(16, 4, 2, mesh.shape["tp"]), (*SP, "tp"))
     placed = (
         P(SP, None),
         P(SP),

time: 190 us -> 170 us (0.89)
  blocking collectives: 80.1 us -> 54.6 us
  starting transfers between devices: 35.4 us -> 41.6 us
    all_to_all x1, blocking collectives: 35.2 us -> 9.72 us  [body(): mine = lax.all_to_all(packed, plane, 0, 0, tiled=True)]
    all_to_all x2, starting transfers between devices: 7.85 us -> 18.9 us  [to_all(): lax.all_to_all(jnp.broadcast_to(x[None], (length, *x.shape)), axis, 0, 0,...]
    all_to_all x1 -> x0, starting transfers between devices: 4.3 us -> none  [body(): mine = lax.all_to_all(packed, plane, 0, 0, tiled=True)]
    ppermute x3, waiting for transfers between devices: 38.5 us -> 41.4 us  [body(): got = lax.ppermute(block, 'x', [(i, (i + back) % 4) for i in range(4)])]
    pallas_call x7 -> x8, Pallas kernels: 15 us -> 14.7 us  [call(): pl.pallas_call(kernel, out_shape=shapes[0] if one else shapes, in_specs=[...]
  transfers between devices with their start and end apart: 12 -> 11, of which waited for: 5 -> 2; matrix products, arithmetic and copies ran while one was open for 3% -> 2% of each run, Pallas kernels for 6% -> 7%
where the time goes in v6:
time: 170 us; the launch traced here: 169 us
  blocking collectives  54.6 us (32%)
  waiting for transfers between devices  46.8 us (28%)
  starting transfers between devices  41.6 us (24%)
  Pallas kernels  14.7 us (9%)
  local copies, waits for them, and re-layouts  10.4 us (6%)
    ppermute x3, waiting for transfers between devices, body(): got = lax.ppermute(block, 'x', [(i, (i + back) % 4) for i in range(4)])  41.4 us
    all_to_all x1, blocking collectives, body(): lax.all_to_all(partial.reshape(n_tp, share, width), 'tp', 0, 0, tiled=True)  19 us
    all_to_all x2, starting transfers between devices, to_all(): lax.all_to_all(jnp.broadcast_to(x[None], (length, *x.shape)), axis, 0, 0,...  18.9 us
    all_to_all x1, blocking collectives, body(): return lax.all_to_all(mixed, 'tp', 0, 0, tiled=True).reshape(rows, width)  16 us
    pallas_call x8, Pallas kernels, call(): pl.pallas_call(kernel, out_shape=shapes[0] if one else shapes, in_specs=[...  14.7 us
    all_to_all x1, blocking collectives, body(): att = lax.all_to_all(att, plane, 0, 0, tiled=True)  9.91 us
    all_to_all x1, blocking collectives, body(): mine = lax.all_to_all(packed, plane, 0, 0, tiled=True)  9.72 us
    ppermute x3, starting transfers between devices, body(): got = lax.ppermute(block, 'x', [(i, (i + back) % 4) for i in range(4)])  9.35 us
  transfers between devices with their start and end apart: 11, of which 2 were waited for; matrix products, arithmetic and copies ran while one was open for 2% of the time, Pallas kernels for 7%

profile of v6, /device:TPU:32, one launch (start us, length us, event | category | flops | bytes accessed | tf_op | source)
XLA Modules:
  0.0 169.1 jit_solution(10432896342268495352)
XLA Ops:
  3.7 9.7 %all_to_all.30 = bf16[8,16,192]{2,1,0:T(8,128)(2,1)S(1)} all-to-all(bf16[8,16,192]{2,1,0:T(8,128)(2,1)S(1)} %get-tuple-element.13), channel_id=1, replica_groups=mesh['z'=16,'x'=4,'c'=2,'tp'=4] {'x','c'}, dimensions={0} | all-to-all | bytes 98304 | tf_op jit(solution)/shard_map/all_to_all | solution.py:214
  13.5 1.1 broadcast_in_dim.30
  14.6 15.3 %all-to-all-start.1 = ((bf16[16,128,256]{2,1,0:T(8,128)(2,1)}), bf16[16,128,256]{2,1,0:T(8,128)(2,1)S(1)}, u32[]{:S(2)}, u32[]{:S(2)}) async-start(bf16[16,128,256]{2,1,0:T(8,128)(2,1)} %broadcast_in_dim.30), calls=%async_computation.1 | async-start | bytes 2097152 | tf_op jit(solution)/shard_map/all_to_all | solution.py:23
  30.4 2.5 %collective-permute-start.1 = (bf16[272,2048]{1,0:T(8,128)(2,1)S(1)}, bf16[272,2048]{1,0:T(8,128)(2,1)}, u32[]{:S(2)}, u32[]{:S(2)}) collective-permute-start(bf16[272,2048]{1,0:T(8,128)(2,1)S(1)} %shard_map.82.b0), channel_id=1, source_target_pairs={{0,8},{8,16},{16,24},{24,0},{1,9},{9,17},{17,25},{25,1},{2,10},{10... | collective-permute-start | bytes 3342344 | tf_op jit(solution)/shard_map/ppermute | solution.py:217
  32.9 4.0 %collective-permute-start.3 = (bf16[272,2048]{1,0:T(8,128)(2,1)S(1)}, bf16[272,2048]{1,0:T(8,128)(2,1)}, u32[]{:S(2)}, u32[]{:S(2)}) collective-permute-start(bf16[272,2048]{1,0:T(8,128)(2,1)S(1)} %shard_map.82.b0), channel_id=1, source_target_pairs={{0,16},{8,24},{16,0},{24,8},{1,17},{9,25},{17,1},{25,9},{2,18},{10... | collective-permute-start | bytes 3342344 | tf_op jit(solution)/shard_map/ppermute | solution.py:217
  36.8 2.9 %collective-permute-start.5 = (bf16[272,2048]{1,0:T(8,128)(2,1)S(1)}, bf16[272,2048]{1,0:T(8,128)(2,1)}, u32[]{:S(2)}, u32[]{:S(2)}) collective-permute-start(bf16[272,2048]{1,0:T(8,128)(2,1)S(1)} %shard_map.82.b0), channel_id=1, source_target_pairs={{0,24},{8,0},{16,8},{24,16},{1,25},{9,1},{17,9},{25,17},{2,26},{10... | collective-permute-start | bytes 3342344 | tf_op jit(solution)/shard_map/ppermute | solution.py:217
  39.7 1.9 %collective-permute-start = (bf16[272,2048]{1,0:T(8,128)(2,1)S(1)}, bf16[272,2048]{1,0:T(8,128)(2,1)}, u32[]{:S(2)}, u32[]{:S(2)}) collective-permute-start(bf16[272,2048]{1,0:T(8,128)(2,1)S(1)} %shard_map.82.b0), channel_id=1, source_target_pairs={{0,4},{4,0},{1,5},{5,1},{2,6},{6,2},{3,7},{7,3},{8,12},{12,8},{9,1... | collective-permute-start | bytes 3342344 | tf_op jit(solution)/shard_map/ppermute | solution.py:213
  41.7 41.4 %collective-permute-done.1.b1 = bf16[272,2048]{1,0:T(8,128)(2,1)} collective-permute-done((bf16[272,2048]{1,0:T(8,128)(2,1)S(1)}, bf16[272,2048]{1,0:T(8,128)(2,1)}, u32[]{:S(2)}, u32[]{:S(2)}) %collective-permute-start.1) | collective-permute-done | bytes 1114144 | tf_op jit(solution)/shard_map/ppermute | solution.py:217
  83.1 1.9 %collective-permute-start.2 = (bf16[272,2048]{1,0:T(8,128)(2,1)}, bf16[272,2048]{1,0:T(8,128)(2,1)}, u32[]{:S(2)}, u32[]{:S(2)}) collective-permute-start(bf16[272,2048]{1,0:T(8,128)(2,1)} %collective-permute-done.1.b1), channel_id=1, source_target_pairs={{0,4},{4,0},{1,5},{5,1},{2,6},{6,2},{3,7},{7,3},{8,12},{12,8},{9,1... | collective-permute-start | bytes 3342344 | tf_op jit(solution)/shard_map/ppermute | solution.py:218
  85.0 2.4 %collective-permute-start.4 = (bf16[272,2048]{1,0:T(8,128)(2,1)}, bf16[272,2048]{1,0:T(8,128)(2,1)}, u32[]{:S(2)}, u32[]{:S(2)}) collective-permute-start(bf16[272,2048]{1,0:T(8,128)(2,1)} %collective-permute-done.3.b2), channel_id=1, source_target_pairs={{0,4},{4,0},{1,5},{5,1},{2,6},{6,2},{3,7},{7,3},{8,12},{12,8},{9,1... | collective-permute-start | bytes 3342344 | tf_op jit(solution)/shard_map/ppermute | solution.py:218
  87.5 1.9 %collective-permute-start.6 = (bf16[272,2048]{1,0:T(8,128)(2,1)}, bf16[272,2048]{1,0:T(8,128)(2,1)}, u32[]{:S(2)}, u32[]{:S(2)}) collective-permute-start(bf16[272,2048]{1,0:T(8,128)(2,1)} %collective-permute-done.5.b3), channel_id=1, source_target_pairs={{0,4},{4,0},{1,5},{5,1},{2,6},{6,2},{3,7},{7,3},{8,12},{12,8},{9,1... | collective-permute-start | bytes 3342344 | tf_op jit(solution)/shard_map/ppermute | solution.py:218
  92.2 1.1 broadcast_in_dim.34
  93.3 3.5 %all-to-all-start.3 = ((bf16[4,256,512]{2,1,0:T(8,128)(2,1)}), bf16[4,256,512]{2,1,0:T(8,128)(2,1)S(1)}, u32[]{:S(2)}, u32[]{:S(2)}) async-start(bf16[4,256,512]{2,1,0:T(8,128)(2,1)} %broadcast_in_dim.34), calls=%async_computation.3 | async-start | bytes 2097152 | tf_op jit(solution)/shard_map/all_to_all | solution.py:23
  96.8 6.3 %shard_map.84 = (bf16[2048,256]{1,0:T(8,128)(2,1)S(1)}, f32[8,256]{1,0:T(8,128)S(1)}, bf16[272,256]{1,0:T(8,128)(2,1)}) custom-call(s32[4]{0:T(128)S(1)} %pad_add_fusion.ids, bf16[272,2048]{1,0:T(8,128)(2,1)S(1)} %shard_map.82.b0, bf16[272,2048]{1,0:T(8,128)(2,1)} %collective-permute-done.s0, bf16[272,2048]{1,0:T(8,128)(2,1)} %collective-permute-done.1.b1, ...), custom_call_target="tpu_custom_call" | custom-call | flops 20000000000 | bytes 4194304 | tf_op jit(solution)/shard_map/pallas_call | solution.py:155
  104.1 3.4 %collective-permute-start.7 = (bf16[272,256]{1,0:T(8,128)(2,1)}, bf16[272,256]{1,0:T(8,128)(2,1)S(1)}, u32[]{:S(2)}, u32[]{:S(2)}) collective-permute-start(bf16[272,256]{1,0:T(8,128)(2,1)} %get-tuple-element.17), channel_id=1, source_target_pairs={{0,32},{32,64},{64,96},{96,128},{128,160},{160,192},{192,224},{224... | collective-permute-start | bytes 417800 | tf_op jit(solution)/shard_map/ppermute | solution.py:233
  107.5 5.3 %all-to-all-done.3.w_mine = bf16[4,256,512]{2,1,0:T(8,128)(2,1)S(1)} async-done(((bf16[4,256,512]{2,1,0:T(8,128)(2,1)}), bf16[4,256,512]{2,1,0:T(8,128)(2,1)S(1)}, u32[]{:S(2)}, u32[]{:S(2)}) %all-to-all-start.3) | async-done | bytes 1048608 | tf_op jit(solution)/shard_map/all_to_all | solution.py:23
  112.8 1.9 %collective-permute-start.8 = (bf16[4,256,512]{2,1,0:T(8,128)(2,1)S(1)}, bf16[4,256,512]{2,1,0:T(8,128)(2,1)S(1)}, u32[]{:S(2)}, u32[]{:S(2)}) collective-permute-start(bf16[4,256,512]{2,1,0:T(8,128)(2,1)S(1)} %all-to-all-done.3.w_mine), channel_id=1, source_target_pairs={{0,4},{4,0},{1,5},{5,1},{2,6},{6,2},{3,7},{7,3},{8,12},{12,8},{9,1... | collective-permute-start | bytes 3145736 | tf_op jit(solution)/shard_map/ppermute | solution.py:223
  114.7 1.2 copy-done.9
  115.9 4.2 %shard_map.85.later = bf16[8,128,128]{2,1,0:T(8,128)(2,1)S(1)} custom-call(bf16[2048,256]{1,0:T(8,128)(2,1)S(1)} %copy-done.9, f32[8,256]{1,0:T(8,128)S(1)} %get-tuple-element.18.docs, f32[1,512]{1,0:T(1,128)S(1)} %maximum_maximum_fusion.line), custom_call_target="tpu_custom_call" | custom-call | flops 20000000000 | bytes 4194304 | tf_op jit(solution)/shard_map/pallas_call | solution.py:155
  120.2 1.4 shard_map.86
  121.6 9.9 %all_to_all.31.att = bf16[8,128,128]{2,1,0:T(8,128)(2,1)S(1)} all-to-all(bf16[8,128,128]{2,1,0:T(8,128)(2,1)S(1)} %shard_map.86), channel_id=1, replica_groups=mesh['z'=16,'x'=4,'c'=2,'tp'=4] {'x','c'}, dimensions={0} | all-to-all | bytes 524288 | tf_op jit(solution)/shard_map/all_to_all | solution.py:237
  131.5 1.5 shard_map.88
  133.0 19.0 %all_to_all.32.partial = bf16[4,64,2048]{2,1,0:T(8,128)(2,1)S(1)} all-to-all(bf16[4,64,2048]{2,1,0:T(8,128)(2,1)S(1)} %bitcast.19), channel_id=1, replica_groups=mesh['z'=16,'x'=4,'c'=2,'tp'=4] {'tp'}, dimensions={0} | all-to-all | bytes 2097152 | tf_op jit(solution)/shard_map/all_to_all | solution.py:243
  152.2 16.0 %all_to_all.33 = bf16[4,64,2048]{2,1,0:T(8,128)(2,1)S(1)} all-to-all(bf16[4,64,2048]{2,1,0:T(8,128)(2,1)S(1)} %shard_map.89), channel_id=1, replica_groups=mesh['z'=16,'x'=4,'c'=2,'tp'=4] {'tp'}, dimensions={0} | all-to-all | bytes 2097152 | tf_op jit(solution)/shard_map/all_to_all | solution.py:245
  (45 shorter events, 9.0 us)
Async XLA Ops:
  0.0 89.4 %copy-start = (f32[1,8,257]{2,1,0:T(8,128)S(1)}, f32[1,8,257]{2,1,0:T(8,128)}, u32[]{:S(2)}) copy-start(f32[1,8,257]{2,1,0:T(8,128)} %param.15) | copy-start | bytes 24676
  0.1 0.8 copy-start.2
  0.9 0.7 copy-start.3
  1.6 0.7 copy-start.4
  2.4 0.7 copy-start.5
  14.6 15.4 %copy-start.1 = (bf16[256,2048]{1,0:T(8,128)(2,1)S(1)}, bf16[256,2048]{1,0:T(8,128)(2,1)}, u32[]{:S(2)}) copy-start(bf16[256,2048]{1,0:T(8,128)(2,1)} %tokens.1) | copy-start | bytes 3145732
  14.6 15.4 %copy-start.6 = (f32[1,2048]{1,0:T(1,128)S(1)}, f32[1,2048]{1,0:T(1,128)}, u32[]{:S(2)}) copy-start(f32[1,2048]{1,0:T(1,128)} %gain.1) | copy-start | bytes 24580
  14.6 15.4 %copy-start.7 = (s32[256]{0:T(256)S(1)}, s32[256]{0:T(256)}, u32[]{:S(2)}) copy-start(s32[256]{0:T(256)} %param.9) | copy-start | bytes 3076
  14.6 77.4 %all-to-all-start.1 = ((bf16[16,128,256]{2,1,0:T(8,128)(2,1)}), bf16[16,128,256]{2,1,0:T(8,128)(2,1)S(1)}, u32[]{:S(2)}, u32[]{:S(2)}) async-start(bf16[16,128,256]{2,1,0:T(8,128)(2,1)} %broadcast_in_dim.30), calls=%async_computation.1 | async-start | bytes 2097152 | tf_op jit(solution)/shard_map/all_to_all | solution.py:23
  30.4 52.7 %collective-permute-start.1 = (bf16[272,2048]{1,0:T(8,128)(2,1)S(1)}, bf16[272,2048]{1,0:T(8,128)(2,1)}, u32[]{:S(2)}, u32[]{:S(2)}) collective-permute-start(bf16[272,2048]{1,0:T(8,128)(2,1)S(1)} %shard_map.82.b0), channel_id=1, source_target_pairs={{0,8},{8,16},{16,24},{24,0},{1,9},{9,17},{17,25},{25,1},{2,10},{10... | collective-permute-start | bytes 3342344 | tf_op jit(solution)/shard_map/ppermute | solution.py:217
  32.9 52.2 %collective-permute-start.3 = (bf16[272,2048]{1,0:T(8,128)(2,1)S(1)}, bf16[272,2048]{1,0:T(8,128)(2,1)}, u32[]{:S(2)}, u32[]{:S(2)}) collective-permute-start(bf16[272,2048]{1,0:T(8,128)(2,1)S(1)} %shard_map.82.b0), channel_id=1, source_target_pairs={{0,16},{8,24},{16,0},{24,8},{1,17},{9,25},{17,1},{25,9},{2,18},{10... | collective-permute-start | bytes 3342344 | tf_op jit(solution)/shard_map/ppermute | solution.py:217
  36.8 50.6 %collective-permute-start.5 = (bf16[272,2048]{1,0:T(8,128)(2,1)S(1)}, bf16[272,2048]{1,0:T(8,128)(2,1)}, u32[]{:S(2)}, u32[]{:S(2)}) collective-permute-start(bf16[272,2048]{1,0:T(8,128)(2,1)S(1)} %shard_map.82.b0), channel_id=1, source_target_pairs={{0,24},{8,0},{16,8},{24,16},{1,25},{9,1},{17,9},{25,17},{2,26},{10... | collective-permute-start | bytes 3342344 | tf_op jit(solution)/shard_map/ppermute | solution.py:217
  39.7 57.1 %collective-permute-start = (bf16[272,2048]{1,0:T(8,128)(2,1)S(1)}, bf16[272,2048]{1,0:T(8,128)(2,1)}, u32[]{:S(2)}, u32[]{:S(2)}) collective-permute-start(bf16[272,2048]{1,0:T(8,128)(2,1)S(1)} %shard_map.82.b0), channel_id=1, source_target_pairs={{0,4},{4,0},{1,5},{5,1},{2,6},{6,2},{3,7},{7,3},{8,12},{12,8},{9,1... | collective-permute-start | bytes 3342344 | tf_op jit(solution)/shard_map/ppermute | solution.py:213
  83.1 13.7 %collective-permute-start.2 = (bf16[272,2048]{1,0:T(8,128)(2,1)}, bf16[272,2048]{1,0:T(8,128)(2,1)}, u32[]{:S(2)}, u32[]{:S(2)}) collective-permute-start(bf16[272,2048]{1,0:T(8,128)(2,1)} %collective-permute-done.1.b1), channel_id=1, source_target_pairs={{0,4},{4,0},{1,5},{5,1},{2,6},{6,2},{3,7},{7,3},{8,12},{12,8},{9,1... | collective-permute-start | bytes 3342344 | tf_op jit(solution)/shard_map/ppermute | solution.py:218
  85.0 11.8 %collective-permute-start.4 = (bf16[272,2048]{1,0:T(8,128)(2,1)}, bf16[272,2048]{1,0:T(8,128)(2,1)}, u32[]{:S(2)}, u32[]{:S(2)}) collective-permute-start(bf16[272,2048]{1,0:T(8,128)(2,1)} %collective-permute-done.3.b2), channel_id=1, source_target_pairs={{0,4},{4,0},{1,5},{5,1},{2,6},{6,2},{3,7},{7,3},{8,12},{12,8},{9,1... | collective-permute-start | bytes 3342344 | tf_op jit(solution)/shard_map/ppermute | solution.py:218
  87.5 9.4 %collective-permute-start.6 = (bf16[272,2048]{1,0:T(8,128)(2,1)}, bf16[272,2048]{1,0:T(8,128)(2,1)}, u32[]{:S(2)}, u32[]{:S(2)}) collective-permute-start(bf16[272,2048]{1,0:T(8,128)(2,1)} %collective-permute-done.5.b3), channel_id=1, source_target_pairs={{0,4},{4,0},{1,5},{5,1},{2,6},{6,2},{3,7},{7,3},{8,12},{12,8},{9,1... | collective-permute-start | bytes 3342344 | tf_op jit(solution)/shard_map/ppermute | solution.py:218
  93.3 19.5 %all-to-all-start.3 = ((bf16[4,256,512]{2,1,0:T(8,128)(2,1)}), bf16[4,256,512]{2,1,0:T(8,128)(2,1)S(1)}, u32[]{:S(2)}, u32[]{:S(2)}) async-start(bf16[4,256,512]{2,1,0:T(8,128)(2,1)} %broadcast_in_dim.34), calls=%async_computation.3 | async-start | bytes 2097152 | tf_op jit(solution)/shard_map/all_to_all | solution.py:23
  103.1 1.0 copy-start.8
  104.1 16.1 %collective-permute-start.7 = (bf16[272,256]{1,0:T(8,128)(2,1)}, bf16[272,256]{1,0:T(8,128)(2,1)S(1)}, u32[]{:S(2)}, u32[]{:S(2)}) collective-permute-start(bf16[272,256]{1,0:T(8,128)(2,1)} %get-tuple-element.17), channel_id=1, source_target_pairs={{0,32},{32,64},{64,96},{96,128},{128,160},{160,192},{192,224},{224... | collective-permute-start | bytes 417800 | tf_op jit(solution)/shard_map/ppermute | solution.py:233
  112.8 18.7 %collective-permute-start.8 = (bf16[4,256,512]{2,1,0:T(8,128)(2,1)S(1)}, bf16[4,256,512]{2,1,0:T(8,128)(2,1)S(1)}, u32[]{:S(2)}, u32[]{:S(2)}) collective-permute-start(bf16[4,256,512]{2,1,0:T(8,128)(2,1)S(1)} %all-to-all-done.3.w_mine), channel_id=1, source_target_pairs={{0,4},{4,0},{1,5},{5,1},{2,6},{6,2},{3,7},{7,3},{8,12},{12,8},{9,1... | collective-permute-start | bytes 3145736 | tf_op jit(solution)/shard_map/ppermute | solution.py:223
  114.7 1.2 copy-start.9
